TPU v7x, 32 devices: a whole 2x2x4 slice. The times are simulated.
32 devices in a mesh: ep: 4 (over y, x), tp: 8 (over z, core).
Axes of the slice: x: 2, y: 2, z: 4, core: 2. Of those that a mesh axis runs over, the one named last changes fastest.
Arguments:
- tokens: bfloat16 [64, 4096], P('ep'), may hold values from -6 to 6
- query_weight: bfloat16 [4096, 4096], P('ep', 'tp'), may hold values from -0.09375 to 0.09375
- key_weight: bfloat16 [4096, 2048], P('ep', 'tp'), may hold values from -0.15625 to 0.15625
- value_weight: bfloat16 [4096, 2048], P('ep', 'tp'), may hold values from -0.09375 to 0.09375
- out_weight: bfloat16 [4096, 4096], P('tp', 'ep'), may hold values from -0.09375 to 0.09375
- head_lambda: float32 [32], P('tp'), may hold values from 0.3 to 0.8
- head_gain: float32 [128], replicated, may hold values from 0.1 to 1.9
- key_cache: bfloat16 [64, 1024, 16, 128], P('ep', None, 'tp'), may hold values from -1000 to 1000
- value_cache: bfloat16 [64, 1024, 16, 128], P('ep', None, 'tp'), may hold values from -6 to 6
- lengths: int32 [64], P('ep'), may hold values from 128 to 1024, as said below
- first_gain: float32 [4096], replicated, may hold values from 0.3 to 3
- second_gain: float32 [4096], P('tp'), may hold values from 0.1 to 1.9
- expert_ids: int32 [64, 2], P('ep'), may hold values from 0 to 15, all different within a row; in each aligned block of 16 rows (0 to 15, 16 to 31, ...) at most 4 rows name the same one
- route_weights: float32 [64, 2], P('ep'), may hold values from 0.1 to 1
- expert_gate: bfloat16 [16, 4096, 2048], P('ep', 'tp'), may hold values from -0.09375 to 0.09375
- expert_up: bfloat16 [16, 4096, 2048], P('ep', 'tp'), may hold values from -0.09375 to 0.09375
- expert_down: bfloat16 [16, 2048, 4096], P('ep', None, 'tp'), may hold values from -0.125 to 0.125
- dense_gate: bfloat16 [4096, 2048], P('tp', 'ep'), may hold values from -0.09375 to 0.09375
- dense_up: bfloat16 [4096, 2048], P('tp', 'ep'), may hold values from -0.09375 to 0.09375
- dense_down: bfloat16 [2048, 4096], P('ep', 'tp'), may hold values from -0.25 to 0.25
- dense_mix: bfloat16 [4096], replicated, may hold values from -0.09375 to 0.09375
Outputs:
- layer_out: bfloat16 [64, 4096], P('ep', 'tp')
Inputs may be any that keep to these rules, and one draw needn't show every extreme that they name: `lengths`: positions below a sequence's length hold its cache; the new token stands at that position. Some sequence has length 1024 in every draw. `expert_ids`: each row names 2 different experts. Among the rows of one device's 16 sequences (aligned blocks) no expert is named more than 4 times, and in every draw some expert is named exactly 4 times in some block.
All inputs are finite; a program needn't handle non-finite values.
Results may differ from a plain program's by a relative error of at most 0.04.
Values may be sent and summed in bfloat16 or wider, within the bound.
No kernel may reach another device: no remote copies, remote signals or barrier semaphores. Data moves between devices by JAX's collectives and lax.ppermute only.
A program may use at most 128 MiB of HBM per device.

v0:
```python
import jax
import jax.numpy as jnp
from jax import lax
from jax.sharding import PartitionSpec as P

SUB = 64
VD = 128
EXPERTS = 16
TOPK = 2
CACHE = 1024
CAP = 4


theta_base = 500000.0
score_scale = 0.125
head_scale = 0.8
residual_scale = 2.0**0.5
layer_epsilon = 1e-05
head_epsilon = 1e-06


def rotate(vector, cosine, sine_table):
    middle = vector.shape[-1] // 2
    lower = vector[..., :middle]
    upper = vector[..., middle:]
    return jnp.concatenate(
        [lower * cosine - upper * sine_table, upper * cosine + lower * sine_table], axis=-1
    )


def widened(array):
    return lax.optimization_barrier(array.astype(jnp.bfloat16)).astype(jnp.float32)


def attend(query_sum, key_sum, value_sum, head_lambda, head_gain, key_cache, value_cache, lengths):
    seq_count = key_cache.shape[0]
    kv_local = key_cache.shape[2]
    group_size = query_sum.shape[1] // (kv_local * 2 * SUB)
    frequency = theta_base ** (-(jnp.arange(SUB // 2, dtype=jnp.float32) * (2.0 / SUB)))
    angles = lengths.astype(jnp.float32)[:, None] * frequency[None, :]
    cosine = jnp.cos(angles)
    sine_table = jnp.sin(angles)
    query_half = widened(query_sum).reshape(seq_count, kv_local, group_size, 2, SUB)
    query_rot = rotate(
        query_half, cosine[:, None, None, None, :], sine_table[:, None, None, None, :]
    )
    query_rot = query_rot.astype(jnp.bfloat16)
    key_half = widened(key_sum).reshape(seq_count, kv_local, 2, SUB)
    key_rot = rotate(key_half, cosine[:, None, None, :], sine_table[:, None, None, :]).astype(
        jnp.bfloat16
    )
    value_new = widened(value_sum).reshape(seq_count, kv_local, 1, VD)
    cached_keys = key_cache.reshape(seq_count, CACHE, kv_local, 2, SUB)
    scores = jnp.einsum(
        "skgcd,sjkcd->skgcj", query_rot, cached_keys, preferred_element_type=jnp.float32
    )
    scores = scores * score_scale
    valid = jnp.arange(CACHE, dtype=jnp.int32)[None, :] < lengths[:, None]
    scores = jnp.where(valid[:, None, None, None, :], scores, -jnp.inf)
    fresh_score = jnp.einsum(
        "skgcd,skcd->skgc", query_rot, key_rot, preferred_element_type=jnp.float32
    )
    fresh_score = fresh_score * score_scale
    highest = jnp.maximum(jnp.max(scores, axis=-1), fresh_score)
    cached_exp = jnp.exp(scores - highest[..., None])
    fresh_exp = jnp.exp(fresh_score - highest)
    denominator = jnp.sum(cached_exp, axis=-1) + fresh_exp
    cached_prob = cached_exp / denominator[..., None]
    fresh_prob = fresh_exp / denominator
    lambdas = head_lambda.reshape(kv_local, group_size)
    mixed_map = (
        cached_prob[:, :, :, 0] - lambdas[None, :, :, None] * cached_prob[:, :, :, 1]
    ).astype(jnp.bfloat16)
    mixed_new = widened(fresh_prob[..., 0] - lambdas[None] * fresh_prob[..., 1])
    head_out = jnp.einsum(
        "skgj,sjke->skge", mixed_map, value_cache, preferred_element_type=jnp.float32
    )
    head_out = head_out + mixed_new[..., None] * value_new
    square_mean = jnp.mean(head_out * head_out, axis=-1, keepdims=True)
    normed = head_out * lax.rsqrt(square_mean + head_epsilon) * head_gain * head_scale
    return normed.astype(jnp.bfloat16).reshape(seq_count, kv_local * group_size * VD)


def on_device(
    tokens,
    query_weight,
    key_weight,
    value_weight,
    out_weight,
    head_lambda,
    head_gain,
    key_cache,
    value_cache,
    lengths,
    first_gain,
    second_gain,
    expert_ids,
    route_weights,
    expert_gate,
    expert_up,
    expert_down,
    dense_gate,
    dense_up,
    dense_down,
    dense_mix,
):
    seq_count = tokens.shape[0]
    model_width = tokens.shape[1]
    ep_count = lax.axis_size("ep")
    tp_count = lax.axis_size("tp")
    query_cols = query_weight.shape[1]
    key_cols = key_weight.shape[1]
    columns = lax.all_to_all(tokens, "ep", split_axis=1, concat_axis=0, tiled=True)
    summed = lax.psum_scatter(
        jnp.concatenate(
            [
                jnp.dot(columns, query_weight, preferred_element_type=jnp.float32),
                jnp.dot(columns, key_weight, preferred_element_type=jnp.float32),
                jnp.dot(columns, value_weight, preferred_element_type=jnp.float32),
            ],
            axis=1,
        ).astype(jnp.bfloat16),
        "ep",
        scatter_dimension=0,
        tiled=True,
    ).astype(jnp.float32)
    query_sum = summed[:, :query_cols]
    key_sum = summed[:, query_cols : query_cols + key_cols]
    value_sum = summed[:, query_cols + key_cols :]
    normed = attend(
        query_sum, key_sum, value_sum, head_lambda, head_gain, key_cache, value_cache, lengths
    )
    all_heads = lax.all_gather(normed, "ep", axis=0, tiled=True)
    column_part = jnp.dot(all_heads, out_weight, preferred_element_type=jnp.float32)
    column_part = lax.psum(column_part.astype(jnp.bfloat16), "tp").astype(jnp.float32)
    attention = lax.all_to_all(
        column_part.astype(jnp.bfloat16), "ep", split_axis=0, concat_axis=1, tiled=True
    )
    residual_in = residual_scale * tokens.astype(jnp.float32) + widened(attention)
    average = jnp.mean(residual_in, axis=-1, keepdims=True)
    centered = residual_in - average
    variance = jnp.mean(centered * centered, axis=-1, keepdims=True)
    hidden_in = (centered * lax.rsqrt(variance + layer_epsilon) * first_gain).astype(jnp.bfloat16)
    slice_width = model_width // tp_count
    own_cols = lax.dynamic_slice_in_dim(
        hidden_in, lax.axis_index("tp") * slice_width, slice_width, 1
    )
    flat_ids = expert_ids.reshape(-1)
    hit_table = (flat_ids[:, None] == jnp.arange(EXPERTS, dtype=jnp.int32)[None, :]).astype(
        jnp.int32
    )
    earlier = jnp.cumsum(hit_table, axis=0) - hit_table
    slot_index = jnp.sum(earlier * hit_table, axis=1)
    target = flat_ids * CAP + slot_index
    placed = jnp.arange(EXPERTS * CAP, dtype=jnp.int32)[:, None] == target[None, :]
    routed_rows = jnp.repeat(own_cols, TOPK, axis=0)
    packed = jnp.dot(placed.astype(jnp.bfloat16), routed_rows, preferred_element_type=jnp.float32)
    packed = packed.astype(jnp.bfloat16).reshape(ep_count, EXPERTS // ep_count, CAP, slice_width)
    arrived = lax.all_to_all(packed, "ep", split_axis=0, concat_axis=2, tiled=True)[0]
    expert_pre_gate = jnp.einsum(
        "erd,edf->erf", arrived, expert_gate, preferred_element_type=jnp.float32
    )
    expert_pre_up = jnp.einsum(
        "erd,edf->erf", arrived, expert_up, preferred_element_type=jnp.float32
    )
    all_rows = lax.all_gather(own_cols, "ep", axis=0, tiled=True)
    dense_pre_gate = jnp.dot(all_rows, dense_gate, preferred_element_type=jnp.float32)
    dense_pre_up = jnp.dot(all_rows, dense_up, preferred_element_type=jnp.float32)
    expert_pre_gate, expert_pre_up, dense_pre_gate, dense_pre_up = (
        lax.psum(expert_pre_gate.astype(jnp.bfloat16), "tp").astype(jnp.float32),
        lax.psum(expert_pre_up.astype(jnp.bfloat16), "tp").astype(jnp.float32),
        lax.psum(dense_pre_gate.astype(jnp.bfloat16), "tp").astype(jnp.float32),
        lax.psum(dense_pre_up.astype(jnp.bfloat16), "tp").astype(jnp.float32),
    )
    expert_hidden = (jax.nn.silu(expert_pre_gate) * expert_pre_up).astype(jnp.bfloat16)
    expert_result = jnp.einsum(
        "erf,efd->erd", expert_hidden, expert_down, preferred_element_type=jnp.float32
    )
    expert_result = expert_result.astype(jnp.bfloat16)
    local_experts = expert_result.shape[0]
    expert_result = expert_result.reshape(1, local_experts, ep_count, CAP, slice_width)
    returned = lax.all_to_all(expert_result, "ep", split_axis=2, concat_axis=0, tiled=True).reshape(
        EXPERTS * CAP, slice_width
    )
    route_gates = route_weights / jnp.sum(route_weights, axis=-1, keepdims=True)
    weighted = placed.astype(jnp.float32) * route_gates.reshape(-1)[None, :]
    combine_matrix = jnp.sum(weighted.T.reshape(seq_count, TOPK, EXPERTS * CAP), axis=1)
    expert_mix = jnp.dot(
        combine_matrix, returned.astype(jnp.float32), precision=lax.Precision.HIGHEST
    )
    dense_hidden = (jax.nn.silu(dense_pre_gate) * dense_pre_up).astype(jnp.bfloat16)
    dense_part = jnp.dot(dense_hidden, dense_down, preferred_element_type=jnp.float32)
    dense_out = widened(
        lax.psum_scatter(
            dense_part.astype(jnp.bfloat16), "ep", scatter_dimension=0, tiled=True
        ).astype(jnp.float32)
    )
    mix_gate = jax.nn.sigmoid(jnp.dot(hidden_in, dense_mix, preferred_element_type=jnp.float32))
    combined = (
        residual_scale * own_cols.astype(jnp.float32) + expert_mix + mix_gate[:, None] * dense_out
    )
    moments = lax.psum((jnp.sum(combined, axis=1), jnp.sum(combined * combined, axis=1)), "tp")
    average = moments[0] / model_width
    variance = moments[1] / model_width - average * average
    layer_out = (
        (combined - average[:, None]) * lax.rsqrt(variance + layer_epsilon)[:, None] * second_gain
    )
    return layer_out.astype(jnp.bfloat16)


def solution(mesh):
    return jax.shard_map(
        on_device,
        mesh=mesh,
        in_specs=(
            P("ep", None),
            P("ep", "tp"),
            P("ep", "tp"),
            P("ep", "tp"),
            P("tp", "ep"),
            P("tp"),
            P(),
            P("ep", None, "tp", None),
            P("ep", None, "tp", None),
            P("ep"),
            P(),
            P("tp"),
            P("ep", None),
            P("ep", None),
            P("ep", "tp", None),
            P("ep", "tp", None),
            P("ep", None, "tp"),
            P("tp", "ep"),
            P("tp", "ep"),
            P("ep", "tp"),
            P(),
        ),
        out_specs=P("ep", "tp"),
        check_vma=False,
    )
```

profile of v0, /device:TPU:0, one launch (start us, length us, event | category | flops | bytes accessed | tf_op | source)
XLA Modules:
  0.0 277.1 jit_solution(7512981496425636407)
XLA Ops:
  6.5 1.7 copy.150
  8.2 5.2 %all-to-all-start = ((bf16[16,4,1024]{2,0,1:T(8,128)(2,1)}), bf16[16,4,1024]{2,0,1:T(8,128)(2,1)S(1)}, u32[]{:S(2)}, u32[]{:S(2)}) async-start(bf16[16,4,1024]{2,0,1:T(8,128)(2,1)} %bitcast.102), calls=%async_computation | async-start | bytes 262144 | tf_op jit(solution)/shard_map/all_to_all | solution.py:113
  13.4 0.7 iota_compare_fusion
  14.1 0.8 copy.126
  14.9 0.1 eq.37
  15.1 0.2 select_reduce_fusion.1
  15.3 3.1 %all-to-all-done = bf16[16,4,1024]{2,0,1:T(8,128)(2,1)S(1)} async-done(((bf16[16,4,1024]{2,0,1:T(8,128)(2,1)}), bf16[16,4,1024]{2,0,1:T(8,128)(2,1)S(1)}, u32[]{:S(2)}, u32[]{:S(2)}) %all-to-all-start) | async-done | bytes 131104 | tf_op jit(solution)/shard_map/all_to_all | solution.py:113
  18.4 1.5 convolution_convert_fusion.3
  19.9 1.2 convolution_convert_fusion.10
  21.2 1.2 convolution_convert_fusion.9
  22.4 0.7 pad_maximum_fusion
  23.2 0.7 convert_element_type.96
  23.9 21.2 %copy.117 = bf16[16,1024,2,128]{1,3,2,0:T(8,128)(2,1)} copy(bf16[16,1024,2,128]{3,2,1,0:T(2,128)(2,1)} %param.28) | data formatting | bytes 16777216 | tf_op args[7]
  45.0 0.1 mul.298
  45.2 0.1 copy.127
  45.3 0.1 multiply_cosine_fusion
  45.4 1.8 reduce-scatter.3.cloned.1.call-done
  47.2 0.7 fusion.48
  47.9 0.1 reshape.222
  48.0 0.7 slice.47
  48.7 0.1 reshape.220
  48.8 0.1 fusion.46
  49.0 0.1 subtract_convert_fusion.1
  49.1 0.1 maximum_bitcast_fusion
  49.2 0.1 subtract_convert_fusion
  49.3 0.3 fusion.35
  49.6 4.8 %fusion.49 = (f32[16,2,2,2]{2,3,1,0:T(2,128)S(1)}, f32[16,2,2,2,1024]{4,2,3,1,0:T(2,128)S(1)}) fusion(bf16[16,1024,2,2,64]{1,4,3,2,0:T(8,128)(2,1)} %bitcast.103, bf16[16,2,2,2,32]{4,2,3,1,0:T(2,128)(2,1)S(1)} %get-tuple-element.14, bf16[16,2,2,2,32]{4,2,3,1,0:T(2,128)(2,1)S(1)} %get-tuple-element.13, pred[16,1024]{1,0:T(8,128)(4,1)S(1)} %iota_compare_fusion), kind=kOutput, calls=%fused_computation.101 | convolution fusion | flops 17203072 | bytes 8946176 | tf_op jit(solution)/shard_map/skgcd,sjkcd->skgcj/dot_general | solution.py:54
  54.5 0.6 fusion.18
  55.1 0.5 fusion.17
  55.6 0.1 copy.120
  55.7 0.1 copy.121
  55.9 0.1 copy.122
  56.0 4.9 %multiply_reduce_fusion.2 = (f32[16,2,2]{2,1,0:T(2,128)S(1)}, f32[16,2,2,128]{3,2,1,0:T(2,128)S(1)}) fusion(f32[16,2,128]{2,1,0:T(2,128)S(1)} %reshape.223, f32[16,2,2]{2,1,0:T(2,128)S(1)} %copy.122, bf16[16,1024,2,128]{3,2,1,0:T(2,128)(2,1)} %param.29, f32[16,2,2,2,1024]{4,2,3,1,0:T(2,128)S(1)} %fusion.17, f32[2,2]{1,0:T(2,128)S(1)} %mul.298), kind=kOutput, calls=%fused_computation.66 | convolution fusion | flops 17006528 | bytes 8962576 | tf_op jit(solution)/shard_map/skgj,sjke->skge/dot_general | solution.py:75
  60.9 0.1 copy.123
  61.0 0.1 copy.124
  61.1 0.1 multiply_convert_fusion.2
  61.2 8.2 %all_gather.6 = bf16[64,512]{1,0:T(8,128)(2,1)S(1)} all-gather(bf16[16,512]{1,0:T(8,128)(2,1)S(1)} %reshape.214), channel_id=1, replica_groups=mesh['ep'=4,'tp'=8] {'ep'}, dimensions={0}, use_global_device_ids=true | all-gather | bytes 81920 | tf_op jit(solution)/shard_map/all_gather | solution.py:133
  69.4 1.0 convolution_convert_fusion.2
  70.4 55.1 %all-reduce.5.cloned.1.call-done = bf16[4,16,1024]{2,1,0:T(8,128)(2,1)} async-done(((bf16[4,16,1024]{2,1,0:T(8,128)(2,1)}), bf16[4,16,1024]{2,1,0:T(8,128)(2,1)}) %all-reduce.5.cloned.1.call-update) | async-done | bytes 131088 | tf_op jit(solution)/shard_map/psum | solution.py:135
  125.5 3.6 %all-to-all-start.1 = ((bf16[4,16,1024]{2,1,0:T(8,128)(2,1)}), bf16[4,16,1024]{2,1,0:T(8,128)(2,1)S(1)}, u32[]{:S(2)}, u32[]{:S(2)}) async-start(bf16[4,16,1024]{2,1,0:T(8,128)(2,1)} %all-reduce.5.cloned.1.call-done), calls=%async_computation.2 | async-start | bytes 262144 | tf_op jit(solution)/shard_map/all_to_all | solution.py:136
  129.2 5.0 %all-to-all-done.1 = bf16[4,16,1024]{2,1,0:T(8,128)(2,1)S(1)} async-done(((bf16[4,16,1024]{2,1,0:T(8,128)(2,1)}), bf16[4,16,1024]{2,1,0:T(8,128)(2,1)S(1)}, u32[]{:S(2)}, u32[]{:S(2)}) %all-to-all-start.1) | async-done | bytes 131104 | tf_op jit(solution)/shard_map/all_to_all | solution.py:136
  134.2 0.2 fusion.24
  134.4 0.2 multiply_reduce_fusion
  134.6 0.1 multiply_convert_fusion
  134.8 7.6 %all_gather.7 = bf16[64,512]{1,0:T(8,128)(2,1)S(1)} all-gather(bf16[16,512]{1,0:T(8,128)(2,1)S(1)} %constant_dynamic-slice_fusion), channel_id=1, replica_groups=mesh['ep'=4,'tp'=8] {'ep'}, dimensions={0}, use_global_device_ids=true | all-gather | bytes 81920 | tf_op jit(solution)/shard_map/all_gather | solution.py:166
  142.4 0.1 convolution_convert_fusion.8
  142.6 0.6 reshape.216
  143.2 3.3 %all-to-all-start.2 = ((bf16[4,4,4,512]{3,2,1,0:T(4,128)(2,1)}), bf16[4,4,4,512]{3,2,1,0:T(4,128)(2,1)S(1)}, u32[]{:S(2)}, u32[]{:S(2)}) async-start(bf16[4,4,4,512]{3,2,1,0:T(4,128)(2,1)} %reshape.216), calls=%async_computation.3 | async-start | bytes 131072 | tf_op jit(solution)/shard_map/all_to_all | solution.py:159
  146.6 0.8 convolution_convert_fusion.5
  147.4 0.8 convolution_convert_fusion.6
  148.3 3.1 %all-to-all-done.2 = bf16[4,4,4,512]{3,2,1,0:T(4,128)(2,1)S(1)} async-done(((bf16[4,4,4,512]{3,2,1,0:T(4,128)(2,1)}), bf16[4,4,4,512]{3,2,1,0:T(4,128)(2,1)S(1)}, u32[]{:S(2)}, u32[]{:S(2)}) %all-to-all-start.2) | async-done | bytes 65568 | tf_op jit(solution)/shard_map/all_to_all | solution.py:159
  151.4 5.3 %convolution_convert_fusion = bf16[4,16,2048]{2,1,0:T(8,128)(2,1)} fusion(bf16[4,16,512]{2,1,0:T(8,128)(2,1)S(1)} %squeeze.19, bf16[4,512,2048]{2,1,0:T(8,128)(2,1)} %param.36), kind=kOutput, calls=%fused_computation.2 | convolution fusion | flops 134348800 | bytes 8716288 | tf_op jit(solution)/shard_map/erd,edf->erf/dot_general | solution.py:163
  156.7 5.4 %convolution_convert_fusion.1 = bf16[4,16,2048]{2,1,0:T(8,128)(2,1)} fusion(bf16[4,16,512]{2,1,0:T(8,128)(2,1)S(1)} %squeeze.19, bf16[4,512,2048]{2,1,0:T(8,128)(2,1)} %param.35), kind=kOutput, calls=%fused_computation.3 | convolution fusion | flops 134348800 | bytes 8716288 | tf_op jit(solution)/shard_map/erd,edf->erf/dot_general | solution.py:160
  162.2 54.9 %all-reduce.7.cloned.1.call-done = (bf16[4,16,2048]{2,1,0:T(8,128)(2,1)}, bf16[4,16,2048]{2,1,0:T(8,128)(2,1)}, bf16[64,512]{1,0:T(8,128)(2,1)}, bf16[64,512]{1,0:T(8,128)(2,1)}) async-done(((bf16[4,16,2048]{2,1,0:T(8,128)(2,1)}, bf16[4,16,2048]{2,1,0:T(8,128)(2,1)}, bf16[64,512]{1,0:T(8,128)(2,1)}, bf16[64,512]{1,0:T(8,128)(2,1)}), (bf16[4,16,2048]{2,1,0:T(8,128)(2,1)}, bf16[4,16,2048]{2,1,0:T(8,128)(2,1)}, ...) | async-done | bytes 655376 | tf_op jit(solution)/shard_map/psum | solution.py:171
  217.1 4.8 %convolution_convert_fusion.7 = bf16[4,16,512]{2,1,0:T(8,128)(2,1)S(1)} fusion(bf16[4,2048,512]{2,1,0:T(8,128)(2,1)} %param.37, bf16[4,16,2048]{2,1,0:T(8,128)(2,1)} %get-tuple-element.9, bf16[4,16,2048]{2,1,0:T(8,128)(2,1)} %get-tuple-element.10), kind=kOutput, calls=%fused_computation.12 | convolution fusion | flops 135299072 | bytes 8978432 | tf_op jit(solution)/shard_map/erf,efd->erd/dot_general | solution.py:176
  221.9 0.6 copy.129
  222.5 3.6 %all-to-all-start.3 = ((bf16[1,4,4,4,512]{4,3,1,0,2:T(4,128)(2,1)}), bf16[1,4,4,4,512]{4,3,1,0,2:T(4,128)(2,1)S(1)}, u32[]{:S(2)}, u32[]{:S(2)}) async-start(bf16[1,4,4,4,512]{4,3,1,0,2:T(4,128)(2,1)} %copy.129), calls=%async_computation.4 | async-start | bytes 131072 | tf_op jit(solution)/shard_map/all_to_all | solution.py:182
  226.2 0.8 convolution_convert_fusion.4
  227.1 0.1 fusion.11
  227.2 3.8 %all-to-all-done.3 = bf16[1,4,4,4,512]{4,3,1,0,2:T(4,128)(2,1)S(1)} async-done(((bf16[1,4,4,4,512]{4,3,1,0,2:T(4,128)(2,1)}), bf16[1,4,4,4,512]{4,3,1,0,2:T(4,128)(2,1)S(1)}, u32[]{:S(2)}, u32[]{:S(2)}) %all-to-all-start.3) | async-done | bytes 65568 | tf_op jit(solution)/shard_map/all_to_all | solution.py:182
  231.0 22.0 %reduce-scatter.5.cloned.1.call-done = bf16[16,512]{1,0:T(8,128)(2,1)} async-done(((bf16[64,512]{1,0:T(8,128)(2,1)}), bf16[16,512]{1,0:T(8,128)(2,1)}) %reduce-scatter.5.cloned.1.call-update) | async-done | bytes 16400 | tf_op jit(solution)/shard_map/reduce_scatter | solution.py:194
  253.1 1.0 fusion.45
  254.1 15.8 %all-reduce = (f32[16]{0:T(128)S(1)}, f32[16]{0:T(128)S(1)}) all-reduce(f32[16]{0:T(128)S(1)} %get-tuple-element.6, f32[16]{0:T(128)S(1)} %get-tuple-element.5), channel_id=1, replica_groups=mesh['ep'=4,'tp'=8] {'tp'}, use_global_device_ids=true, to_apply=%region_19.20 | all-reduce | flops 32 | bytes 256 | tf_op jit(solution)/shard_map/psum | solution.py:202
  269.9 0.7 multiply_convert_fusion.1
  (64 shorter events, 1.0 us)
Async XLA Ops:
  6.5 62.9 %copy-start = (bf16[512,1024]{1,0:T(8,128)(2,1)S(1)}, bf16[512,1024]{1,0:T(8,128)(2,1)}, u32[]{:S(2)}) copy-start(bf16[512,1024]{1,0:T(8,128)(2,1)} %param.25) | copy-start | bytes 3145732
  8.2 10.2 %all-to-all-start = ((bf16[16,4,1024]{2,0,1:T(8,128)(2,1)}), bf16[16,4,1024]{2,0,1:T(8,128)(2,1)S(1)}, u32[]{:S(2)}, u32[]{:S(2)}) async-start(bf16[16,4,1024]{2,0,1:T(8,128)(2,1)} %bitcast.102), calls=%async_computation | async-start | bytes 262144 | tf_op jit(solution)/shard_map/all_to_all | solution.py:113
  13.4 33.8 %reduce-scatter.3.cloned.1.call-start = ((), (), s32[]{:S(2)}) async-start(), calls=%async_computation.6 | async-start | bytes 163840 | tf_op jit(solution)/shard_map/reduce_scatter | solution.py:114
  23.1 102.4 %all-reduce.5.cloned.1.call-start = ((), (), s32[]{:S(2)}) async-start(), calls=%async_computation.7 | async-start | bytes 262144 | tf_op jit(solution)/shard_map/psum | solution.py:135
  23.9 21.2 %copy-start.13 = (f32[4]{0:T(128)S(1)}, f32[4]{0:T(128)}, u32[]{:S(2)}) copy-start(f32[4]{0:T(128)} %param.26) | copy-start | bytes 52
  54.3 6.7 %copy-start.9 = (f32[128]{0:T(128)S(1)}, f32[128]{0:T(128)}, u32[]{:S(2)}) copy-start(f32[128]{0:T(128)} %param.27) | copy-start | bytes 1540
  54.3 16.0 %copy-start.6 = (s32[16,2]{0,1:T(2,128)S(1)}, s32[16,2]{0,1:T(2,128)}, u32[]{:S(2)}) copy-start(s32[16,2]{0,1:T(2,128)} %param.33) | copy-start | bytes 388
  54.4 74.8 %copy-start.5 = (bf16[4096]{0:T(1024)(128)(2,1)S(1)}, bf16[4096]{0:T(1024)(128)(2,1)}, u32[]{:S(2)}) copy-start(bf16[4096]{0:T(1024)(128)(2,1)} %param.41) | copy-start | bytes 24580
  54.4 74.8 %copy-start.7 = (f32[16,2]{0,1:T(2,128)S(1)}, f32[16,2]{0,1:T(2,128)}, u32[]{:S(2)}) copy-start(f32[16,2]{0,1:T(2,128)} %param.34) | copy-start | bytes 388
  54.4 79.8 %copy-start.1 = (bf16[16,4096]{1,0:T(8,128)(2,1)S(1)}, bf16[16,4096]{1,0:T(8,128)(2,1)}, u32[]{:S(2)}) copy-start(bf16[16,4096]{1,0:T(8,128)(2,1)} %param.21) | copy-start | bytes 393220
  54.4 80.2 %copy-start.4 = (f32[4096]{0:T(1024)S(1)}, f32[4096]{0:T(1024)}, u32[]{:S(2)}) copy-start(f32[4096]{0:T(1024)} %param.31) | copy-start | bytes 49156
  54.4 92.2 %copy-start.2 = (bf16[512,512]{1,0:T(8,128)(2,1)S(1)}, bf16[512,512]{1,0:T(8,128)(2,1)}, u32[]{:S(2)}) copy-start(bf16[512,512]{1,0:T(8,128)(2,1)} %param.39) | copy-start | bytes 1572868
  54.4 93.0 %copy-start.3 = (bf16[512,512]{1,0:T(8,128)(2,1)S(1)}, bf16[512,512]{1,0:T(8,128)(2,1)}, u32[]{:S(2)}) copy-start(bf16[512,512]{1,0:T(8,128)(2,1)} %param.38) | copy-start | bytes 1572868
  125.5 8.7 %all-to-all-start.1 = ((bf16[4,16,1024]{2,1,0:T(8,128)(2,1)}), bf16[4,16,1024]{2,1,0:T(8,128)(2,1)S(1)}, u32[]{:S(2)}, u32[]{:S(2)}) async-start(bf16[4,16,1024]{2,1,0:T(8,128)(2,1)} %all-reduce.5.cloned.1.call-done), calls=%async_computation.2 | async-start | bytes 262144 | tf_op jit(solution)/shard_map/all_to_all | solution.py:136
  143.2 8.1 %all-to-all-start.2 = ((bf16[4,4,4,512]{3,2,1,0:T(4,128)(2,1)}), bf16[4,4,4,512]{3,2,1,0:T(4,128)(2,1)S(1)}, u32[]{:S(2)}, u32[]{:S(2)}) async-start(bf16[4,4,4,512]{3,2,1,0:T(4,128)(2,1)} %reshape.216), calls=%async_computation.3 | async-start | bytes 131072 | tf_op jit(solution)/shard_map/all_to_all | solution.py:159
  146.5 70.5 %all-reduce.7.cloned.1.call-start = ((), (), s32[]{:S(2)}) async-start(), calls=%async_computation.9 | async-start | bytes 1310720 | tf_op jit(solution)/shard_map/psum | solution.py:171
  156.7 69.5 %copy-start.10 = (bf16[512,512]{1,0:T(8,128)(2,1)S(1)}, bf16[512,512]{1,0:T(8,128)(2,1)}, u32[]{:S(2)}) copy-start(bf16[512,512]{1,0:T(8,128)(2,1)} %param.40) | copy-start | bytes 1572868
  156.7 113.2 %copy-start.8 = (f32[512]{0:T(512)S(1)}, f32[512]{0:T(512)}, u32[]{:S(2)}) copy-start(f32[512]{0:T(512)} %param.32) | copy-start | bytes 6148
  217.1 9.1 %copy-start.11 = (bf16[64,512]{1,0:T(8,128)(2,1)S(1)}, bf16[64,512]{1,0:T(8,128)(2,1)}, u32[]{:S(2)}) copy-start(bf16[64,512]{1,0:T(8,128)(2,1)} %get-tuple-element.11) | copy-start | bytes 196612
  217.1 9.1 %copy-start.12 = (bf16[64,512]{1,0:T(8,128)(2,1)S(1)}, bf16[64,512]{1,0:T(8,128)(2,1)}, u32[]{:S(2)}) copy-start(bf16[64,512]{1,0:T(8,128)(2,1)} %get-tuple-element.12) | copy-start | bytes 196612
  222.5 8.5 %all-to-all-start.3 = ((bf16[1,4,4,4,512]{4,3,1,0,2:T(4,128)(2,1)}), bf16[1,4,4,4,512]{4,3,1,0,2:T(4,128)(2,1)S(1)}, u32[]{:S(2)}, u32[]{:S(2)}) async-start(bf16[1,4,4,4,512]{4,3,1,0,2:T(4,128)(2,1)} %copy.129), calls=%async_computation.4 | async-start | bytes 131072 | tf_op jit(solution)/shard_map/all_to_all | solution.py:182
  226.2 26.9 %reduce-scatter.5.cloned.1.call-start = ((), (), s32[]{:S(2)}) async-start(), calls=%async_computation.8 | async-start | bytes 81920 | tf_op jit(solution)/shard_map/reduce_scatter | solution.py:194
Sparse Core Ops, SparseCore 0:
  23.3 23.8 reduce-scatter.2
  70.5 54.9 all-reduce.4
  162.2 54.8 all-reduce.6
  229.4 23.6 reduce-scatter.4
where the time goes:
time: 279 us; the launch traced here: 277 us
  waiting for transfers between devices  149 us (53%)
  matrix products  34 us (12%)
  blocking collectives  31.6 us (11%)
  local copies, waits for them, and re-layouts  27.8 us (10%)
  starting transfers between devices  15.9 us (6%)
  between operations  13.5 us (5%)
  other arithmetic  5.45 us (2%)
    psum x1, waiting for transfers between devices, on_device(): lax.psum(column_part.astype(jnp.bfloat16), 'tp').astype(jnp.float32)  55.1 us
    psum x1, waiting for transfers between devices, on_device(): lax.psum(expert_pre_up.astype(jnp.bfloat16), 'tp').astype(jnp.float32)  54.9 us
    reduce_scatter x1, waiting for transfers between devices, on_device(): lax.psum_scatter(dense_part.astype(jnp.bfloat16), 'ep', scatter_dimension...  22 us
    unnamed x31, local copies, waits for them, and re-layouts  22 us
    psum x1, blocking collectives, on_device(): lax.psum((jnp.sum(combined, axis=1), jnp.sum(combined * combined, axis=1)...  15.8 us
    all_gather x1, blocking collectives, on_device(): all_heads = lax.all_gather(normed, 'ep', axis=0, tiled=True)  8.17 us
    all_gather x1, blocking collectives, on_device(): all_rows = lax.all_gather(own_cols, 'ep', axis=0, tiled=True)  7.64 us
  transfers between devices with their start and end apart: 8, of which 8 were waited for; matrix products, arithmetic and copies ran while one was open for 10% of the time, Pallas kernels for 0%

commit v1 on v0

v1 whole, which is shorter than its diff:
```python
import jax
import jax.numpy as jnp
from jax import lax
from jax.experimental import pallas as pl
from jax.experimental.pallas import tpu as pltpu
from jax.sharding import PartitionSpec as P

SUB = 64
VD = 128
TOPK = 2
CAP = 4
LANES = 128
CHUNK = 256

theta_base = 500000.0
score_scale = 0.125
head_scale = 0.8
residual_scale = 2.0**0.5
layer_epsilon = 1e-05
head_epsilon = 1e-06

F32 = jnp.float32
BF16 = jnp.bfloat16


def xor_permute(array, axis, count, distance):
    return lax.ppermute(array, axis, [(i, i ^ distance) for i in range(count)])


def attend_kernel(
    lengths_ref,
    qkv_ref,
    cos_ref,
    sin_ref,
    lambda_ref,
    gain_ref,
    keys_ref,
    values_ref,
    out_ref,
    key_buf,
    value_buf,
    query_rows,
    key_rows,
    value_rows,
    score_buf,
    out_rows,
    sems,
    *,
    seq_count,
    kv_local,
    group_size,
    cache,
):
    heads = kv_local * group_size
    chunks = cache // CHUNK
    span = CHUNK * kv_local

    def copy(which, s, c):
        source, target = (keys_ref, key_buf) if which == 0 else (values_ref, value_buf)
        return pltpu.make_async_copy(
            source.at[s, pl.ds(c * span, span)],
            target.at[s, pl.ds(c * span, span)],
            sems.at[which, s, c],
        )

    def start(s, carry):
        for c in range(chunks):

            @pl.when(c * CHUNK < lengths_ref[s])
            def _():
                copy(0, s, c).start()
                copy(1, s, c).start()

        return carry

    lax.fori_loop(0, seq_count, start, 0)

    cosine = cos_ref[...]
    sine = sin_ref[...]
    lane = lax.broadcasted_iota(jnp.int32, (seq_count, LANES), 1)
    low_half = (lane % SUB) < (SUB // 2)
    first_sub = lane < SUB

    def rotated(block):
        swapped = jnp.where(
            low_half, pltpu.roll(block, LANES - SUB // 2, 1), pltpu.roll(block, SUB // 2, 1)
        )
        return (block * cosine + swapped * sine).astype(BF16).astype(F32)

    def column(index):
        return qkv_ref[:, index * LANES : (index + 1) * LANES].astype(F32)

    for h in range(heads):
        turned = rotated(column(h)) * score_scale
        query_rows[:, h, :] = jnp.where(first_sub, turned, 0.0)
        query_rows[:, heads + h, :] = jnp.where(first_sub, 0.0, turned)
    for k in range(kv_local):
        turned = rotated(column(heads + k))
        fresh_value = column(heads + kv_local + k)
        for g in range(group_size):
            key_rows[:, k * group_size + g, :] = turned
            key_rows[:, heads + k * group_size + g, :] = turned
            value_rows[:, k * group_size + g, :] = fresh_value
            value_rows[:, heads + k * group_size + g, :] = fresh_value

    rows = 2 * heads
    row_kv = (lax.broadcasted_iota(jnp.int32, (rows, span), 0) % heads) // group_size
    position = lax.broadcasted_iota(jnp.int32, (rows, span), 1)
    own_kv = (position % kv_local) == row_kv
    position = position // kv_local
    head_weight = lambda_ref[...]

    def one(s, carry):
        length = lengths_ref[s]
        query = query_rows[s]
        fresh = jnp.sum(query * key_rows[s], axis=1, keepdims=True)
        query_low = query.astype(BF16)
        for c in range(chunks):

            @pl.when(c * CHUNK < length)
            def _():
                copy(0, s, c).wait()
                part = lax.dot_general(
                    query_low,
                    key_buf[s, c * span : (c + 1) * span, :],
                    (((1,), (1,)), ((), ())),
                    preferred_element_type=F32,
                )
                taken = own_kv & (position + c * CHUNK < length)
                score_buf[:, c * span : (c + 1) * span] = jnp.where(taken, part, -jnp.inf)

            @pl.when(c * CHUNK >= length)
            def _():
                score_buf[:, c * span : (c + 1) * span] = jnp.full((rows, span), -jnp.inf, F32)

        scores = score_buf[...]
        highest = jnp.maximum(jnp.max(scores, axis=1, keepdims=True), fresh)
        weights = jnp.exp(scores - highest)
        fresh_weight = jnp.exp(fresh - highest)
        total = jnp.sum(weights, axis=1, keepdims=True) + fresh_weight
        factor = head_weight / total
        score_buf[...] = weights * factor
        fresh_part = fresh_weight * factor
        fresh_map = (fresh_part + pltpu.roll(fresh_part, heads, 0)).astype(BF16).astype(F32)
        out_rows[s] = fresh_map * value_rows[s]
        for c in range(chunks):

            @pl.when(c * CHUNK < length)
            def _():
                copy(1, s, c).wait()
                part = score_buf[:, c * span : (c + 1) * span]
                mixed = (part + pltpu.roll(part, heads, 0)).astype(BF16)
                out_rows[s] += jnp.dot(
                    mixed,
                    value_buf[s, c * span : (c + 1) * span, :],
                    preferred_element_type=F32,
                )

        return carry

    lax.fori_loop(0, seq_count, one, 0)
    for h in range(heads):
        head = out_rows[:, h, :]
        square_mean = jnp.mean(head * head, axis=1, keepdims=True)
        normed = head * lax.rsqrt(square_mean + head_epsilon) * gain_ref[...] * head_scale
        out_ref[:, h * LANES : (h + 1) * LANES] = normed.astype(BF16)


def attend(qkv, head_lambda, head_gain, key_cache, value_cache, lengths):
    seq_count, cache, kv_local, _ = key_cache.shape
    heads = head_lambda.shape[0]
    group_size = heads // kv_local
    frequency = theta_base ** (-(jnp.arange(SUB // 2, dtype=F32) * (2.0 / SUB)))
    angles = lengths.astype(F32)[:, None] * frequency[None, :]
    cosine = jnp.cos(angles)
    sine = jnp.sin(angles)
    cosine = jnp.concatenate([cosine] * (2 * LANES // SUB), axis=1)
    sine = jnp.concatenate([-sine, sine] * (LANES // SUB), axis=1)
    weight = jnp.concatenate([jnp.ones_like(head_lambda), -head_lambda])[:, None]
    keys = key_cache.reshape(seq_count, cache * kv_local, 2 * SUB)
    values = value_cache.reshape(seq_count, cache * kv_local, VD)
    rows = 2 * heads
    chunks = cache // CHUNK
    vmem = pl.BlockSpec(memory_space=pltpu.VMEM)
    hbm = pl.BlockSpec(memory_space=pl.ANY)
    return pl.pallas_call(
        lambda *refs: attend_kernel(
            *refs, seq_count=seq_count, kv_local=kv_local, group_size=group_size, cache=cache
        ),
        out_shape=jax.ShapeDtypeStruct((seq_count, heads * VD), BF16),
        in_specs=[pl.BlockSpec(memory_space=pltpu.SMEM), vmem, vmem, vmem, vmem, vmem, hbm, hbm],
        out_specs=vmem,
        scratch_shapes=[
            pltpu.VMEM((seq_count, cache * kv_local, 2 * SUB), BF16),
            pltpu.VMEM((seq_count, cache * kv_local, VD), BF16),
            pltpu.VMEM((seq_count, rows, LANES), F32),
            pltpu.VMEM((seq_count, rows, LANES), F32),
            pltpu.VMEM((seq_count, rows, LANES), F32),
            pltpu.VMEM((rows, cache * kv_local), F32),
            pltpu.VMEM((seq_count, rows, LANES), F32),
            pltpu.SemaphoreType.DMA((2, seq_count, chunks)),
        ],
        compiler_params=pltpu.CompilerParams(vmem_limit_bytes=28 * 1024 * 1024),
        name="attend",
    )(lengths, qkv, cosine, sine, weight, head_gain[None, :], keys, values)


def split_three(array):
    high = array.astype(BF16)
    rest = array - high.astype(F32)
    middle = rest.astype(BF16)
    low = (rest - middle.astype(F32)).astype(BF16)
    return [high, middle, low]


def halves_sum(array, axis, count, distance, dim):
    bit = (lax.axis_index(axis) & distance) != 0
    low, high = jnp.split(array, 2, axis=dim)
    kept = jnp.where(bit, high, low)
    sent = jnp.where(bit, low, high)
    got = xor_permute(sent.astype(BF16), axis, count, distance)
    return kept.astype(F32) + got.astype(F32)


def halves_join(array, axis, count, distance, dim):
    bit = (lax.axis_index(axis) & distance) != 0
    got = xor_permute(array, axis, count, distance)
    return jnp.concatenate(
        [jnp.where(bit, got, array), jnp.where(bit, array, got)], axis=dim
    )


def blocks_xor(array, index, count, dim):
    step = 1
    while step < count:
        size = array.shape[dim] // count
        parts = jnp.split(array, count, axis=dim)
        swapped = jnp.concatenate([parts[b ^ step] for b in range(count)], axis=dim)
        array = jnp.where((index & step) != 0, swapped, array)
        step *= 2
    return array


def doubled_sum(array, axis, count):
    step = 1
    while step < count:
        array = array + xor_permute(array, axis, count, step)
        step *= 2
    return array


def on_device(
    tokens,
    query_weight,
    key_weight,
    value_weight,
    out_weight,
    head_lambda,
    head_gain,
    key_cache,
    value_cache,
    lengths,
    first_gain,
    second_gain,
    expert_ids,
    route_weights,
    expert_gate,
    expert_up,
    expert_down,
    dense_gate,
    dense_up,
    dense_down,
    dense_mix,
):
    seq_count, model_width = tokens.shape
    ep_count = lax.axis_size("ep")
    tp_count = lax.axis_size("tp")
    ep = lax.axis_index("ep")
    tp = lax.axis_index("tp")
    block_width = model_width // ep_count
    slice_width = model_width // tp_count
    local_experts = expert_gate.shape[0]

    extra = jnp.concatenate(
        [expert_ids.astype(BF16)] + split_three(route_weights), axis=1
    )
    extra = jnp.pad(extra, ((0, 0), (0, LANES - extra.shape[1])))

    def piece(distance):
        part = lax.dynamic_slice_in_dim(tokens, (ep ^ distance) * block_width, block_width, 1)
        return jnp.concatenate([part, extra], axis=1)

    pieces = [piece(0)]
    for distance in range(1, ep_count):
        pieces.append(xor_permute(piece(distance), "ep", ep_count, distance))
    arrived = jnp.concatenate(pieces, axis=0)
    columns = arrived[:, :block_width]
    carried = arrived[:, block_width : block_width + 4 * TOPK]
    total_rows = ep_count * seq_count

    projected = jnp.concatenate(
        [
            jnp.dot(columns, query_weight, preferred_element_type=F32),
            jnp.dot(columns, key_weight, preferred_element_type=F32),
            jnp.dot(columns, value_weight, preferred_element_type=F32),
        ],
        axis=1,
    )
    qkv = projected[:seq_count]
    for distance in range(1, ep_count):
        part = projected[distance * seq_count : (distance + 1) * seq_count].astype(BF16)
        qkv = qkv + xor_permute(part, "ep", ep_count, distance).astype(F32)
    normed = attend(
        qkv.astype(BF16), head_lambda, head_gain, key_cache, value_cache, lengths
    )

    all_heads = jnp.concatenate(
        [normed]
        + [xor_permute(normed, "ep", ep_count, distance) for distance in range(1, ep_count)],
        axis=0,
    )
    column_part = jnp.dot(all_heads, out_weight, preferred_element_type=F32).astype(BF16)
    piece_width = block_width // tp_count
    scattered = lax.all_to_all(
        column_part.reshape(total_rows, tp_count, piece_width),
        "tp",
        split_axis=1,
        concat_axis=1,
        tiled=True,
    )
    attention = jnp.sum(scattered.astype(F32), axis=1).astype(BF16)
    own_tokens = lax.dynamic_slice_in_dim(columns, tp * piece_width, piece_width, 1)
    residual = residual_scale * own_tokens.astype(F32) + attention.astype(F32)
    residual = residual.astype(BF16)
    ratio = tp_count // ep_count

    def route(turn):
        pairs = []
        for c in range(ep_count):
            for h in range(ratio):
                for q in range(ep_count):
                    source = c * tp_count + h * ep_count + q
                    pairs.append((source, (q ^ turn) * tp_count + c * ratio + h))
        return pairs

    gathered = jnp.concatenate(
        [lax.ppermute(residual, ("ep", "tp"), route(turn)) for turn in range(ep_count)], axis=1
    )
    gathered = blocks_xor(gathered, ep, ep_count, 1)
    gathered = blocks_xor(gathered, ep ^ (tp // ratio), ep_count, 0).astype(F32)
    moments = doubled_sum(
        jnp.stack([jnp.sum(gathered, axis=1), jnp.sum(gathered * gathered, axis=1)]),
        "tp",
        tp_count,
    )
    average = moments[0] / model_width
    variance = moments[1] / model_width - average * average
    own_gain = lax.dynamic_slice_in_dim(first_gain, tp * slice_width, slice_width, 0)
    hidden = (
        (gathered - average[:, None]) * lax.rsqrt(variance + layer_epsilon)[:, None] * own_gain
    ).astype(BF16)

    ids = carried[:, :TOPK].astype(jnp.int32)
    weights = sum(
        carried[:, TOPK * (i + 1) : TOPK * (i + 2)].astype(F32) for i in range(3)
    )
    gates = weights / jnp.sum(weights, axis=1, keepdims=True)
    pair_count = seq_count * TOPK
    pair_ids = ids.reshape(ep_count, pair_count)
    order = jnp.arange(pair_count, dtype=jnp.int32)
    same = (pair_ids[:, :, None] == pair_ids[:, None, :]) & (order[None, :] < order[:, None])
    rank = jnp.sum(same.astype(jnp.int32), axis=2)
    local = pair_ids - ep * local_experts
    block = jnp.arange(ep_count, dtype=jnp.int32)[:, None]
    slot_count = local_experts * ep_count * CAP
    slot = jnp.where(
        (local >= 0) & (local < local_experts),
        local * (ep_count * CAP) + block * CAP + rank,
        slot_count,
    ).reshape(total_rows, TOPK)
    slots = jnp.arange(slot_count, dtype=jnp.int32)
    hit = slot[:, :, None] == slots[None, None, :]
    placed = jnp.sum(hit.astype(F32), axis=1).astype(BF16)
    combine = jnp.sum(jnp.where(hit, gates[:, :, None], 0.0), axis=1)

    routed = lax.dot_general(
        placed, hidden, (((0,), (0,)), ((), ())), preferred_element_type=F32
    ).astype(BF16)
    routed = routed.reshape(local_experts, ep_count * CAP, slice_width)

    def expert_dot(rows, weight):
        return jnp.einsum("erd,edf->erf", rows, weight, preferred_element_type=F32)

    fold = total_rows // slot_count

    def folded(array):
        return jnp.concatenate(jnp.split(array, fold, axis=0), axis=1)

    def both(expert_weight, dense_weight):
        expert_part = expert_dot(routed, expert_weight).reshape(slot_count, -1)
        dense_part = jnp.dot(hidden, dense_weight, preferred_element_type=F32)
        return jnp.concatenate([expert_part, folded(dense_part)], axis=1)

    pre = jnp.stack([both(expert_gate, dense_gate), both(expert_up, dense_up)])
    distance, dim = 1, 1
    while distance < tp_count:
        pre = halves_sum(pre, "tp", tp_count, distance, dim)
        distance, dim = distance * 2, 2
    active = (jax.nn.silu(pre[0]) * pre[1]).astype(BF16)
    while distance > 1:
        distance //= 2
        active = halves_join(active, "tp", tp_count, distance, 0 if distance == 1 else 1)
    expert_width = expert_gate.shape[2]
    expert_hidden = active[:, :expert_width].reshape(local_experts, ep_count * CAP, expert_width)
    dense_hidden = jnp.concatenate(jnp.split(active[:, expert_width:], fold, axis=1), axis=0)
    result = expert_dot(expert_hidden, expert_down).astype(BF16).reshape(slot_count, slice_width)
    dense_part = jnp.dot(dense_hidden, dense_down, preferred_element_type=F32)

    own_mix = lax.dynamic_slice_in_dim(dense_mix, tp * slice_width, slice_width, 0)
    mix_sum = doubled_sum(
        jnp.sum(hidden.astype(F32) * own_mix.astype(F32), axis=1)[None, :], "tp", tp_count
    )[0]
    mix_gate = jax.nn.sigmoid(mix_sum)
    mixed = jnp.dot(combine, result.astype(F32), precision=lax.Precision.HIGHEST)
    mixed = mixed + mix_gate[:, None] * dense_part
    combined = residual_scale * hidden[:seq_count].astype(F32) + mixed[:seq_count]
    for distance in range(1, ep_count):
        part = mixed[distance * seq_count : (distance + 1) * seq_count].astype(BF16)
        combined = combined + xor_permute(part, "ep", ep_count, distance).astype(F32)
    moments = doubled_sum(
        jnp.stack([jnp.sum(combined, axis=1), jnp.sum(combined * combined, axis=1)]),
        "tp",
        tp_count,
    )
    average = moments[0] / model_width
    variance = moments[1] / model_width - average * average
    layer_out = (
        (combined - average[:, None]) * lax.rsqrt(variance + layer_epsilon)[:, None] * second_gain
    )
    return layer_out.astype(BF16)


def solution(mesh):
    return jax.shard_map(
        on_device,
        mesh=mesh,
        in_specs=(
            P("ep", None),
            P("ep", "tp"),
            P("ep", "tp"),
            P("ep", "tp"),
            P("tp", "ep"),
            P("tp"),
            P(),
            P("ep", None, "tp", None),
            P("ep", None, "tp", None),
            P("ep"),
            P(),
            P("tp"),
            P("ep", None),
            P("ep", None),
            P("ep", "tp", None),
            P("ep", "tp", None),
            P("ep", None, "tp"),
            P("tp", "ep"),
            P("tp", "ep"),
            P("ep", "tp"),
            P(),
        ),
        out_specs=P("ep", "tp"),
        check_vma=False,
    )
```

time: 279 us -> 186 us (0.67)
  waiting for transfers between devices: 149 us -> 73.1 us
  blocking collectives: 31.6 us -> 0 us
  Pallas kernels: 0 us -> 29.4 us
  starting transfers between devices: 15.9 us -> 43.3 us
  local copies, waits for them, and re-layouts: 27.8 us -> 11.8 us
  matrix products: 34 us -> 20.6 us
  between operations: 13.5 us -> 0.6 us
    psum x2 -> x0, waiting for transfers between devices: 110 us -> none  [the longest x1 55.1 us: on_device(): lax.psum(column_part.astype(jnp.bfloat16), 'tp').astype(jnp.float32)]
    ppermute x0 -> x31, waiting for transfers between devices: none -> 68 us  [the longest x27 63.3 us: xor_permute(): return lax.ppermute(array, axis, [(i, i ^ distance) for i in range(count)])]
    ppermute x0 -> x31, starting transfers between devices: none -> 38.4 us  [the longest x27 29.1 us: xor_permute(): return lax.ppermute(array, axis, [(i, i ^ distance) for i in range(count)])]
    pallas_call x0 -> x1, Pallas kernels: none -> 29.4 us  [attend(): pl.pallas_call(lambda *refs: attend_kernel(*refs, seq_count=seq_count, kv...]
    reduce_scatter x2 -> x0, waiting for transfers between devices: 23.8 us -> none  [the longest x1 22 us: on_device(): lax.psum_scatter(dense_part.astype(jnp.bfloat16), 'ep', scatter_dimension...]
    all_gather x2 -> x0, blocking collectives: 15.8 us -> none  [the longest x1 8.17 us: on_device(): all_heads = lax.all_gather(normed, 'ep', axis=0, tiled=True)]
    psum x1 -> x0, blocking collectives: 15.8 us -> none  [on_device(): lax.psum((jnp.sum(combined, axis=1), jnp.sum(combined * combined, axis=1)...]
    unnamed x31 -> x20, local copies, waits for them, and re-layouts: 22 us -> 7.48 us
  transfers between devices with their start and end apart: 8 -> 32, of which waited for: 8 -> 25; matrix products, arithmetic and copies ran while one was open for 10% -> 2% of each run, Pallas kernels for 0% -> 0%
where the time goes in v1:
time: 186 us; the launch traced here: 185 us
  waiting for transfers between devices  73.1 us (39%)
  starting transfers between devices  43.3 us (23%)
  Pallas kernels  29.4 us (16%)
  matrix products  20.6 us (11%)
  local copies, waits for them, and re-layouts  11.8 us (6%)
  other arithmetic  6.57 us (4%)
    ppermute x27, waiting for transfers between devices, xor_permute(): return lax.ppermute(array, axis, [(i, i ^ distance) for i in range(count)])  63.3 us
    pallas_call x1, Pallas kernels, attend(): pl.pallas_call(lambda *refs: attend_kernel(*refs, seq_count=seq_count, kv...  29.4 us
    ppermute x27, starting transfers between devices, xor_permute(): return lax.ppermute(array, axis, [(i, i ^ distance) for i in range(count)])  29.1 us
    dot_general x3, matrix products, expert_dot(): return jnp.einsum('erd,edf->erf', rows, weight, preferred_element_type=F32)  13.8 us
    ppermute x4, starting transfers between devices, on_device(): lax.ppermute(residual, ('ep', 'tp'), route(turn))  9.32 us
    unnamed x20, local copies, waits for them, and re-layouts  7.48 us
    all_to_all x1, waiting for transfers between devices, on_device(): lax.all_to_all(column_part.reshape(total_rows, tp_count, piece_width), 't...  5.11 us
    all_to_all x1, starting transfers between devices, on_device(): lax.all_to_all(column_part.reshape(total_rows, tp_count, piece_width), 't...  4.88 us
  transfers between devices with their start and end apart: 32, of which 25 were waited for; matrix products, arithmetic and copies ran while one was open for 2% of the time, Pallas kernels for 0%

profile of v1, /device:TPU:0, one launch (start us, length us, event | category | flops | bytes accessed | tf_op | source)
XLA Modules:
  0.0 185.4 jit_solution(5461329669273373018)
XLA Ops:
  0.0 0.9 constant_dynamic-slice_fusion.3
  1.4 0.8 fusion.58
  2.2 0.7 convert_element_type.131
  3.1 3.1 %collective-permute-start = (bf16[16,1152]{0,1:T(8,128)(2,1)S(1)}, bf16[16,1152]{0,1:T(8,128)(2,1)S(1)}, u32[]{:S(2)}, u32[]{:S(2)}) collective-permute-start(bf16[16,1152]{0,1:T(8,128)(2,1)S(1)} %get-tuple-element.41), channel_id=1, source_target_pairs={{0,8},{8,0},{16,24},{24,16},{1,9},{9,1},{17,25},{25,17},{2,10},{10... | collective-permute-start | bytes 110600 | tf_op jit(solution)/shard_map/ppermute | solution.py:27
  6.1 1.5 collective-permute-start.1
  7.7 0.7 convert_element_type.142
  8.4 0.7 neg.27
  9.6 4.4 %collective-permute-done = bf16[16,1152]{0,1:T(8,128)(2,1)S(1)} collective-permute-done((bf16[16,1152]{0,1:T(8,128)(2,1)S(1)}, bf16[16,1152]{0,1:T(8,128)(2,1)S(1)}, u32[]{:S(2)}, u32[]{:S(2)}) %collective-permute-start) | collective-permute-done | bytes 36896 | tf_op jit(solution)/shard_map/ppermute | solution.py:27
  14.0 6.9 %collective-permute-done.1 = bf16[16,1152]{0,1:T(8,128)(2,1)S(1)} collective-permute-done((bf16[16,1152]{0,1:T(8,128)(2,1)S(1)}, bf16[16,1152]{0,1:T(8,128)(2,1)S(1)}, u32[]{:S(2)}, u32[]{:S(2)}) %collective-permute-start.1) | collective-permute-done | bytes 36896 | tf_op jit(solution)/shard_map/ppermute | solution.py:27
  20.9 0.4 pad_maximum_fusion.4
  21.3 1.5 fusion.47
  22.9 1.3 fusion.43
  24.2 1.3 fusion.45
  25.5 1.3 collective-permute-start.3
  26.8 0.8 collective-permute-start.4
  27.6 1.4 collective-permute-start.5
  29.1 0.6 collective-permute-done.3
  29.7 1.0 collective-permute-done.4
  30.7 1.7 collective-permute-done.5
  32.5 3.4 %copy-done.1 = bf16[16,1024,2,128]{3,2,1,0:T(2,128)(2,1)S(1)} copy-done((bf16[16,1024,2,128]{3,2,1,0:T(2,128)(2,1)S(1)}, bf16[16,1024,2,128]{3,2,1,0:T(2,128)(2,1)}, u32[]{:S(2)}) %copy-start.1) | copy-done | bytes 8388632
  35.9 3.4 %copy-done.2 = bf16[16,1024,2,128]{3,2,1,0:T(2,128)(2,1)S(1)} copy-done((bf16[16,1024,2,128]{3,2,1,0:T(2,128)(2,1)S(1)}, bf16[16,1024,2,128]{3,2,1,0:T(2,128)(2,1)}, u32[]{:S(2)}) %copy-start.2) | copy-done | bytes 8388632
  39.3 29.4 %attend.1 = bf16[16,512]{1,0:T(8,128)(2,1)S(1)} custom-call(s32[16]{0:T(128)S(1)} %copy-done.3, bf16[16,1024]{1,0:T(8,128)(2,1)S(1)} %fusion.16.refs_1_, f32[16,128]{1,0:T(8,128)S(1)} %get-tuple-element.52.refs_2_, f32[16,128]{1,0:T(8,128)S(1)} %get-tuple-element.53.refs_3_, f32[8,1]{1,0:T(8,128)S(1)} %copy.73.refs_4_, f32[1,128]{1,0:T(1,128)S(1)} %bitcast.82, ...), custom_call_target="tpu_custom_call" | custom-call | tf_op jit(solution)/shard_map/attend/pallas_call | solution.py:186
  68.8 9.5 %collective-permute-start.7 = (bf16[16,512]{1,0:T(8,128)(2,1)S(1)}, bf16[16,512]{1,0:T(8,128)(2,1)S(1)}, u32[]{:S(2)}, u32[]{:S(2)}) collective-permute-start(bf16[16,512]{1,0:T(8,128)(2,1)S(1)} %attend.1), channel_id=1, source_target_pairs={{0,16},{8,24},{16,0},{24,8},{1,17},{9,25},{17,1},{25,9},{2,18},{10... | collective-permute-start | bytes 49160 | tf_op jit(solution)/shard_map/ppermute | solution.py:27
  78.3 0.8 dynamic-slice_convert_fusion
  79.1 1.0 collective-permute-done.7
  80.0 2.9 %collective-permute-done.8 = bf16[16,512]{1,0:T(8,128)(2,1)S(1)} collective-permute-done((bf16[16,512]{1,0:T(8,128)(2,1)S(1)}, bf16[16,512]{1,0:T(8,128)(2,1)S(1)}, u32[]{:S(2)}, u32[]{:S(2)}) %collective-permute-start.8) | collective-permute-done | bytes 16416 | tf_op jit(solution)/shard_map/ppermute | solution.py:27
  83.3 0.7 copy.89
  83.9 4.9 %all-to-all-start = ((bf16[64,8,128]{2,0,1:T(8,128)(2,1)}), bf16[64,8,128]{2,0,1:T(8,128)(2,1)S(1)}, u32[]{:S(2)}, u32[]{:S(2)}) async-start(bf16[64,8,128]{2,0,1:T(8,128)(2,1)} %bitcast.79), calls=%async_computation | async-start | bytes 262144 | tf_op jit(solution)/shard_map/all_to_all | solution.py:324
  88.8 0.8 dynamic_slice.26
  90.5 5.1 %all-to-all-done = bf16[64,8,128]{2,0,1:T(8,128)(2,1)S(1)} async-done(((bf16[64,8,128]{2,0,1:T(8,128)(2,1)}), bf16[64,8,128]{2,0,1:T(8,128)(2,1)S(1)}, u32[]{:S(2)}, u32[]{:S(2)}) %all-to-all-start) | async-done | bytes 131104 | tf_op jit(solution)/shard_map/all_to_all | solution.py:324
  95.7 0.7 collective-permute-start.10
  96.4 7.0 %collective-permute-start.11 = (bf16[64,128]{0,1:T(8,128)(2,1)S(1)}, bf16[64,128]{0,1:T(8,128)(2,1)S(1)}, u32[]{:S(2)}, u32[]{:S(2)}) collective-permute-start(bf16[64,128]{0,1:T(8,128)(2,1)S(1)} %add_convert_fusion), channel_id=1, source_target_pairs={{0,24},{1,16},{2,8},{3,0},{4,25},{5,17},{6,9},{7,1},{8,26},{9,18},... | collective-permute-start | bytes 49160 | tf_op jit(solution)/shard_map/ppermute | solution.py:347
  103.4 1.6 collective-permute-start.9
  105.1 1.2 collective-permute-done.11
  106.3 3.5 %collective-permute-done.12 = bf16[64,128]{0,1:T(8,128)(2,1)S(1)} collective-permute-done((bf16[64,128]{0,1:T(8,128)(2,1)S(1)}, bf16[64,128]{0,1:T(8,128)(2,1)S(1)}, u32[]{:S(2)}, u32[]{:S(2)}) %collective-permute-start.12) | collective-permute-done | bytes 16416 | tf_op jit(solution)/shard_map/ppermute | solution.py:347
  110.8 1.0 collective-permute-done.13
  111.9 3.5 %collective-permute-done.14 = f32[2,64]{1,0:T(2,128)S(1)} collective-permute-done((f32[2,64]{1,0:T(2,128)S(1)}, f32[2,64]{1,0:T(2,128)S(1)}, u32[]{:S(2)}, u32[]{:S(2)}) %collective-permute-start.14) | collective-permute-done | bytes 544 | tf_op jit(solution)/shard_map/ppermute | solution.py:27
  115.5 0.8 collective-permute-start.15
  116.4 3.7 %collective-permute-done.15 = f32[2,64]{1,0:T(2,128)S(1)} collective-permute-done((f32[2,64]{1,0:T(2,128)S(1)}, f32[2,64]{1,0:T(2,128)S(1)}, u32[]{:S(2)}, u32[]{:S(2)}) %collective-permute-start.15) | collective-permute-done | bytes 544 | tf_op jit(solution)/shard_map/ppermute | solution.py:27
  120.7 4.6 %fusion.60 = f32[4,16,2048]{2,1,0:T(8,128)S(1)} fusion(bf16[4,16,512]{2,1,0:T(8,128)(2,1)S(1)} %bitcast.86, bf16[4,512,2048]{2,1,0:T(8,128)(2,1)} %param.35), kind=kOutput, calls=%fused_computation.137 | convolution fusion | flops 134217728 | bytes 8978432 | tf_op jit(solution)/shard_map/erd,edf->erf/dot_general | solution.py:392
  125.4 4.6 %fusion.62 = f32[4,16,2048]{2,1,0:T(8,128)S(1)} fusion(bf16[4,16,512]{2,1,0:T(8,128)(2,1)S(1)} %bitcast.87, bf16[4,512,2048]{2,1,0:T(8,128)(2,1)} %param.36), kind=kOutput, calls=%fused_computation.139 | convolution fusion | flops 134217728 | bytes 8978432 | tf_op jit(solution)/shard_map/erd,edf->erf/dot_general | solution.py:392
  130.5 1.6 collective-permute-done.16
  132.3 6.2 %collective-permute-done.17 = bf16[2,32,1280]{2,1,0:T(8,128)(2,1)S(1)} collective-permute-done((bf16[2,32,1280]{2,1,0:T(8,128)(2,1)S(1)}, bf16[2,32,1280]{2,1,0:T(8,128)(2,1)S(1)}, u32[]{:S(2)}, u32[]{:S(2)}) %collective-permute-start.17) | collective-permute-done | bytes 163872 | tf_op jit(solution)/shard_map/ppermute | solution.py:27
  138.6 1.0 collective-permute-start.18
  139.6 5.3 %collective-permute-done.18 = bf16[2,32,640]{2,1,0:T(8,128)(2,1)S(1)} collective-permute-done((bf16[2,32,640]{2,1,0:T(8,128)(2,1)S(1)}, bf16[2,32,640]{2,1,0:T(8,128)(2,1)S(1)}, u32[]{:S(2)}, u32[]{:S(2)}) %collective-permute-start.18) | collective-permute-done | bytes 81952 | tf_op jit(solution)/shard_map/ppermute | solution.py:27
  145.2 4.8 %collective-permute-done.19 = bf16[32,640]{1,0:T(8,128)(2,1)S(1)} collective-permute-done((bf16[32,640]{1,0:T(8,128)(2,1)S(1)}, bf16[32,640]{1,0:T(8,128)(2,1)S(1)}, u32[]{:S(2)}, u32[]{:S(2)}) %collective-permute-start.19) | collective-permute-done | bytes 40992 | tf_op jit(solution)/shard_map/ppermute | solution.py:27
  150.1 2.0 %collective-permute-start.23 = (f32[1,64]{1,0:T(1,128)S(1)}, f32[1,64]{1,0:T(1,128)S(1)}, u32[]{:S(2)}, u32[]{:S(2)}) collective-permute-start(f32[1,64]{1,0:T(1,128)S(1)} %bitcast_add_fusion), channel_id=1, source_target_pairs={{0,2},{1,3},{2,0},{3,1},{4,6},{5,7},{6,4},{7,5},{8,10},{9,11},{10,... | collective-permute-start | bytes 776 | tf_op jit(solution)/shard_map/ppermute | solution.py:27
  152.1 2.5 %collective-permute-done.23 = f32[1,64]{1,0:T(1,128)S(1)} collective-permute-done((f32[1,64]{1,0:T(1,128)S(1)}, f32[1,64]{1,0:T(1,128)S(1)}, u32[]{:S(2)}, u32[]{:S(2)}) %collective-permute-start.23) | collective-permute-done | bytes 288 | tf_op jit(solution)/shard_map/ppermute | solution.py:27
  154.6 1.8 collective-permute-start.24
  156.5 2.6 %collective-permute-done.24 = f32[1,64]{1,0:T(1,128)S(1)} collective-permute-done((f32[1,64]{1,0:T(1,128)S(1)}, f32[1,64]{1,0:T(1,128)S(1)}, u32[]{:S(2)}, u32[]{:S(2)}) %collective-permute-start.24) | collective-permute-done | bytes 288 | tf_op jit(solution)/shard_map/ppermute | solution.py:27
  159.2 4.6 %convolution_convert_fusion.1 = bf16[4,16,512]{2,1,0:T(8,128)(2,1)S(1)} fusion(bf16[4,16,2048]{2,1,0:T(8,128)(2,1)S(1)} %bitcast.85, bf16[4,2048,512]{2,1,0:T(8,128)(2,1)} %param.37), kind=kOutput, calls=%fused_computation.6 | convolution fusion | flops 134250496 | bytes 8716288 | tf_op jit(solution)/shard_map/erd,edf->erf/dot_general | solution.py:392
  163.8 0.3 fusion.64
  164.1 1.4 fusion.59
  165.7 0.9 collective-permute-start.25
  166.6 2.5 %collective-permute-start.26 = (bf16[16,512]{0,1:T(8,128)(2,1)S(1)}, bf16[16,512]{0,1:T(8,128)(2,1)S(1)}, u32[]{:S(2)}, u32[]{:S(2)}) collective-permute-start(bf16[16,512]{0,1:T(8,128)(2,1)S(1)} %get-tuple-element.23), channel_id=1, source_target_pairs={{0,16},{8,24},{16,0},{24,8},{1,17},{9,25},{17,1},{25,9},{2,18},{10... | collective-permute-start | bytes 49160 | tf_op jit(solution)/shard_map/ppermute | solution.py:27
  169.3 2.2 %collective-permute-done.25 = bf16[16,512]{0,1:T(8,128)(2,1)S(1)} collective-permute-done((bf16[16,512]{0,1:T(8,128)(2,1)S(1)}, bf16[16,512]{0,1:T(8,128)(2,1)S(1)}, u32[]{:S(2)}, u32[]{:S(2)}) %collective-permute-start.25) | collective-permute-done | bytes 16416 | tf_op jit(solution)/shard_map/ppermute | solution.py:27
  171.5 1.5 collective-permute-done.26
  173.0 1.9 %collective-permute-done.27 = bf16[16,512]{0,1:T(8,128)(2,1)S(1)} collective-permute-done((bf16[16,512]{0,1:T(8,128)(2,1)S(1)}, bf16[16,512]{0,1:T(8,128)(2,1)S(1)}, u32[]{:S(2)}, u32[]{:S(2)}) %collective-permute-start.27) | collective-permute-done | bytes 16416 | tf_op jit(solution)/shard_map/ppermute | solution.py:27
  175.2 1.1 collective-permute-done.28
  176.3 1.1 collective-permute-start.29
  177.5 2.5 %collective-permute-done.29 = f32[2,16]{1,0:T(2,128)S(1)} collective-permute-done((f32[2,16]{1,0:T(2,128)S(1)}, f32[2,16]{1,0:T(2,128)S(1)}, u32[]{:S(2)}, u32[]{:S(2)}) %collective-permute-start.29) | collective-permute-done | bytes 160 | tf_op jit(solution)/shard_map/ppermute | solution.py:27
  180.0 0.5 collective-permute-start.30
  180.5 4.0 %collective-permute-done.30 = f32[2,16]{1,0:T(2,128)S(1)} collective-permute-done((f32[2,16]{1,0:T(2,128)S(1)}, f32[2,16]{1,0:T(2,128)S(1)}, u32[]{:S(2)}, u32[]{:S(2)}) %collective-permute-start.30) | collective-permute-done | bytes 160 | tf_op jit(solution)/shard_map/ppermute | solution.py:27
  184.7 0.7 copy.80
  (113 shorter events, 6.6 us)
Async XLA Ops:
  0.0 82.9 %copy-start = (bf16[512,1024]{1,0:T(8,128)(2,1)S(1)}, bf16[512,1024]{1,0:T(8,128)(2,1)}, u32[]{:S(2)}) copy-start(bf16[512,1024]{1,0:T(8,128)(2,1)} %param.25) | copy-start | bytes 3145732
  0.0 32.5 %copy-start.3 = (s32[16]{0:T(128)S(1)}, s32[16]{0:T(128)}, u32[]{:S(2)}) copy-start(s32[16]{0:T(128)} %refs_0_.1) | copy-start | bytes 196
  0.0 32.5 %copy-start.4 = (f32[128]{0:T(128)S(1)}, f32[128]{0:T(128)}, u32[]{:S(2)}) copy-start(f32[128]{0:T(128)} %param.27) | copy-start | bytes 1540
  3.1 10.9 %collective-permute-start = (bf16[16,1152]{0,1:T(8,128)(2,1)S(1)}, bf16[16,1152]{0,1:T(8,128)(2,1)S(1)}, u32[]{:S(2)}, u32[]{:S(2)}) collective-permute-start(bf16[16,1152]{0,1:T(8,128)(2,1)S(1)} %get-tuple-element.41), channel_id=1, source_target_pairs={{0,8},{8,0},{16,24},{24,16},{1,9},{9,1},{17,25},{25,17},{2,10},{10... | collective-permute-start | bytes 110600 | tf_op jit(solution)/shard_map/ppermute | solution.py:27
  6.1 14.8 %collective-permute-start.1 = (bf16[16,1152]{0,1:T(8,128)(2,1)S(1)}, bf16[16,1152]{0,1:T(8,128)(2,1)S(1)}, u32[]{:S(2)}, u32[]{:S(2)}) collective-permute-start(bf16[16,1152]{0,1:T(8,128)(2,1)S(1)} %get-tuple-element.42), channel_id=1, source_target_pairs={{0,16},{8,24},{16,0},{24,8},{1,17},{9,25},{17,1},{25,9},{2,18},{10... | collective-permute-start | bytes 110600 | tf_op jit(solution)/shard_map/ppermute | solution.py:27
  7.7 13.3 %collective-permute-start.2 = (bf16[16,1152]{0,1:T(8,128)(2,1)S(1)}, bf16[16,1152]{0,1:T(8,128)(2,1)S(1)}, u32[]{:S(2)}, u32[]{:S(2)}) collective-permute-start(bf16[16,1152]{0,1:T(8,128)(2,1)S(1)} %get-tuple-element.43), channel_id=1, source_target_pairs={{0,24},{8,16},{16,8},{24,0},{1,25},{9,17},{17,9},{25,1},{2,26},{10... | collective-permute-start | bytes 110600 | tf_op jit(solution)/shard_map/ppermute | solution.py:27
  25.5 4.2 %collective-permute-start.3 = (bf16[16,1024]{1,0:T(8,128)(2,1)S(1)}, bf16[16,1024]{1,0:T(8,128)(2,1)S(1)}, u32[]{:S(2)}, u32[]{:S(2)}) collective-permute-start(bf16[16,1024]{1,0:T(8,128)(2,1)S(1)} %get-tuple-element.32), channel_id=1, source_target_pairs={{0,8},{8,0},{16,24},{24,16},{1,9},{9,1},{17,25},{25,17},{2,10},{10... | collective-permute-start | bytes 98312 | tf_op jit(solution)/shard_map/ppermute | solution.py:27
  26.8 3.9 %collective-permute-start.4 = (bf16[16,1024]{1,0:T(8,128)(2,1)S(1)}, bf16[16,1024]{1,0:T(8,128)(2,1)S(1)}, u32[]{:S(2)}, u32[]{:S(2)}) collective-permute-start(bf16[16,1024]{1,0:T(8,128)(2,1)S(1)} %get-tuple-element.34), channel_id=1, source_target_pairs={{0,16},{8,24},{16,0},{24,8},{1,17},{9,25},{17,1},{25,9},{2,18},{10... | collective-permute-start | bytes 98312 | tf_op jit(solution)/shard_map/ppermute | solution.py:27
  27.6 4.8 %collective-permute-start.5 = (bf16[16,1024]{1,0:T(8,128)(2,1)S(1)}, bf16[16,1024]{1,0:T(8,128)(2,1)S(1)}, u32[]{:S(2)}, u32[]{:S(2)}) collective-permute-start(bf16[16,1024]{1,0:T(8,128)(2,1)S(1)} %get-tuple-element.33), channel_id=1, source_target_pairs={{0,24},{8,16},{16,8},{24,0},{1,25},{9,17},{17,9},{25,1},{2,26},{10... | collective-permute-start | bytes 98312 | tf_op jit(solution)/shard_map/ppermute | solution.py:27
  32.5 3.4 %copy-start.1 = (bf16[16,1024,2,128]{3,2,1,0:T(2,128)(2,1)S(1)}, bf16[16,1024,2,128]{3,2,1,0:T(2,128)(2,1)}, u32[]{:S(2)}) copy-start(bf16[16,1024,2,128]{3,2,1,0:T(2,128)(2,1)} %param.28) | copy-start | bytes 25165828
  35.9 3.4 %copy-start.2 = (bf16[16,1024,2,128]{3,2,1,0:T(2,128)(2,1)S(1)}, bf16[16,1024,2,128]{3,2,1,0:T(2,128)(2,1)}, u32[]{:S(2)}) copy-start(bf16[16,1024,2,128]{3,2,1,0:T(2,128)(2,1)} %param.29) | copy-start | bytes 25165828
  68.7 51.8 %copy-start.5 = (bf16[512,512]{1,0:T(8,128)(2,1)S(1)}, bf16[512,512]{1,0:T(8,128)(2,1)}, u32[]{:S(2)}) copy-start(bf16[512,512]{1,0:T(8,128)(2,1)} %param.38) | copy-start | bytes 1572868
  68.7 10.3 %collective-permute-start.6 = (bf16[16,512]{1,0:T(8,128)(2,1)S(1)}, bf16[16,512]{1,0:T(8,128)(2,1)S(1)}, u32[]{:S(2)}, u32[]{:S(2)}) collective-permute-start(bf16[16,512]{1,0:T(8,128)(2,1)S(1)} %attend.1), channel_id=1, source_target_pairs={{0,8},{8,0},{16,24},{24,16},{1,9},{9,1},{17,25},{25,17},{2,10},{10... | collective-permute-start | bytes 49160 | tf_op jit(solution)/shard_map/ppermute | solution.py:27
  68.8 11.2 %collective-permute-start.7 = (bf16[16,512]{1,0:T(8,128)(2,1)S(1)}, bf16[16,512]{1,0:T(8,128)(2,1)S(1)}, u32[]{:S(2)}, u32[]{:S(2)}) collective-permute-start(bf16[16,512]{1,0:T(8,128)(2,1)S(1)} %attend.1), channel_id=1, source_target_pairs={{0,16},{8,24},{16,0},{24,8},{1,17},{9,25},{17,1},{25,9},{2,18},{10... | collective-permute-start | bytes 49160 | tf_op jit(solution)/shard_map/ppermute | solution.py:27
  78.3 4.6 %collective-permute-start.8 = (bf16[16,512]{1,0:T(8,128)(2,1)S(1)}, bf16[16,512]{1,0:T(8,128)(2,1)S(1)}, u32[]{:S(2)}, u32[]{:S(2)}) collective-permute-start(bf16[16,512]{1,0:T(8,128)(2,1)S(1)} %attend.1), channel_id=1, source_target_pairs={{0,24},{8,16},{16,8},{24,0},{1,25},{9,17},{17,9},{25,1},{2,26},{10... | collective-permute-start | bytes 49160 | tf_op jit(solution)/shard_map/ppermute | solution.py:27
  83.9 11.6 %all-to-all-start = ((bf16[64,8,128]{2,0,1:T(8,128)(2,1)}), bf16[64,8,128]{2,0,1:T(8,128)(2,1)S(1)}, u32[]{:S(2)}, u32[]{:S(2)}) async-start(bf16[64,8,128]{2,0,1:T(8,128)(2,1)} %bitcast.79), calls=%async_computation | async-start | bytes 262144 | tf_op jit(solution)/shard_map/all_to_all | solution.py:324
  95.7 9.4 %collective-permute-start.10 = (bf16[64,128]{0,1:T(8,128)(2,1)S(1)}, bf16[64,128]{0,1:T(8,128)(2,1)S(1)}, u32[]{:S(2)}, u32[]{:S(2)}) collective-permute-start(bf16[64,128]{0,1:T(8,128)(2,1)S(1)} %add_convert_fusion), channel_id=1, source_target_pairs={{0,0},{1,8},{2,16},{3,24},{4,1},{5,9},{6,17},{7,25},{8,2},{9,10},{... | collective-permute-start | bytes 49160 | tf_op jit(solution)/shard_map/ppermute | solution.py:347
  96.4 9.9 %collective-permute-start.11 = (bf16[64,128]{0,1:T(8,128)(2,1)S(1)}, bf16[64,128]{0,1:T(8,128)(2,1)S(1)}, u32[]{:S(2)}, u32[]{:S(2)}) collective-permute-start(bf16[64,128]{0,1:T(8,128)(2,1)S(1)} %add_convert_fusion), channel_id=1, source_target_pairs={{0,24},{1,16},{2,8},{3,0},{4,25},{5,17},{6,9},{7,1},{8,26},{9,18},... | collective-permute-start | bytes 49160 | tf_op jit(solution)/shard_map/ppermute | solution.py:347
  103.4 6.4 %collective-permute-start.12 = (bf16[64,128]{0,1:T(8,128)(2,1)S(1)}, bf16[64,128]{0,1:T(8,128)(2,1)S(1)}, u32[]{:S(2)}, u32[]{:S(2)}) collective-permute-start(bf16[64,128]{0,1:T(8,128)(2,1)S(1)} %add_convert_fusion), channel_id=1, source_target_pairs={{0,16},{1,24},{2,0},{3,8},{4,17},{5,25},{6,1},{7,9},{8,18},{9,26},... | collective-permute-start | bytes 49160 | tf_op jit(solution)/shard_map/ppermute | solution.py:347
  103.4 6.4 %collective-permute-start.9 = (bf16[64,128]{0,1:T(8,128)(2,1)S(1)}, bf16[64,128]{0,1:T(8,128)(2,1)S(1)}, u32[]{:S(2)}, u32[]{:S(2)}) collective-permute-start(bf16[64,128]{0,1:T(8,128)(2,1)S(1)} %add_convert_fusion), channel_id=1, source_target_pairs={{0,8},{1,0},{2,24},{3,16},{4,9},{5,1},{6,25},{7,17},{8,10},{9,2},{... | collective-permute-start | bytes 49160 | tf_op jit(solution)/shard_map/ppermute | solution.py:347
  110.6 1.2 collective-permute-start.13
  111.9 3.6 %collective-permute-start.14 = (f32[2,64]{1,0:T(2,128)S(1)}, f32[2,64]{1,0:T(2,128)S(1)}, u32[]{:S(2)}, u32[]{:S(2)}) collective-permute-start(f32[2,64]{1,0:T(2,128)S(1)} %fusion.41), channel_id=1, source_target_pairs={{0,2},{1,3},{2,0},{3,1},{4,6},{5,7},{6,4},{7,5},{8,10},{9,11},{10,... | collective-permute-start | bytes 1544 | tf_op jit(solution)/shard_map/ppermute | solution.py:27
  115.5 4.5 %collective-permute-start.15 = (f32[2,64]{1,0:T(2,128)S(1)}, f32[2,64]{1,0:T(2,128)S(1)}, u32[]{:S(2)}, u32[]{:S(2)}) collective-permute-start(f32[2,64]{1,0:T(2,128)S(1)} %fusion.85), channel_id=1, source_target_pairs={{0,4},{1,5},{2,6},{3,7},{4,0},{5,1},{6,2},{7,3},{8,12},{9,13},{10,... | collective-permute-start | bytes 1544 | tf_op jit(solution)/shard_map/ppermute | solution.py:27
  120.7 9.2 %copy-start.6 = (bf16[512,512]{1,0:T(8,128)(2,1)S(1)}, bf16[512,512]{1,0:T(8,128)(2,1)}, u32[]{:S(2)}) copy-start(bf16[512,512]{1,0:T(8,128)(2,1)} %param.39) | copy-start | bytes 1572868
  130.4 1.7 collective-permute-start.16
  132.2 6.3 %collective-permute-start.17 = (bf16[2,32,1280]{2,1,0:T(8,128)(2,1)S(1)}, bf16[2,32,1280]{2,1,0:T(8,128)(2,1)S(1)}, u32[]{:S(2)}, u32[]{:S(2)}) collective-permute-start(bf16[2,32,1280]{2,1,0:T(8,128)(2,1)S(1)} %select_convert_fusion.1), channel_id=1, source_target_pairs={{0,2},{1,3},{2,0},{3,1},{4,6},{5,7},{6,4},{7,5},{8,10},{9,11},{10,... | collective-permute-start | bytes 491528 | tf_op jit(solution)/shard_map/ppermute | solution.py:27
  132.3 52.3 %copy-start.7 = (f32[512]{0:T(512)S(1)}, f32[512]{0:T(512)}, u32[]{:S(2)}) copy-start(f32[512]{0:T(512)} %param.32) | copy-start | bytes 6148
  138.6 6.3 %collective-permute-start.18 = (bf16[2,32,640]{2,1,0:T(8,128)(2,1)S(1)}, bf16[2,32,640]{2,1,0:T(8,128)(2,1)S(1)}, u32[]{:S(2)}, u32[]{:S(2)}) collective-permute-start(bf16[2,32,640]{2,1,0:T(8,128)(2,1)S(1)} %select_convert_fusion.2), channel_id=1, source_target_pairs={{0,4},{1,5},{2,6},{3,7},{4,0},{5,1},{6,2},{7,3},{8,12},{9,13},{10,... | collective-permute-start | bytes 245768 | tf_op jit(solution)/shard_map/ppermute | solution.py:27
  145.0 5.0 %collective-permute-start.19 = (bf16[32,640]{1,0:T(8,128)(2,1)S(1)}, bf16[32,640]{1,0:T(8,128)(2,1)S(1)}, u32[]{:S(2)}, u32[]{:S(2)}) collective-permute-start(bf16[32,640]{1,0:T(8,128)(2,1)S(1)} %fusion.12), channel_id=1, source_target_pairs={{0,4},{1,5},{2,6},{3,7},{4,0},{5,1},{6,2},{7,3},{8,12},{9,13},{10,... | collective-permute-start | bytes 122888 | tf_op jit(solution)/shard_map/ppermute | solution.py:27
  145.1 5.0 %collective-permute-start.22 = (f32[1,64]{1,0:T(1,128)S(1)}, f32[1,64]{1,0:T(1,128)S(1)}, u32[]{:S(2)}, u32[]{:S(2)}) collective-permute-start(f32[1,64]{1,0:T(1,128)S(1)} %bitcast.101), channel_id=1, source_target_pairs={{0,1},{1,0},{2,3},{3,2},{4,5},{5,4},{6,7},{7,6},{8,9},{9,8},{10,11... | collective-permute-start | bytes 776 | tf_op jit(solution)/shard_map/ppermute | solution.py:27
  150.0 6.4 %collective-permute-start.20 = (bf16[32,1280]{1,0:T(8,128)(2,1)S(1)}, bf16[32,1280]{1,0:T(8,128)(2,1)S(1)}, u32[]{:S(2)}, u32[]{:S(2)}) collective-permute-start(bf16[32,1280]{1,0:T(8,128)(2,1)S(1)} %pad_maximum_fusion.7), channel_id=1, source_target_pairs={{0,2},{1,3},{2,0},{3,1},{4,6},{5,7},{6,4},{7,5},{8,10},{9,11},{10,... | collective-permute-start | bytes 245768 | tf_op jit(solution)/shard_map/ppermute | solution.py:27
  150.1 4.5 %collective-permute-start.23 = (f32[1,64]{1,0:T(1,128)S(1)}, f32[1,64]{1,0:T(1,128)S(1)}, u32[]{:S(2)}, u32[]{:S(2)}) collective-permute-start(f32[1,64]{1,0:T(1,128)S(1)} %bitcast_add_fusion), channel_id=1, source_target_pairs={{0,2},{1,3},{2,0},{3,1},{4,6},{5,7},{6,4},{7,5},{8,10},{9,11},{10,... | collective-permute-start | bytes 776 | tf_op jit(solution)/shard_map/ppermute | solution.py:27
  154.6 4.5 %collective-permute-start.24 = (f32[1,64]{1,0:T(1,128)S(1)}, f32[1,64]{1,0:T(1,128)S(1)}, u32[]{:S(2)}, u32[]{:S(2)}) collective-permute-start(f32[1,64]{1,0:T(1,128)S(1)} %add.168), channel_id=1, source_target_pairs={{0,4},{1,5},{2,6},{3,7},{4,0},{5,1},{6,2},{7,3},{8,12},{9,13},{10,... | collective-permute-start | bytes 776 | tf_op jit(solution)/shard_map/ppermute | solution.py:27
  156.5 2.7 %collective-permute-start.21 = (bf16[32,2560]{1,0:T(8,128)(2,1)S(1)}, bf16[32,2560]{1,0:T(8,128)(2,1)S(1)}, u32[]{:S(2)}, u32[]{:S(2)}) collective-permute-start(bf16[32,2560]{1,0:T(8,128)(2,1)S(1)} %pad_maximum_fusion.6), channel_id=1, source_target_pairs={{0,1},{1,0},{2,3},{3,2},{4,5},{5,4},{6,7},{7,6},{8,9},{9,8},{10,11... | collective-permute-start | bytes 491528 | tf_op jit(solution)/shard_map/ppermute | solution.py:27
  165.7 5.8 %collective-permute-start.25 = (bf16[16,512]{0,1:T(8,128)(2,1)S(1)}, bf16[16,512]{0,1:T(8,128)(2,1)S(1)}, u32[]{:S(2)}, u32[]{:S(2)}) collective-permute-start(bf16[16,512]{0,1:T(8,128)(2,1)S(1)} %get-tuple-element.21), channel_id=1, source_target_pairs={{0,8},{8,0},{16,24},{24,16},{1,9},{9,1},{17,25},{25,17},{2,10},{10... | collective-permute-start | bytes 49160 | tf_op jit(solution)/shard_map/ppermute | solution.py:27
  166.6 6.4 %collective-permute-start.26 = (bf16[16,512]{0,1:T(8,128)(2,1)S(1)}, bf16[16,512]{0,1:T(8,128)(2,1)S(1)}, u32[]{:S(2)}, u32[]{:S(2)}) collective-permute-start(bf16[16,512]{0,1:T(8,128)(2,1)S(1)} %get-tuple-element.23), channel_id=1, source_target_pairs={{0,16},{8,24},{16,0},{24,8},{1,17},{9,25},{17,1},{25,9},{2,18},{10... | collective-permute-start | bytes 49160 | tf_op jit(solution)/shard_map/ppermute | solution.py:27
  169.1 5.9 %collective-permute-start.27 = (bf16[16,512]{0,1:T(8,128)(2,1)S(1)}, bf16[16,512]{0,1:T(8,128)(2,1)S(1)}, u32[]{:S(2)}, u32[]{:S(2)}) collective-permute-start(bf16[16,512]{0,1:T(8,128)(2,1)S(1)} %get-tuple-element.22), channel_id=1, source_target_pairs={{0,24},{8,16},{16,8},{24,0},{1,25},{9,17},{17,9},{25,1},{2,26},{10... | collective-permute-start | bytes 49160 | tf_op jit(solution)/shard_map/ppermute | solution.py:27
  175.1 1.2 collective-permute-start.28
  176.3 3.6 %collective-permute-start.29 = (f32[2,16]{1,0:T(2,128)S(1)}, f32[2,16]{1,0:T(2,128)S(1)}, u32[]{:S(2)}, u32[]{:S(2)}) collective-permute-start(f32[2,16]{1,0:T(2,128)S(1)} %fusion.40), channel_id=1, source_target_pairs={{0,2},{1,3},{2,0},{3,1},{4,6},{5,7},{6,4},{7,5},{8,10},{9,11},{10,... | collective-permute-start | bytes 392 | tf_op jit(solution)/shard_map/ppermute | solution.py:27
  180.0 4.5 %collective-permute-start.30 = (f32[2,16]{1,0:T(2,128)S(1)}, f32[2,16]{1,0:T(2,128)S(1)}, u32[]{:S(2)}, u32[]{:S(2)}) collective-permute-start(f32[2,16]{1,0:T(2,128)S(1)} %fusion.84), channel_id=1, source_target_pairs={{0,4},{1,5},{2,6},{3,7},{4,0},{5,1},{6,2},{7,3},{8,12},{9,13},{10,... | collective-permute-start | bytes 392 | tf_op jit(solution)/shard_map/ppermute | solution.py:27

commit v2 on v0

v2 whole, which is shorter than its diff:
```python
import functools

import jax
import jax.numpy as jnp
import numpy as np
from jax import lax
from jax.experimental import pallas as pl
from jax.experimental.pallas import tpu as pltpu
from jax.sharding import PartitionSpec as P

SUB = 64
VD = 128
TOPK = 2
CAP = 4
LANES = 128
TAIL = 8
STATS = 4

theta_base = 500000.0
score_scale = 0.125
head_scale = 0.8
residual_scale = 2.0**0.5
layer_epsilon = 1e-05
head_epsilon = 1e-06

F32 = jnp.float32
BF16 = jnp.bfloat16

IN_VMEM = pl.BlockSpec(memory_space=pltpu.VMEM)
IN_SMEM = pl.BlockSpec(memory_space=pltpu.SMEM)


def call(kernel, name, outs, args, scalars=0, scratch=(), mib=4, **sizes):
    return pl.pallas_call(
        functools.partial(kernel, **sizes),
        out_shape=[jax.ShapeDtypeStruct(shape, dtype) for shape, dtype in outs],
        in_specs=[IN_SMEM] * scalars + [IN_VMEM] * (len(args) - scalars),
        out_specs=[IN_VMEM] * len(outs),
        scratch_shapes=[pltpu.VMEM(shape, dtype) for shape, dtype in scratch],
        compiler_params=pltpu.CompilerParams(vmem_limit_bytes=mib * 1024 * 1024),
        name=name,
    )(*args)


def xor_permute(array, axis, count, distance):
    return lax.ppermute(array, axis, [(i, i ^ distance) for i in range(count)])


def xor_all(arrays, axis, count):
    return [xor_permute(arrays[d - 1], axis, count, d) for d in range(1, count)]


def aligned(index, size):
    return pl.ds(pl.multiple_of(index * size, LANES), size)


def iota(shape, dim):
    return lax.broadcasted_iota(jnp.int32, shape, dim)


def row_of(column):
    size = column.shape[0]
    eye = iota((size, size), 0) == iota((size, size), 1)
    return jnp.sum(jnp.where(eye, column, 0.0), axis=0, keepdims=True)


def column_of(row, start, size):
    width = row.shape[1]
    eye = iota((size, width), 0) + start == iota((size, width), 1)
    return jnp.sum(jnp.where(eye, row, 0.0), axis=1, keepdims=True)


def pieces_of(value, count):
    parts = []
    for _ in range(count):
        part = value.astype(BF16).astype(F32)
        parts.append(part)
        value = value - part
    return parts


WEIGHT_LANE = TOPK
MEAN_LANE = WEIGHT_LANE + 3 * TOPK


def prepare_kernel(lengths, tokens, ids, weights, frequency, *outs, ep_count):
    seq_count, width = tokens.shape
    block = width // ep_count
    ep = lax.axis_index("ep")
    lane = iota((seq_count, LANES), 1)
    extra = jnp.zeros((seq_count, LANES), F32)
    fields = []
    for k in range(TOPK):
        fields.append((k, column_of(ids[k : k + 1, :].astype(F32), 0, seq_count)))
        weight = column_of(weights[k : k + 1, :], 0, seq_count)
        for i, part in enumerate(pieces_of(weight, 3)):
            fields.append((WEIGHT_LANE + 3 * k + i, part))
    mean = jnp.sum(tokens[...].astype(F32), axis=1, keepdims=True) * (1.0 / width)
    for i, part in enumerate(pieces_of(mean, 3)):
        fields.append((MEAN_LANE + i, part))
    for place, value in fields:
        extra = jnp.where(lane == place, value, extra)
    extra = extra.astype(BF16)
    for d in range(ep_count):
        outs[d][:, :block] = tokens[:, aligned(ep ^ d, block)]
        outs[d][:, block:] = extra
    row = iota((seq_count, LANES), 0)
    position = jnp.zeros((seq_count, LANES), F32)
    for s in range(seq_count):
        position = jnp.where(row == s, lengths[s].astype(F32), position)
    angle = position * frequency[...]
    low_half = (lane % SUB) < (SUB // 2)
    sine = jnp.sin(angle)
    outs[ep_count][...] = jnp.cos(angle)
    outs[ep_count + 1][...] = jnp.where(low_half, -sine, sine)


def project_kernel(*refs, ep_count):
    pieces, weights, outs = refs[:ep_count], refs[ep_count : ep_count + 3], refs[ep_count + 3 :]
    rows = pieces[0].shape[0]
    block = weights[0].shape[0]
    columns = jnp.concatenate([piece[:, :block] for piece in pieces], axis=0)
    start = 0
    for weight in weights:
        size = weight.shape[1]
        part = jnp.dot(columns, weight[...], preferred_element_type=F32)
        for d in range(ep_count):
            outs[d][:, start : start + size] = part[d * rows : (d + 1) * rows].astype(
                outs[d].dtype
            )
        start += size


def attend_kernel(lengths, lambdas, *refs, ep_count, group):
    sums = refs[:ep_count]
    cos_ref, sin_ref, gain, keys, values, out, query_rows, key_rows, value_rows, out_rows = refs[
        ep_count:
    ]
    seq_count = keys.shape[0]
    heads = lambdas.shape[0]
    kv_local = (sums[0].shape[1] // LANES - heads) // 2
    per_kv = heads // kv_local
    width = keys.shape[1]
    rows = 2 * heads
    cosine = cos_ref[...]
    sine = sin_ref[...]
    lane = iota((seq_count, LANES), 1)
    low_half = (lane % SUB) < (SUB // 2)
    first_sub = lane < SUB

    def column(index):
        place = slice(index * LANES, (index + 1) * LANES)
        total = sums[0][:, place]
        for other in sums[1:]:
            total = total + other[:, place].astype(F32)
        return total.astype(BF16).astype(F32)

    def rotated(block):
        swapped = jnp.where(
            low_half, pltpu.roll(block, LANES - SUB // 2, 1), pltpu.roll(block, SUB // 2, 1)
        )
        return (block * cosine + swapped * sine).astype(BF16).astype(F32)

    for h in range(heads):
        turned = rotated(column(h)) * score_scale
        query_rows[:, h, :] = jnp.where(first_sub, turned, 0.0)
        query_rows[:, heads + h, :] = jnp.where(first_sub, 0.0, turned)
    for k in range(kv_local):
        turned = rotated(column(heads + k))
        fresh_value = column(heads + kv_local + k)
        for g in range(per_kv):
            for place in (k * per_kv + g, heads + k * per_kv + g):
                key_rows[:, place, :] = turned
                value_rows[:, place, :] = fresh_value

    row_kv = (iota((rows, width), 0) % heads) // per_kv
    place = iota((rows, width), 1)
    position = jnp.where((place % kv_local) == row_kv, place // kv_local, width)
    head_row = iota((rows, 1), 0)
    head_weight = jnp.ones((rows, 1), F32)
    for h in range(heads):
        head_weight = jnp.where(head_row == heads + h, -lambdas[h], head_weight)

    def several(step, carry):
        base = step * group
        scores, mixed = [], []
        for u in range(group):
            part = lax.dot_general(
                query_rows[base + u].astype(BF16),
                keys[base + u],
                (((1,), (1,)), ((), ())),
                preferred_element_type=F32,
            )
            scores.append(jnp.where(position < lengths[base + u], part, -jnp.inf))
        for u in range(group):
            fresh = jnp.sum(
                query_rows[base + u] * key_rows[base + u], axis=1, keepdims=True
            )
            highest = jnp.maximum(jnp.max(scores[u], axis=1, keepdims=True), fresh)
            weight = jnp.exp(scores[u] - highest)
            fresh_weight = jnp.exp(fresh - highest)
            factor = head_weight / (jnp.sum(weight, axis=1, keepdims=True) + fresh_weight)
            weight = weight * factor
            fresh_weight = jnp.broadcast_to(fresh_weight * factor, (rows, LANES))
            mixed.append((weight + pltpu.roll(weight, heads, 0)).astype(BF16))
            fresh_weight = fresh_weight + pltpu.roll(fresh_weight, heads, 0)
            out_rows[base + u] = fresh_weight.astype(BF16).astype(F32) * value_rows[base + u]
        for u in range(group):
            out_rows[base + u] += jnp.dot(
                mixed[u], values[base + u], preferred_element_type=F32
            )
        return carry

    lax.fori_loop(0, seq_count // group, several, 0)
    for h in range(heads):
        head = out_rows[:, h, :]
        square_mean = jnp.mean(head * head, axis=1, keepdims=True)
        normed = head * lax.rsqrt(square_mean + head_epsilon) * gain[...] * head_scale
        out[:, h * LANES : (h + 1) * LANES] = normed.astype(BF16)


def out_kernel(*refs, ep_count, ratio):
    heads, weight, outs, full = (
        refs[:ep_count],
        refs[ep_count],
        refs[ep_count + 1 : ep_count + 1 + ratio],
        refs[-1],
    )
    rows = jnp.concatenate([ref[...] for ref in heads], axis=0)
    full[...] = jnp.dot(rows, weight[...], preferred_element_type=F32)
    side = lax.axis_index("tp") % ratio
    size = outs[0].shape[1]
    for d in range(ratio):
        outs[d][...] = full[:, aligned(side ^ d, size)].astype(outs[d].dtype)


def add_kernel(*refs):
    total = refs[0][...].astype(F32)
    for ref in refs[1:-1]:
        total = total + ref[...].astype(F32)
    refs[-1][...] = total.astype(refs[-1].dtype)


def residual_kernel(*refs, ep_count, ratio):
    sums, pieces, out = refs[:ep_count], refs[ep_count : 2 * ep_count], refs[-1]
    rows = pieces[0].shape[0]
    size = out.shape[1]
    side = lax.axis_index("tp") % ratio
    block = pieces[0].shape[1] - LANES
    for d in range(ep_count):
        place = slice(d * rows, (d + 1) * rows)
        total = sums[0][place, :].astype(F32)
        for other in sums[1:]:
            total = total + other[place, :].astype(F32)
        extra = pieces[d][:, block:].astype(F32)
        mean = extra[:, MEAN_LANE : MEAN_LANE + 1]
        for i in range(1, 3):
            mean = mean + extra[:, MEAN_LANE + i : MEAN_LANE + i + 1]
        own = pieces[d][:, aligned(side, size)].astype(F32)
        out[place, :] = (residual_scale * (own - mean) + total).astype(BF16)


def send_part(sent, value):
    rows = value.shape[1]
    sent[:, : rows - STATS, :] = value[:, : rows - STATS, :].astype(BF16)
    sums = value[0, rows - STATS :, :] + value[1, rows - STATS :, :]
    high = sums.astype(BF16)
    sent[0, rows - STATS :, :] = high
    sent[1, rows - STATS :, :] = (sums - high.astype(F32)).astype(BF16)


def experts_kernel(*refs, ep_count, ratio, width):
    own = refs[0]
    arrivals = refs[1:ep_count]
    pieces = refs[ep_count : 2 * ep_count]
    (
        gain_ref,
        mix_ref,
        expert_gate,
        expert_up,
        dense_gate,
        dense_up,
        sent,
        kept,
        placed_out,
        info_out,
        own_out,
        full,
    ) = refs[2 * ep_count :]
    ep = lax.axis_index("ep")
    tp = lax.axis_index("tp")
    seq_count = pieces[0].shape[0]
    total_rows, size = own.shape
    local_experts = expert_gate.shape[0]
    expert_rows = ep_count * CAP
    slot_count = local_experts * expert_rows
    distance = ep ^ (tp // ratio)
    blocks = []
    for i in range(ep_count):
        rows = own[i * seq_count : (i + 1) * seq_count, :].astype(F32)
        rows = jnp.where(distance == 0, rows, 0.0)
        for d in range(1, ep_count):
            j = i ^ d
            rows = rows + arrivals[d - 1][j * seq_count : (j + 1) * seq_count, :].astype(F32)
        blocks.append(rows)
    own_out[...] = blocks[0]
    rows = jnp.concatenate(blocks, axis=0)
    gain = gain_ref[:, aligned(tp, size)]
    mix = mix_ref[:, aligned(tp, size)].astype(F32)
    scaled = rows * gain
    hidden = scaled.astype(BF16)

    block = pieces[0].shape[1] - LANES
    extra = jnp.concatenate([piece[:, block:] for piece in pieces], axis=0).astype(F32)
    token_row = iota((total_rows, total_rows), 0)
    token_lane = iota((total_rows, total_rows), 1)
    earlier = (token_lane < token_row) & (token_lane // seq_count == token_row // seq_count)
    ids = [extra[:, k : k + 1] for k in range(TOPK)]
    id_rows = [row_of(column) for column in ids]
    weights = []
    for k in range(TOPK):
        first = WEIGHT_LANE + 3 * k
        weights.append(
            extra[:, first : first + 1]
            + extra[:, first + 1 : first + 2]
            + extra[:, first + 2 : first + 3]
        )
    weight_sum = weights[0]
    for k in range(1, TOPK):
        weight_sum = weight_sum + weights[k]
    token_block = (iota((total_rows, 1), 0) // seq_count).astype(F32)
    slot_row = iota((slot_count, total_rows), 0).astype(F32)
    placed = jnp.zeros((slot_count, total_rows), F32)
    info = jnp.zeros((total_rows, LANES), F32)
    info_lane = iota((total_rows, LANES), 1)
    first_expert = (ep * local_experts).astype(F32)
    for k in range(TOPK):
        same = jnp.zeros((total_rows, total_rows), F32)
        for other in id_rows:
            same = same + jnp.where(earlier & (ids[k] == other), 1.0, 0.0)
        rank = jnp.sum(same, axis=1, keepdims=True)
        local = ids[k] - first_expert
        slot = local * expert_rows + token_block * CAP + rank
        slot = jnp.where((local >= 0.0) & (local < local_experts), slot, -1.0)
        placed = placed + jnp.where(slot_row == row_of(slot), 1.0, 0.0)
        info = jnp.where(info_lane == k, slot, info)
        info = jnp.where(info_lane == TOPK + k, weights[k] / weight_sum, info)
    info_out[...] = info
    placed_out[...] = placed
    routed = jnp.dot(placed.astype(BF16), hidden, preferred_element_type=F32).astype(BF16)

    sums = [
        jnp.sum(rows, axis=1, keepdims=True),
        jnp.sum(rows * rows, axis=1, keepdims=True),
        jnp.sum(scaled * mix, axis=1, keepdims=True),
        jnp.broadcast_to(jnp.sum(gain * mix, axis=1, keepdims=True), (total_rows, 1)),
    ]
    gain_high = gain.astype(BF16).astype(F32)
    gain_row = iota((16, size), 0)
    gain_rows = jnp.where(
        gain_row == 0, gain_high, jnp.where(gain_row == 1, gain - gain_high, 0.0)
    ).astype(BF16)
    expert_width = expert_gate.shape[2]
    dense_width = dense_gate.shape[1]
    fold = total_rows // slot_count
    full[:, slot_count:, :] = jnp.zeros((2, TAIL, full.shape[2]), F32)
    dense_rows = jnp.concatenate([hidden, gain_rows], axis=0)
    for plane, (expert_weight, dense_weight) in enumerate(
        ((expert_gate, dense_gate), (expert_up, dense_up))
    ):
        for e in range(local_experts):
            lhs = jnp.concatenate(
                [routed[e * expert_rows : (e + 1) * expert_rows], gain_rows], axis=0
            )
            part = jnp.dot(lhs, expert_weight[e], preferred_element_type=F32)
            full[plane, e * expert_rows : (e + 1) * expert_rows, :expert_width] = part[
                :expert_rows
            ]
            full[plane, slot_count + e : slot_count + e + 1, :expert_width] = (
                part[expert_rows : expert_rows + 1] + part[expert_rows + 1 : expert_rows + 2]
            )
        part = jnp.dot(dense_rows, dense_weight[...], preferred_element_type=F32)
        gain_part = part[total_rows : total_rows + 1] + part[total_rows + 1 : total_rows + 2]
        for f in range(fold):
            place = slice(expert_width + f * dense_width, expert_width + (f + 1) * dense_width)
            full[plane, :slot_count, place] = part[f * slot_count : (f + 1) * slot_count]
            for e in range(local_experts):
                full[plane, slot_count + e : slot_count + e + 1, place] = gain_part
    for start in range(0, full.shape[2], width):
        for i in range(STATS):
            at = slot_count + TAIL - STATS + i
            full[0, at : at + 1, start : start + total_rows] = row_of(sums[i])
    half = full.shape[2] // 2
    side = tp & 1
    send_part(sent, full[:, :, aligned(1 - side, half)])
    kept[...] = full[:, :, aligned(side, half)]


def columns_kernel(kept_in, got, sent, kept, full, *, bit):
    full[...] = kept_in[...] + got[...].astype(F32)
    half = full.shape[2] // 2
    side = (lax.axis_index("tp") >> bit) & 1
    send_part(sent, full[:, :, aligned(1 - side, half)])
    kept[...] = full[:, :, aligned(side, half)]


def rows_kernel(kept_in, got, sent, kept, full, *, bit):
    full[...] = kept_in[...] + got[...].astype(F32)
    half = (full.shape[1] - TAIL) // 2
    side = (lax.axis_index("tp") >> bit) & 1
    tail = full[:, 2 * half :, :]
    other = full[:, pl.ds(pl.multiple_of((1 - side) * half, 8), half), :]
    send_part(sent, jnp.concatenate([other, tail], axis=1))
    kept[:, :half, :] = full[:, pl.ds(pl.multiple_of(side * half, 8), half), :]
    kept[:, half:, :] = tail


def act_kernel(
    kept, got, placed, act, stats, *, model_width, expert_width, dense_width, expert_rows, bits
):
    column_bits, row_bits = bits
    total = kept[...] + got[...].astype(F32)
    rows = total.shape[1] - TAIL
    width = total.shape[2]
    slot_count, total_rows = placed.shape
    tp = lax.axis_index("tp")
    sums = total[0, rows + TAIL - STATS :, :] + total[1, rows + TAIL - STATS :, :]
    sums = sums[:, :total_rows]
    mean = sums[0:1] * (1.0 / model_width)
    variance = sums[1:2] * (1.0 / model_width) - mean * mean
    scale = lax.rsqrt(variance + layer_epsilon)
    gate = jax.nn.sigmoid(scale * (sums[2:3] - mean * sums[3:4]))
    stats[0:1, :] = mean
    stats[1:2, :] = scale
    stats[2:3, :] = gate
    first_row = 0
    size = slot_count
    for bit in row_bits:
        size //= 2
        first_row = first_row + ((tp >> bit) & 1) * size
    first_column = 0
    size = expert_width + dense_width * (total_rows // slot_count)
    for bit in column_bits:
        size //= 2
        first_column = first_column + ((tp >> bit) & 1) * size
    mine = placed[pl.ds(pl.multiple_of(first_row, 8), rows), :]
    scale_used = jnp.sum(mine * scale, axis=1, keepdims=True)
    mean_used = jnp.sum(mine * mean, axis=1, keepdims=True)
    column = iota((rows, width), 1) + first_column
    scale_used = jnp.broadcast_to(scale_used, (rows, width))
    mean_used = jnp.broadcast_to(mean_used, (rows, width))
    for f in range(total_rows // slot_count):
        dense = column >= expert_width + f * dense_width
        start = first_row + f * slot_count
        scale_used = jnp.where(dense, column_of(scale, start, rows), scale_used)
        mean_used = jnp.where(dense, column_of(mean, start, rows), mean_used)
    expert = (iota((rows, width), 0) + first_row) // expert_rows
    pre = []
    for plane in range(2):
        gain_sum = jnp.zeros((rows, width), F32)
        for e in range(slot_count // expert_rows):
            gain_sum = jnp.where(expert == e, total[plane, rows + e : rows + e + 1, :], gain_sum)
        pre.append(scale_used * (total[plane, :rows, :] - mean_used * gain_sum))
    act[0] = (pre[0] / (1.0 + jnp.exp(-pre[0])) * pre[1]).astype(BF16)


def down_kernel(
    acts,
    stats,
    info,
    own_rows,
    gain_ref,
    expert_down,
    dense_down,
    *refs,
    ep_count,
    places,
):
    outs, joined = refs[:ep_count], refs[ep_count]
    tp = lax.axis_index("tp")
    piece_rows, piece_width = acts.shape[1:]
    for index, (row, column) in enumerate(places):
        block = acts[index ^ reverse_bits(tp, len(places))]
        joined[row : row + piece_rows, column : column + piece_width] = block
    local_experts, expert_width, size = expert_down.shape
    dense_width = dense_down.shape[0]
    slot_count = joined.shape[0]
    expert_rows = slot_count // local_experts
    total_rows = info.shape[0]
    seq_count = total_rows // ep_count
    results = []
    for e in range(local_experts):
        lhs = joined[e * expert_rows : (e + 1) * expert_rows, :expert_width]
        results.append(jnp.dot(lhs, expert_down[e], preferred_element_type=F32))
    result = jnp.concatenate(results, axis=0).astype(BF16)
    fold = total_rows // slot_count
    dense_rows = jnp.concatenate(
        [
            joined[:, expert_width + f * dense_width : expert_width + (f + 1) * dense_width]
            for f in range(fold)
        ],
        axis=0,
    )
    dense = jnp.dot(dense_rows, dense_down[...], preferred_element_type=F32)
    mixed = column_of(stats[2:3, :], 0, total_rows) * dense
    slot_lane = iota((total_rows, slot_count), 1).astype(F32)
    for k in range(TOPK):
        chosen = jnp.where(info[:, k : k + 1] == slot_lane, 1.0, 0.0).astype(BF16)
        picked = jnp.dot(chosen, result, preferred_element_type=F32)
        mixed = mixed + info[:, TOPK + k : TOPK + k + 1] * picked
    gain = gain_ref[:, aligned(tp, size)]
    mean = column_of(stats[0:1, :], 0, seq_count)
    scale = column_of(stats[1:2, :], 0, seq_count)
    hidden = (own_rows[...] - mean) * scale * gain
    outs[0][...] = mixed[:seq_count] + residual_scale * hidden
    for d in range(1, ep_count):
        outs[d][...] = mixed[d * seq_count : (d + 1) * seq_count].astype(BF16)


def reverse_bits(index, count):
    steps = count.bit_length() - 1
    total = 0
    for step in range(steps):
        total = total + (((index >> step) & 1) << (steps - 1 - step))
    return total


def combine_kernel(*refs):
    combined, moments = refs[-2:]
    total = refs[0][...]
    for ref in refs[1:-2]:
        total = total + ref[...].astype(F32)
    combined[...] = total
    moments[...] = jnp.zeros(moments.shape, F32)
    rows = total.shape[0]
    moments[0:1, :rows] = row_of(jnp.sum(total, axis=1, keepdims=True))
    moments[1:2, :rows] = row_of(jnp.sum(total * total, axis=1, keepdims=True))


def norm_kernel(*refs, model_width):
    combined, gain = refs[0], refs[1]
    out = refs[-1]
    sums = refs[2][...]
    for ref in refs[3:-1]:
        sums = sums + ref[...]
    mean = sums[0:1] * (1.0 / model_width)
    variance = sums[1:2] * (1.0 / model_width) - mean * mean
    rows = combined.shape[0]
    scale = column_of(lax.rsqrt(variance + layer_epsilon), 0, rows)
    out[...] = ((combined[...] - column_of(mean, 0, rows)) * scale * gain[...]).astype(BF16)


def on_device(
    tokens,
    query_weight,
    key_weight,
    value_weight,
    out_weight,
    head_lambda,
    head_gain,
    key_cache,
    value_cache,
    lengths,
    first_gain,
    second_gain,
    expert_ids,
    route_weights,
    expert_gate,
    expert_up,
    expert_down,
    dense_gate,
    dense_up,
    dense_down,
    dense_mix,
):
    seq_count, model_width = tokens.shape
    ep_count = lax.axis_size("ep")
    tp_count = lax.axis_size("tp")
    ratio = tp_count // ep_count
    block_width = model_width // ep_count
    slice_width = model_width // tp_count
    local_experts, _, expert_width = expert_gate.shape
    dense_width = dense_gate.shape[1]
    expert_rows = ep_count * CAP
    slot_count = local_experts * expert_rows
    total_rows = ep_count * seq_count
    heads = head_lambda.shape[0]
    cache, kv_local = key_cache.shape[1:3]

    frequency = theta_base ** (-(np.arange(SUB // 2, dtype=np.float64) * (2.0 / SUB)))
    frequency = np.tile(frequency, LANES // (SUB // 2)).astype(np.float32)[None, :]
    piece = ((seq_count, block_width + LANES), BF16)
    table = ((seq_count, LANES), F32)
    *pieces, cosine, sine = call(
        prepare_kernel,
        "prepare",
        [piece] * ep_count + [table] * 2,
        [lengths, tokens, expert_ids.T, route_weights.T, jnp.asarray(frequency)],
        scalars=1,
        ep_count=ep_count,
    )
    pieces = [pieces[0]] + xor_all(pieces[1:], "ep", ep_count)
    qkv_width = (heads + 2 * kv_local) * LANES
    sums = call(
        project_kernel,
        "project",
        [((seq_count, qkv_width), F32)] + [((seq_count, qkv_width), BF16)] * (ep_count - 1),
        pieces + [query_weight, key_weight, value_weight],
        ep_count=ep_count,
    )
    sums = [sums[0]] + xor_all(sums[1:], "ep", ep_count)
    rows_scratch = ((seq_count, 2 * heads, LANES), F32)
    (normed,) = call(
        attend_kernel,
        "attend",
        [((seq_count, heads * VD), BF16)],
        [lengths, head_lambda]
        + sums
        + [
            cosine,
            sine,
            head_gain[None, :],
            key_cache.reshape(seq_count, cache * kv_local, 2 * SUB),
            value_cache.reshape(seq_count, cache * kv_local, VD),
        ],
        scalars=2,
        scratch=[rows_scratch] * 4,
        ep_count=ep_count,
        group=min(8, seq_count),
    )
    all_heads = [normed] + xor_all([normed] * (ep_count - 1), "ep", ep_count)
    part = (total_rows, slice_width)
    parts = call(
        out_kernel,
        "outproj",
        [(part, F32)] + [(part, BF16)] * (ratio - 1),
        all_heads + [out_weight],
        scratch=[((total_rows, block_width), F32)],
        ep_count=ep_count,
        ratio=ratio,
    )
    parts = [parts[0]] + [
        xor_permute(parts[d], "tp", tp_count, d) for d in range(1, ratio)
    ]
    (part_sum,) = call(add_kernel, "pairsum", [(part, BF16)], parts)

    def device(ep, place, side):
        return ep * tp_count + place * ratio + side

    groups = [(c, h) for c in range(ep_count) for h in range(ratio)]
    both = ("ep", "tp")
    gathered = [part_sum] + [
        lax.ppermute(part_sum, both, [(device(c, c ^ d, h), device(c, c, h)) for c, h in groups])
        for d in range(1, ep_count)
    ]
    (residual,) = call(
        residual_kernel,
        "residual",
        [(part, BF16)],
        gathered + pieces,
        ep_count=ep_count,
        ratio=ratio,
    )
    arrivals = [
        lax.ppermute(residual, both, [(device(c, c, h), device(c ^ d, c, h)) for c, h in groups])
        for d in range(1, ep_count)
    ]

    width = expert_width + dense_width * (total_rows // slot_count)
    column_bits, row_bits = [], []
    piece_width, piece_rows = width, slot_count
    for bit in range(tp_count.bit_length() - 1):
        if piece_width % (2 * LANES) == 0 and not row_bits:
            column_bits.append(bit)
            piece_width //= 2
        else:
            row_bits.append(bit)
            piece_rows //= 2
    full_rows = slot_count + TAIL
    half = (2, full_rows, width // 2)
    sent, kept, placed, info, own_rows = call(
        experts_kernel,
        "experts",
        [
            (half, BF16),
            (half, F32),
            ((slot_count, total_rows), F32),
            ((total_rows, LANES), F32),
            ((seq_count, slice_width), F32),
        ],
        [residual]
        + arrivals
        + pieces
        + [
            first_gain[None, :],
            dense_mix[None, :],
            expert_gate,
            expert_up,
            dense_gate,
            dense_up,
        ],
        scratch=[((2, full_rows, width), F32)],
        mib=8,
        ep_count=ep_count,
        ratio=ratio,
        width=piece_width,
    )
    shape = list(half)
    for bit in range(1, tp_count.bit_length() - 1):
        got = xor_permute(sent, "tp", tp_count, 1 << (bit - 1))
        before = tuple(shape)
        if bit in column_bits:
            shape[2] //= 2
        else:
            shape[1] = (shape[1] - TAIL) // 2 + TAIL
        sent, kept = call(
            columns_kernel if bit in column_bits else rows_kernel,
            "fold%d" % bit,
            [(tuple(shape), BF16), (tuple(shape), F32)],
            [kept, got],
            scratch=[(before, F32)],
            bit=bit,
        )
    got = xor_permute(sent, "tp", tp_count, tp_count // 2)
    act, stats = call(
        act_kernel,
        "act",
        [((1, piece_rows, piece_width), BF16), ((8, total_rows), F32)],
        [kept, got, placed],
        model_width=model_width,
        expert_width=expert_width,
        dense_width=dense_width,
        expert_rows=expert_rows,
        bits=(column_bits, row_bits),
    )
    distance = tp_count // 2
    while distance:
        act = jnp.concatenate([act, xor_permute(act, "tp", tp_count, distance)], axis=0)
        distance //= 2
    steps = tp_count.bit_length() - 1
    places = []
    for index in range(tp_count):
        row, column, rows, columns = 0, 0, slot_count, width
        for bit in range(steps):
            up = (index >> (steps - 1 - bit)) & 1
            if bit in column_bits:
                columns //= 2
                column += up * columns
            else:
                rows //= 2
                row += up * rows
        places.append((row, column))
    mixed = call(
        down_kernel,
        "down",
        [((seq_count, slice_width), F32)]
        + [((seq_count, slice_width), BF16)] * (ep_count - 1),
        [act, stats, info, own_rows, first_gain[None, :], expert_down, dense_down],
        scratch=[((slot_count, width), BF16)],
        ep_count=ep_count,
        places=tuple(places),
    )
    mixed = [mixed[0]] + xor_all(mixed[1:], "ep", ep_count)
    combined, moments = call(
        combine_kernel,
        "combine",
        [((seq_count, slice_width), F32), ((8, LANES), F32)],
        mixed,
    )
    distance = 1
    while distance < tp_count:
        other = xor_permute(moments, "tp", tp_count, distance)
        distance *= 2
        if distance < tp_count:
            moments = moments + other
    (layer_out,) = call(
        norm_kernel,
        "norm",
        [((seq_count, slice_width), BF16)],
        [combined, second_gain[None, :], moments, other],
        model_width=model_width,
    )
    return layer_out


def solution(mesh):
    return jax.shard_map(
        on_device,
        mesh=mesh,
        in_specs=(
            P("ep", None),
            P("ep", "tp"),
            P("ep", "tp"),
            P("ep", "tp"),
            P("tp", "ep"),
            P("tp"),
            P(),
            P("ep", None, "tp", None),
            P("ep", None, "tp", None),
            P("ep"),
            P(),
            P("tp"),
            P("ep", None),
            P("ep", None),
            P("ep", "tp", None),
            P("ep", "tp", None),
            P("ep", None, "tp"),
            P("tp", "ep"),
            P("tp", "ep"),
            P("ep", "tp"),
            P(),
        ),
        out_specs=P("ep", "tp"),
        check_vma=False,
    )
```

time: 279 us -> 112 us (0.40)
  waiting for transfers between devices: 149 us -> 54.1 us
  matrix products: 34 us -> 0 us
  blocking collectives: 31.6 us -> 0 us
  starting transfers between devices: 15.9 us -> 29.5 us
  between operations: 13.5 us -> 0.32 us
  local copies, waits for them, and re-layouts: 27.8 us -> 15 us
  Pallas kernels: 0 us -> 12.3 us
  other arithmetic: 5.45 us -> 0.09 us
    psum x2 -> x0, waiting for transfers between devices: 110 us -> none  [the longest x1 55.1 us: on_device(): lax.psum(column_part.astype(jnp.bfloat16), 'tp').astype(jnp.float32)]
    ppermute x0 -> x28, waiting for transfers between devices: none -> 54.1 us  [the longest x22 45.5 us: xor_permute(): return lax.ppermute(array, axis, [(i, i ^ distance) for i in range(count)])]
    dot_general x16 -> x0, matrix products: 34 us -> none  [the longest x1 5.35 us: on_device(): jnp.einsum('erd,edf->erf', arrived, expert_gate, preferred_element_type=j...]
    ppermute x0 -> x28, starting transfers between devices: none -> 29.5 us  [the longest x22 21.8 us: xor_permute(): return lax.ppermute(array, axis, [(i, i ^ distance) for i in range(count)])]
    reduce_scatter x2 -> x0, waiting for transfers between devices: 23.8 us -> none  [the longest x1 22 us: on_device(): lax.psum_scatter(dense_part.astype(jnp.bfloat16), 'ep', scatter_dimension...]
    all_gather x2 -> x0, blocking collectives: 15.8 us -> none  [the longest x1 8.17 us: on_device(): all_heads = lax.all_gather(normed, 'ep', axis=0, tiled=True)]
    psum x1 -> x0, blocking collectives: 15.8 us -> none  [on_device(): lax.psum((jnp.sum(combined, axis=1), jnp.sum(combined * combined, axis=1)...]
    all_to_all x4 -> x0, starting transfers between devices: 15.8 us -> none  [the longest x1 5.19 us: on_device(): lax.all_to_all(tokens, 'ep', split_axis=1, concat_axis=0, tiled=True)]
  transfers between devices with their start and end apart: 8 -> 28, of which waited for: 8 -> 26; matrix products, arithmetic and copies ran while one was open for 10% -> 0% of each run, Pallas kernels for 0% -> 0%
where the time goes in v2:
time: 112 us; the launch traced here: 111 us
  waiting for transfers between devices  54.1 us (48%)
  starting transfers between devices  29.5 us (26%)
  local copies, waits for them, and re-layouts  15 us (13%)
  Pallas kernels  12.3 us (11%)
    ppermute x22, waiting for transfers between devices, xor_permute(): return lax.ppermute(array, axis, [(i, i ^ distance) for i in range(count)])  45.5 us
    ppermute x22, starting transfers between devices, xor_permute(): return lax.ppermute(array, axis, [(i, i ^ distance) for i in range(count)])  21.8 us
    unnamed x46, local copies, waits for them, and re-layouts  15 us
    pallas_call x13, Pallas kernels, call(): pl.pallas_call(functools.partial(kernel, **sizes), out_shape=[jax.ShapeDt...  12.3 us
    ppermute x3, waiting for transfers between devices, on_device(): lax.ppermute(part_sum, both, [(device(c, c ^ d, h), device(c, c, h)) for...  6.75 us
    ppermute x3, starting transfers between devices, on_device(): lax.ppermute(residual, both, [(device(c, c, h), device(c ^ d, c, h)) for...  3.88 us
    ppermute x3, starting transfers between devices, on_device(): lax.ppermute(part_sum, both, [(device(c, c ^ d, h), device(c, c, h)) for...  3.88 us
  transfers between devices with their start and end apart: 28, of which 26 were waited for; matrix products, arithmetic and copies ran while one was open for 0% of the time, Pallas kernels for 0%

profile of v2, /device:TPU:0, one launch (start us, length us, event | category | flops | bytes accessed | tf_op | source)
XLA Modules:
  0.0 111.3 jit_solution(4702685431942786191)
XLA Ops:
  0.0 0.9 copy-done.11
  0.9 0.7 copy-done.13
  1.6 0.7 copy-done.15
  2.2 0.7 copy-done.16
  2.9 0.7 copy-done.19
  3.6 0.7 prepare.1
  4.3 3.0 %collective-permute-start = (bf16[16,1152]{1,0:T(8,128)(2,1)S(1)}, bf16[16,1152]{1,0:T(8,128)(2,1)S(1)}, u32[]{:S(2)}, u32[]{:S(2)}) collective-permute-start(bf16[16,1152]{1,0:T(8,128)(2,1)S(1)} %get-tuple-element.35), channel_id=1, source_target_pairs={{0,8},{8,0},{16,24},{24,16},{1,9},{9,1},{17,25},{25,17},{2,10},{10... | collective-permute-start | bytes 110600 | tf_op jit(solution)/shard_map/ppermute | solution.py:46
  7.3 1.5 %collective-permute-start.1 = (bf16[16,1152]{1,0:T(8,128)(2,1)S(1)}, bf16[16,1152]{1,0:T(8,128)(2,1)S(1)}, u32[]{:S(2)}, u32[]{:S(2)}) collective-permute-start(bf16[16,1152]{1,0:T(8,128)(2,1)S(1)} %get-tuple-element.36), channel_id=1, source_target_pairs={{0,16},{8,24},{16,0},{24,8},{1,17},{9,25},{17,1},{25,9},{2,18},{10... | collective-permute-start | bytes 110600 | tf_op jit(solution)/shard_map/ppermute | solution.py:46
  8.8 0.4 collective-permute-done.refs_1_.refs_5_
  9.2 2.0 %collective-permute-done.1.refs_2_.refs_6_ = bf16[16,1152]{1,0:T(8,128)(2,1)S(1)} collective-permute-done((bf16[16,1152]{1,0:T(8,128)(2,1)S(1)}, bf16[16,1152]{1,0:T(8,128)(2,1)S(1)}, u32[]{:S(2)}, u32[]{:S(2)}) %collective-permute-start.1) | collective-permute-done | bytes 36896 | tf_op jit(solution)/shard_map/ppermute | solution.py:46
  11.3 2.4 %collective-permute-done.2.refs_3_.refs_7_ = bf16[16,1152]{1,0:T(8,128)(2,1)S(1)} collective-permute-done((bf16[16,1152]{1,0:T(8,128)(2,1)S(1)}, bf16[16,1152]{1,0:T(8,128)(2,1)S(1)}, u32[]{:S(2)}, u32[]{:S(2)}) %collective-permute-start.2) | collective-permute-done | bytes 36896 | tf_op jit(solution)/shard_map/ppermute | solution.py:46
  13.7 1.2 %copy-done.4 = bf16[1024,512]{1,0:T(8,128)(2,1)S(1)} copy-done((bf16[1024,512]{1,0:T(8,128)(2,1)S(1)}, bf16[1024,512]{1,0:T(8,128)(2,1)}, u32[]{:S(2)}) %copy-start.4) | copy-done | bytes 1048600
  14.9 1.0 copy-done.6
  16.0 1.0 copy-done.7
  17.0 0.5 project.1
  17.5 0.6 collective-permute-start.3
  18.1 2.9 %collective-permute-start.5 = (bf16[16,1024]{1,0:T(8,128)(2,1)S(1)}, bf16[16,1024]{1,0:T(8,128)(2,1)S(1)}, u32[]{:S(2)}, u32[]{:S(2)}) collective-permute-start(bf16[16,1024]{1,0:T(8,128)(2,1)S(1)} %get-tuple-element.41), channel_id=1, source_target_pairs={{0,24},{8,16},{16,8},{24,0},{1,25},{9,17},{17,9},{25,1},{2,26},{10... | collective-permute-start | bytes 98312 | tf_op jit(solution)/shard_map/ppermute | solution.py:46
  21.0 0.4 collective-permute-done.3.refs_1_
  21.5 0.5 collective-permute-done.4.refs_2_
  22.0 0.9 collective-permute-done.5.refs_3_
  22.9 3.4 %copy-done = bf16[16,1024,2,128]{3,2,1,0:T(2,128)(2,1)S(1)} copy-done((bf16[16,1024,2,128]{3,2,1,0:T(2,128)(2,1)S(1)}, bf16[16,1024,2,128]{3,2,1,0:T(2,128)(2,1)}, u32[]{:S(2)}) %copy-start) | copy-done | bytes 8388632
  26.3 3.4 %copy-done.1 = bf16[16,1024,2,128]{3,2,1,0:T(2,128)(2,1)S(1)} copy-done((bf16[16,1024,2,128]{3,2,1,0:T(2,128)(2,1)S(1)}, bf16[16,1024,2,128]{3,2,1,0:T(2,128)(2,1)}, u32[]{:S(2)}) %copy-start.1) | copy-done | bytes 8388632
  29.7 0.7 copy-done.17
  30.4 0.7 copy-done.18
  31.1 4.4 %attend.1.refs_0_ = bf16[16,512]{1,0:T(8,128)(2,1)S(1)} custom-call(s32[16]{0:T(128)S(1)} %copy-done.13, f32[4]{0:T(128)S(1)} %copy-done.17, f32[16,1024]{1,0:T(8,128)S(1)} %get-tuple-element.38.refs_0_, bf16[16,1024]{1,0:T(8,128)(2,1)S(1)} %collective-permute-done.3.refs_1_, bf16[16,1024]{1,0:T(8,128)(2,1)S(1)} %collective-permute-done.4.refs_2_, ...), custom_call_target="tpu_custom_call" | custom-call | tf_op jit(solution)/shard_map/attend/pallas_call | solution.py:34
  35.4 3.0 %collective-permute-start.8 = (bf16[16,512]{1,0:T(8,128)(2,1)S(1)}, bf16[16,512]{1,0:T(8,128)(2,1)S(1)}, u32[]{:S(2)}, u32[]{:S(2)}) collective-permute-start(bf16[16,512]{1,0:T(8,128)(2,1)S(1)} %attend.1.refs_0_), channel_id=1, source_target_pairs={{0,24},{8,16},{16,8},{24,0},{1,25},{9,17},{17,9},{25,1},{2,26},{10... | collective-permute-start | bytes 49160 | tf_op jit(solution)/shard_map/ppermute | solution.py:46
  38.4 0.5 collective-permute-start.7
  39.0 1.1 collective-permute-done.8.refs_3_
  40.1 2.0 %collective-permute-done.7.refs_2_ = bf16[16,512]{1,0:T(8,128)(2,1)S(1)} collective-permute-done((bf16[16,512]{1,0:T(8,128)(2,1)S(1)}, bf16[16,512]{1,0:T(8,128)(2,1)S(1)}, u32[]{:S(2)}, u32[]{:S(2)}) %collective-permute-start.7) | collective-permute-done | bytes 16416 | tf_op jit(solution)/shard_map/ppermute | solution.py:46
  42.1 0.5 collective-permute-done.6.refs_1_
  42.6 0.3 outproj.1
  43.0 1.2 %collective-permute-done.9.refs_1_ = bf16[64,512]{1,0:T(8,128)(2,1)S(1)} collective-permute-done((bf16[64,512]{1,0:T(8,128)(2,1)S(1)}, bf16[64,512]{1,0:T(8,128)(2,1)S(1)}, u32[]{:S(2)}, u32[]{:S(2)}) %collective-permute-start.9) | collective-permute-done | bytes 65568 | tf_op jit(solution)/shard_map/ppermute | solution.py:46
  44.3 1.3 %collective-permute-start.12 = (bf16[64,512]{1,0:T(8,128)(2,1)S(1)}, bf16[64,512]{1,0:T(8,128)(2,1)S(1)}, u32[]{:S(2)}, u32[]{:S(2)}) collective-permute-start(bf16[64,512]{1,0:T(8,128)(2,1)S(1)} %pairsum.1.refs_0_), channel_id=1, source_target_pairs={{6,0},{7,1},{12,10},{13,11},{18,20},{19,21},{24,30},{25,31}} | collective-permute-start | bytes 196616 | tf_op jit(solution)/shard_map/ppermute | solution.py:653
  45.6 1.3 %collective-permute-start.11 = (bf16[64,512]{1,0:T(8,128)(2,1)S(1)}, bf16[64,512]{1,0:T(8,128)(2,1)S(1)}, u32[]{:S(2)}, u32[]{:S(2)}) collective-permute-start(bf16[64,512]{1,0:T(8,128)(2,1)S(1)} %pairsum.1.refs_0_), channel_id=1, source_target_pairs={{4,0},{5,1},{14,10},{15,11},{16,20},{17,21},{26,30},{27,31}} | collective-permute-start | bytes 196616 | tf_op jit(solution)/shard_map/ppermute | solution.py:653
  46.9 1.3 %collective-permute-start.10 = (bf16[64,512]{1,0:T(8,128)(2,1)S(1)}, bf16[64,512]{1,0:T(8,128)(2,1)S(1)}, u32[]{:S(2)}, u32[]{:S(2)}) collective-permute-start(bf16[64,512]{1,0:T(8,128)(2,1)S(1)} %pairsum.1.refs_0_), channel_id=1, source_target_pairs={{2,0},{3,1},{8,10},{9,11},{22,20},{23,21},{28,30},{29,31}} | collective-permute-start | bytes 196616 | tf_op jit(solution)/shard_map/ppermute | solution.py:653
  48.2 4.1 %collective-permute-done.12.refs_3_ = bf16[64,512]{1,0:T(8,128)(2,1)S(1)} collective-permute-done((bf16[64,512]{1,0:T(8,128)(2,1)S(1)}, bf16[64,512]{1,0:T(8,128)(2,1)S(1)}, u32[]{:S(2)}, u32[]{:S(2)}) %collective-permute-start.12) | collective-permute-done | bytes 65568 | tf_op jit(solution)/shard_map/ppermute | solution.py:653
  52.3 1.3 %collective-permute-done.11.refs_2_ = bf16[64,512]{1,0:T(8,128)(2,1)S(1)} collective-permute-done((bf16[64,512]{1,0:T(8,128)(2,1)S(1)}, bf16[64,512]{1,0:T(8,128)(2,1)S(1)}, u32[]{:S(2)}, u32[]{:S(2)}) %collective-permute-start.11) | collective-permute-done | bytes 65568 | tf_op jit(solution)/shard_map/ppermute | solution.py:653
  53.7 1.3 %collective-permute-done.10.refs_1_ = bf16[64,512]{1,0:T(8,128)(2,1)S(1)} collective-permute-done((bf16[64,512]{1,0:T(8,128)(2,1)S(1)}, bf16[64,512]{1,0:T(8,128)(2,1)S(1)}, u32[]{:S(2)}, u32[]{:S(2)}) %collective-permute-start.10) | collective-permute-done | bytes 65568 | tf_op jit(solution)/shard_map/ppermute | solution.py:653
  55.1 1.3 %collective-permute-start.15 = (bf16[64,512]{1,0:T(8,128)(2,1)S(1)}, bf16[64,512]{1,0:T(8,128)(2,1)S(1)}, u32[]{:S(2)}, u32[]{:S(2)}) collective-permute-start(bf16[64,512]{1,0:T(8,128)(2,1)S(1)} %residual.1.refs_0_), channel_id=1, source_target_pairs={{0,24},{1,25},{10,18},{11,19},{20,12},{21,13},{30,6},{31,7}} | collective-permute-start | bytes 196616 | tf_op jit(solution)/shard_map/ppermute | solution.py:665
  56.4 1.3 %collective-permute-start.14 = (bf16[64,512]{1,0:T(8,128)(2,1)S(1)}, bf16[64,512]{1,0:T(8,128)(2,1)S(1)}, u32[]{:S(2)}, u32[]{:S(2)}) collective-permute-start(bf16[64,512]{1,0:T(8,128)(2,1)S(1)} %residual.1.refs_0_), channel_id=1, source_target_pairs={{0,16},{1,17},{10,26},{11,27},{20,4},{21,5},{30,14},{31,15}} | collective-permute-start | bytes 196616 | tf_op jit(solution)/shard_map/ppermute | solution.py:665
  57.7 1.3 %collective-permute-start.13 = (bf16[64,512]{1,0:T(8,128)(2,1)S(1)}, bf16[64,512]{1,0:T(8,128)(2,1)S(1)}, u32[]{:S(2)}, u32[]{:S(2)}) collective-permute-start(bf16[64,512]{1,0:T(8,128)(2,1)S(1)} %residual.1.refs_0_), channel_id=1, source_target_pairs={{0,8},{1,9},{10,2},{11,3},{20,28},{21,29},{30,22},{31,23}} | collective-permute-start | bytes 196616 | tf_op jit(solution)/shard_map/ppermute | solution.py:665
  59.1 0.5 collective-permute-done.14.refs_2_
  59.6 1.3 %collective-permute-done.13.refs_1_ = bf16[64,512]{1,0:T(8,128)(2,1)S(1)} collective-permute-done((bf16[64,512]{1,0:T(8,128)(2,1)S(1)}, bf16[64,512]{1,0:T(8,128)(2,1)S(1)}, u32[]{:S(2)}, u32[]{:S(2)}) %collective-permute-start.13) | collective-permute-done | bytes 65568 | tf_op jit(solution)/shard_map/ppermute | solution.py:665
  61.0 3.7 %experts.1 = (bf16[2,72,1280]{2,1,0:T(8,128)(2,1)S(1)}, f32[2,72,1280]{2,1,0:T(8,128)S(1)}, f32[64,64]{1,0:T(8,128)S(1)}, f32[64,128]{1,0:T(8,128)S(1)}, f32[16,512]{1,0:T(8,128)S(1)}) custom-call(bf16[64,512]{1,0:T(8,128)(2,1)S(1)} %residual.1.refs_0_, bf16[64,512]{1,0:T(8,128)(2,1)S(1)} %collective-permute-done.13.refs_1_, ...), custom_call_target="tpu_custom_call" | custom-call | tf_op jit(solution)/shard_map/experts/pallas_call | solution.py:34
  64.7 1.7 %collective-permute-done.16.got = bf16[2,72,1280]{2,1,0:T(8,128)(2,1)S(1)} collective-permute-done((bf16[2,72,1280]{2,1,0:T(8,128)(2,1)S(1)}, bf16[2,72,1280]{2,1,0:T(8,128)(2,1)S(1)}, u32[]{:S(2)}, u32[]{:S(2)}) %collective-permute-start.16) | collective-permute-done | bytes 368672 | tf_op jit(solution)/shard_map/ppermute | solution.py:46
  66.6 1.9 %collective-permute-start.17 = (bf16[2,72,640]{2,1,0:T(8,128)(2,1)S(1)}, bf16[2,72,640]{2,1,0:T(8,128)(2,1)S(1)}, u32[]{:S(2)}, u32[]{:S(2)}) collective-permute-start(bf16[2,72,640]{2,1,0:T(8,128)(2,1)S(1)} %get-tuple-element.49), channel_id=1, source_target_pairs={{0,2},{1,3},{2,0},{3,1},{4,6},{5,7},{6,4},{7,5},{8,10},{9,11},{10,... | collective-permute-start | bytes 552968 | tf_op jit(solution)/shard_map/ppermute | solution.py:46
  68.5 4.9 %collective-permute-done.17.got = bf16[2,72,640]{2,1,0:T(8,128)(2,1)S(1)} collective-permute-done((bf16[2,72,640]{2,1,0:T(8,128)(2,1)S(1)}, bf16[2,72,640]{2,1,0:T(8,128)(2,1)S(1)}, u32[]{:S(2)}, u32[]{:S(2)}) %collective-permute-start.17) | collective-permute-done | bytes 184352 | tf_op jit(solution)/shard_map/ppermute | solution.py:46
  73.5 1.7 %collective-permute-start.18 = (bf16[2,40,640]{2,1,0:T(8,128)(2,1)S(1)}, bf16[2,40,640]{2,1,0:T(8,128)(2,1)S(1)}, u32[]{:S(2)}, u32[]{:S(2)}) collective-permute-start(bf16[2,40,640]{2,1,0:T(8,128)(2,1)S(1)} %get-tuple-element.51), channel_id=1, source_target_pairs={{0,4},{1,5},{2,6},{3,7},{4,0},{5,1},{6,2},{7,3},{8,12},{9,13},{10,... | collective-permute-start | bytes 307208 | tf_op jit(solution)/shard_map/ppermute | solution.py:46
  75.2 5.6 %collective-permute-done.18.got = bf16[2,40,640]{2,1,0:T(8,128)(2,1)S(1)} collective-permute-done((bf16[2,40,640]{2,1,0:T(8,128)(2,1)S(1)}, bf16[2,40,640]{2,1,0:T(8,128)(2,1)S(1)}, u32[]{:S(2)}, u32[]{:S(2)}) %collective-permute-start.18) | collective-permute-done | bytes 102432 | tf_op jit(solution)/shard_map/ppermute | solution.py:46
  81.0 5.2 %collective-permute-done.19 = bf16[1,32,640]{2,1,0:T(8,128)(2,1)S(1)} collective-permute-done((bf16[1,32,640]{2,1,0:T(8,128)(2,1)S(1)}, bf16[1,32,640]{2,1,0:T(8,128)(2,1)S(1)}, u32[]{:S(2)}, u32[]{:S(2)}) %collective-permute-start.19) | collective-permute-done | bytes 40992 | tf_op jit(solution)/shard_map/ppermute | solution.py:46
  86.4 4.3 %collective-permute-done.20 = bf16[2,32,640]{2,1,0:T(8,128)(2,1)S(1)} collective-permute-done((bf16[2,32,640]{2,1,0:T(8,128)(2,1)S(1)}, bf16[2,32,640]{2,1,0:T(8,128)(2,1)S(1)}, u32[]{:S(2)}, u32[]{:S(2)}) %collective-permute-start.20) | collective-permute-done | bytes 81952 | tf_op jit(solution)/shard_map/ppermute | solution.py:46
  90.8 1.4 %collective-permute-done.21 = bf16[4,32,640]{2,1,0:T(8,128)(2,1)S(1)} collective-permute-done((bf16[4,32,640]{2,1,0:T(8,128)(2,1)S(1)}, bf16[4,32,640]{2,1,0:T(8,128)(2,1)S(1)}, u32[]{:S(2)}, u32[]{:S(2)}) %collective-permute-start.21) | collective-permute-done | bytes 163872 | tf_op jit(solution)/shard_map/ppermute | solution.py:46
  92.3 1.4 %down.1 = (f32[16,512]{1,0:T(8,128)S(1)}, bf16[16,512]{1,0:T(8,128)(2,1)S(1)}, bf16[16,512]{1,0:T(8,128)(2,1)S(1)}, bf16[16,512]{1,0:T(8,128)(2,1)S(1)}) custom-call(bf16[8,32,640]{2,1,0:T(8,128)(2,1)S(1)} %pad_maximum_fusion.acts, f32[8,64]{1,0:T(8,128)S(1)} %get-tuple-element.54.stats, f32[64,128]{1,0:T(8,128)S(1)} %get-tuple-element.55.info, ...), custom_call_target="tpu_custom_call" | custom-call | tf_op jit(solution)/shard_map/down/pallas_call | solution.py:34
  93.7 2.0 %collective-permute-start.22 = (bf16[16,512]{1,0:T(8,128)(2,1)S(1)}, bf16[16,512]{1,0:T(8,128)(2,1)S(1)}, u32[]{:S(2)}, u32[]{:S(2)}) collective-permute-start(bf16[16,512]{1,0:T(8,128)(2,1)S(1)} %get-tuple-element.58), channel_id=1, source_target_pairs={{0,8},{8,0},{16,24},{24,16},{1,9},{9,1},{17,25},{25,17},{2,10},{10... | collective-permute-start | bytes 49160 | tf_op jit(solution)/shard_map/ppermute | solution.py:46
  95.7 0.8 collective-permute-start.23
  96.5 1.0 collective-permute-start.24
  97.5 2.0 %collective-permute-done.23.refs_2_ = bf16[16,512]{1,0:T(8,128)(2,1)S(1)} collective-permute-done((bf16[16,512]{1,0:T(8,128)(2,1)S(1)}, bf16[16,512]{1,0:T(8,128)(2,1)S(1)}, u32[]{:S(2)}, u32[]{:S(2)}) %collective-permute-start.23) | collective-permute-done | bytes 16416 | tf_op jit(solution)/shard_map/ppermute | solution.py:46
  99.5 1.7 %collective-permute-done.24.refs_3_ = bf16[16,512]{1,0:T(8,128)(2,1)S(1)} collective-permute-done((bf16[16,512]{1,0:T(8,128)(2,1)S(1)}, bf16[16,512]{1,0:T(8,128)(2,1)S(1)}, u32[]{:S(2)}, u32[]{:S(2)}) %collective-permute-start.24) | collective-permute-done | bytes 16416 | tf_op jit(solution)/shard_map/ppermute | solution.py:46
  101.3 1.2 %collective-permute-done.25 = f32[8,128]{1,0:T(8,128)S(1)} collective-permute-done((f32[8,128]{1,0:T(8,128)S(1)}, f32[8,128]{1,0:T(8,128)S(1)}, u32[]{:S(2)}, u32[]{:S(2)}) %collective-permute-start.25) | collective-permute-done | bytes 4128 | tf_op jit(solution)/shard_map/ppermute | solution.py:46
  102.5 0.6 collective-permute-start.26
  103.0 3.0 %collective-permute-done.26 = f32[8,128]{1,0:T(8,128)S(1)} collective-permute-done((f32[8,128]{1,0:T(8,128)S(1)}, f32[8,128]{1,0:T(8,128)S(1)}, u32[]{:S(2)}, u32[]{:S(2)}) %collective-permute-start.26) | collective-permute-done | bytes 4128 | tf_op jit(solution)/shard_map/ppermute | solution.py:46
  106.1 1.5 %collective-permute-start.27 = (f32[8,128]{1,0:T(8,128)S(1)}, f32[8,128]{1,0:T(8,128)S(1)}, u32[]{:S(2)}, u32[]{:S(2)}) collective-permute-start(f32[8,128]{1,0:T(8,128)S(1)} %add.7.refs_2_), channel_id=1, source_target_pairs={{0,4},{1,5},{2,6},{3,7},{4,0},{5,1},{6,2},{7,3},{8,12},{9,13},{10,... | collective-permute-start | bytes 12296 | tf_op jit(solution)/shard_map/ppermute | solution.py:46
  107.6 3.0 %collective-permute-done.27.refs_3_ = f32[8,128]{1,0:T(8,128)S(1)} collective-permute-done((f32[8,128]{1,0:T(8,128)S(1)}, f32[8,128]{1,0:T(8,128)S(1)}, u32[]{:S(2)}, u32[]{:S(2)}) %collective-permute-start.27) | collective-permute-done | bytes 4128 | tf_op jit(solution)/shard_map/ppermute | solution.py:46
  110.6 0.7 norm.1
  (58 shorter events, 1.7 us)
Async XLA Ops:
  0.0 0.9 copy-start.11
  0.9 0.7 copy-start.13
  1.6 0.7 copy-start.15
  2.2 0.7 copy-start.16
  2.9 0.7 copy-start.19
  4.3 5.0 %collective-permute-start = (bf16[16,1152]{1,0:T(8,128)(2,1)S(1)}, bf16[16,1152]{1,0:T(8,128)(2,1)S(1)}, u32[]{:S(2)}, u32[]{:S(2)}) collective-permute-start(bf16[16,1152]{1,0:T(8,128)(2,1)S(1)} %get-tuple-element.35), channel_id=1, source_target_pairs={{0,8},{8,0},{16,24},{24,16},{1,9},{9,1},{17,25},{25,17},{2,10},{10... | collective-permute-start | bytes 110600 | tf_op jit(solution)/shard_map/ppermute | solution.py:46
  7.3 4.0 %collective-permute-start.1 = (bf16[16,1152]{1,0:T(8,128)(2,1)S(1)}, bf16[16,1152]{1,0:T(8,128)(2,1)S(1)}, u32[]{:S(2)}, u32[]{:S(2)}) collective-permute-start(bf16[16,1152]{1,0:T(8,128)(2,1)S(1)} %get-tuple-element.36), channel_id=1, source_target_pairs={{0,16},{8,24},{16,0},{24,8},{1,17},{9,25},{17,1},{25,9},{2,18},{10... | collective-permute-start | bytes 110600 | tf_op jit(solution)/shard_map/ppermute | solution.py:46
  8.8 4.9 %collective-permute-start.2 = (bf16[16,1152]{1,0:T(8,128)(2,1)S(1)}, bf16[16,1152]{1,0:T(8,128)(2,1)S(1)}, u32[]{:S(2)}, u32[]{:S(2)}) collective-permute-start(bf16[16,1152]{1,0:T(8,128)(2,1)S(1)} %get-tuple-element.37), channel_id=1, source_target_pairs={{0,24},{8,16},{16,8},{24,0},{1,25},{9,17},{17,9},{25,1},{2,26},{10... | collective-permute-start | bytes 110600 | tf_op jit(solution)/shard_map/ppermute | solution.py:46
  13.7 1.2 %copy-start.4 = (bf16[1024,512]{1,0:T(8,128)(2,1)S(1)}, bf16[1024,512]{1,0:T(8,128)(2,1)}, u32[]{:S(2)}) copy-start(bf16[1024,512]{1,0:T(8,128)(2,1)} %refs_4_.2) | copy-start | bytes 3145732
  14.9 1.0 copy-start.6
  16.0 1.0 copy-start.7
  17.0 25.6 %copy-start.5 = (bf16[512,1024]{1,0:T(8,128)(2,1)S(1)}, bf16[512,1024]{1,0:T(8,128)(2,1)}, u32[]{:S(2)}) copy-start(bf16[512,1024]{1,0:T(8,128)(2,1)} %refs_4_.3) | copy-start | bytes 3145732
  17.5 4.0 %collective-permute-start.3 = (bf16[16,1024]{1,0:T(8,128)(2,1)S(1)}, bf16[16,1024]{1,0:T(8,128)(2,1)S(1)}, u32[]{:S(2)}, u32[]{:S(2)}) collective-permute-start(bf16[16,1024]{1,0:T(8,128)(2,1)S(1)} %get-tuple-element.39), channel_id=1, source_target_pairs={{0,8},{8,0},{16,24},{24,16},{1,9},{9,1},{17,25},{25,17},{2,10},{10... | collective-permute-start | bytes 98312 | tf_op jit(solution)/shard_map/ppermute | solution.py:46
  18.1 3.9 %collective-permute-start.4 = (bf16[16,1024]{1,0:T(8,128)(2,1)S(1)}, bf16[16,1024]{1,0:T(8,128)(2,1)S(1)}, u32[]{:S(2)}, u32[]{:S(2)}) collective-permute-start(bf16[16,1024]{1,0:T(8,128)(2,1)S(1)} %get-tuple-element.40), channel_id=1, source_target_pairs={{0,16},{8,24},{16,0},{24,8},{1,17},{9,25},{17,1},{25,9},{2,18},{10... | collective-permute-start | bytes 98312 | tf_op jit(solution)/shard_map/ppermute | solution.py:46
  18.1 4.8 %collective-permute-start.5 = (bf16[16,1024]{1,0:T(8,128)(2,1)S(1)}, bf16[16,1024]{1,0:T(8,128)(2,1)S(1)}, u32[]{:S(2)}, u32[]{:S(2)}) collective-permute-start(bf16[16,1024]{1,0:T(8,128)(2,1)S(1)} %get-tuple-element.41), channel_id=1, source_target_pairs={{0,24},{8,16},{16,8},{24,0},{1,25},{9,17},{17,9},{25,1},{2,26},{10... | collective-permute-start | bytes 98312 | tf_op jit(solution)/shard_map/ppermute | solution.py:46
  22.9 3.4 %copy-start = (bf16[16,1024,2,128]{3,2,1,0:T(2,128)(2,1)S(1)}, bf16[16,1024,2,128]{3,2,1,0:T(2,128)(2,1)}, u32[]{:S(2)}) copy-start(bf16[16,1024,2,128]{3,2,1,0:T(2,128)(2,1)} %param.29) | copy-start | bytes 25165828
  26.3 3.4 %copy-start.1 = (bf16[16,1024,2,128]{3,2,1,0:T(2,128)(2,1)S(1)}, bf16[16,1024,2,128]{3,2,1,0:T(2,128)(2,1)}, u32[]{:S(2)}) copy-start(bf16[16,1024,2,128]{3,2,1,0:T(2,128)(2,1)} %param.30) | copy-start | bytes 25165828
  29.7 0.7 copy-start.17
  30.4 0.7 copy-start.18
  31.0 28.0 %copy-start.20 = (bf16[4096]{0:T(1024)(128)(2,1)S(1)}, bf16[4096]{0:T(1024)(128)(2,1)}, u32[]{:S(2)}) copy-start(bf16[4096]{0:T(1024)(128)(2,1)} %param.42) | copy-start | bytes 24580
  31.0 29.9 %copy-start.2 = (bf16[4,512,2048]{2,1,0:T(8,128)(2,1)S(1)}, bf16[4,512,2048]{2,1,0:T(8,128)(2,1)}, u32[]{:S(2)}) copy-start(bf16[4,512,2048]{2,1,0:T(8,128)(2,1)} %refs_10_.1) | copy-start | bytes 25165828
  31.0 29.9 %copy-start.3 = (bf16[4,512,2048]{2,1,0:T(8,128)(2,1)S(1)}, bf16[4,512,2048]{2,1,0:T(8,128)(2,1)}, u32[]{:S(2)}) copy-start(bf16[4,512,2048]{2,1,0:T(8,128)(2,1)} %refs_11_.1) | copy-start | bytes 25165828
  31.0 29.9 %copy-start.9 = (bf16[512,512]{1,0:T(8,128)(2,1)S(1)}, bf16[512,512]{1,0:T(8,128)(2,1)}, u32[]{:S(2)}) copy-start(bf16[512,512]{1,0:T(8,128)(2,1)} %refs_12_.1) | copy-start | bytes 1572868
  31.0 29.9 %copy-start.10 = (bf16[512,512]{1,0:T(8,128)(2,1)S(1)}, bf16[512,512]{1,0:T(8,128)(2,1)}, u32[]{:S(2)}) copy-start(bf16[512,512]{1,0:T(8,128)(2,1)} %refs_13_.1) | copy-start | bytes 1572868
  31.0 29.9 %copy-start.12 = (f32[4096]{0:T(1024)S(1)}, f32[4096]{0:T(1024)}, u32[]{:S(2)}) copy-start(f32[4096]{0:T(1024)} %param.32) | copy-start | bytes 49156
  35.4 4.7 %collective-permute-start.8 = (bf16[16,512]{1,0:T(8,128)(2,1)S(1)}, bf16[16,512]{1,0:T(8,128)(2,1)S(1)}, u32[]{:S(2)}, u32[]{:S(2)}) collective-permute-start(bf16[16,512]{1,0:T(8,128)(2,1)S(1)} %attend.1.refs_0_), channel_id=1, source_target_pairs={{0,24},{8,16},{16,8},{24,0},{1,25},{9,17},{17,9},{25,1},{2,26},{10... | collective-permute-start | bytes 49160 | tf_op jit(solution)/shard_map/ppermute | solution.py:46
  38.4 3.7 %collective-permute-start.7 = (bf16[16,512]{1,0:T(8,128)(2,1)S(1)}, bf16[16,512]{1,0:T(8,128)(2,1)S(1)}, u32[]{:S(2)}, u32[]{:S(2)}) collective-permute-start(bf16[16,512]{1,0:T(8,128)(2,1)S(1)} %attend.1.refs_0_), channel_id=1, source_target_pairs={{0,16},{8,24},{16,0},{24,8},{1,17},{9,25},{17,1},{25,9},{2,18},{10... | collective-permute-start | bytes 49160 | tf_op jit(solution)/shard_map/ppermute | solution.py:46
  38.9 3.7 %collective-permute-start.6 = (bf16[16,512]{1,0:T(8,128)(2,1)S(1)}, bf16[16,512]{1,0:T(8,128)(2,1)S(1)}, u32[]{:S(2)}, u32[]{:S(2)}) collective-permute-start(bf16[16,512]{1,0:T(8,128)(2,1)S(1)} %attend.1.refs_0_), channel_id=1, source_target_pairs={{0,8},{8,0},{16,24},{24,16},{1,9},{9,1},{17,25},{25,17},{2,10},{10... | collective-permute-start | bytes 49160 | tf_op jit(solution)/shard_map/ppermute | solution.py:46
  43.0 1.3 %collective-permute-start.9 = (bf16[64,512]{1,0:T(8,128)(2,1)S(1)}, bf16[64,512]{1,0:T(8,128)(2,1)S(1)}, u32[]{:S(2)}, u32[]{:S(2)}) collective-permute-start(bf16[64,512]{1,0:T(8,128)(2,1)S(1)} %get-tuple-element.45), channel_id=1, source_target_pairs={{0,1},{1,0},{2,3},{3,2},{4,5},{5,4},{6,7},{7,6},{8,9},{9,8},{10,11... | collective-permute-start | bytes 196616 | tf_op jit(solution)/shard_map/ppermute | solution.py:46
  44.3 8.0 %collective-permute-start.12 = (bf16[64,512]{1,0:T(8,128)(2,1)S(1)}, bf16[64,512]{1,0:T(8,128)(2,1)S(1)}, u32[]{:S(2)}, u32[]{:S(2)}) collective-permute-start(bf16[64,512]{1,0:T(8,128)(2,1)S(1)} %pairsum.1.refs_0_), channel_id=1, source_target_pairs={{6,0},{7,1},{12,10},{13,11},{18,20},{19,21},{24,30},{25,31}} | collective-permute-start | bytes 196616 | tf_op jit(solution)/shard_map/ppermute | solution.py:653
  45.6 8.1 %collective-permute-start.11 = (bf16[64,512]{1,0:T(8,128)(2,1)S(1)}, bf16[64,512]{1,0:T(8,128)(2,1)S(1)}, u32[]{:S(2)}, u32[]{:S(2)}) collective-permute-start(bf16[64,512]{1,0:T(8,128)(2,1)S(1)} %pairsum.1.refs_0_), channel_id=1, source_target_pairs={{4,0},{5,1},{14,10},{15,11},{16,20},{17,21},{26,30},{27,31}} | collective-permute-start | bytes 196616 | tf_op jit(solution)/shard_map/ppermute | solution.py:653
  46.9 8.1 %collective-permute-start.10 = (bf16[64,512]{1,0:T(8,128)(2,1)S(1)}, bf16[64,512]{1,0:T(8,128)(2,1)S(1)}, u32[]{:S(2)}, u32[]{:S(2)}) collective-permute-start(bf16[64,512]{1,0:T(8,128)(2,1)S(1)} %pairsum.1.refs_0_), channel_id=1, source_target_pairs={{2,0},{3,1},{8,10},{9,11},{22,20},{23,21},{28,30},{29,31}} | collective-permute-start | bytes 196616 | tf_op jit(solution)/shard_map/ppermute | solution.py:653
  55.1 3.9 %collective-permute-start.15 = (bf16[64,512]{1,0:T(8,128)(2,1)S(1)}, bf16[64,512]{1,0:T(8,128)(2,1)S(1)}, u32[]{:S(2)}, u32[]{:S(2)}) collective-permute-start(bf16[64,512]{1,0:T(8,128)(2,1)S(1)} %residual.1.refs_0_), channel_id=1, source_target_pairs={{0,24},{1,25},{10,18},{11,19},{20,12},{21,13},{30,6},{31,7}} | collective-permute-start | bytes 196616 | tf_op jit(solution)/shard_map/ppermute | solution.py:665
  56.4 3.2 %collective-permute-start.14 = (bf16[64,512]{1,0:T(8,128)(2,1)S(1)}, bf16[64,512]{1,0:T(8,128)(2,1)S(1)}, u32[]{:S(2)}, u32[]{:S(2)}) collective-permute-start(bf16[64,512]{1,0:T(8,128)(2,1)S(1)} %residual.1.refs_0_), channel_id=1, source_target_pairs={{0,16},{1,17},{10,26},{11,27},{20,4},{21,5},{30,14},{31,15}} | collective-permute-start | bytes 196616 | tf_op jit(solution)/shard_map/ppermute | solution.py:665
  57.7 3.2 %collective-permute-start.13 = (bf16[64,512]{1,0:T(8,128)(2,1)S(1)}, bf16[64,512]{1,0:T(8,128)(2,1)S(1)}, u32[]{:S(2)}, u32[]{:S(2)}) collective-permute-start(bf16[64,512]{1,0:T(8,128)(2,1)S(1)} %residual.1.refs_0_), channel_id=1, source_target_pairs={{0,8},{1,9},{10,2},{11,3},{20,28},{21,29},{30,22},{31,23}} | collective-permute-start | bytes 196616 | tf_op jit(solution)/shard_map/ppermute | solution.py:665
  60.9 31.3 %slice-start = ((s8[8388608]{0:T(1024)(128)(4,1)}), s8[4194304]{0:T(1024)(128)(4,1)S(1)}, s32[]{:S(2)}) async-start(s8[8388608]{0:T(1024)(128)(4,1)} %bitcast.9), calls=%async_computation | async-start | bytes 8388608
  61.0 31.3 %slice-start.1 = ((s8[8388608]{0:T(1024)(128)(4,1)}), s8[4194304]{0:T(1024)(128)(4,1)S(1)}, s32[]{:S(2)}) async-start(s8[8388608]{0:T(1024)(128)(4,1)} %bitcast.9), calls=%async_computation.1 | async-start | bytes 8388608
  61.0 31.3 %copy-start.8 = (bf16[512,512]{1,0:T(8,128)(2,1)S(1)}, bf16[512,512]{1,0:T(8,128)(2,1)}, u32[]{:S(2)}) copy-start(bf16[512,512]{1,0:T(8,128)(2,1)} %dense_down.1) | copy-start | bytes 1572868
  64.6 46.0 %copy-start.14 = (f32[512]{0:T(512)S(1)}, f32[512]{0:T(512)}, u32[]{:S(2)}) copy-start(f32[512]{0:T(512)} %param.33) | copy-start | bytes 6148
  64.6 1.8 %collective-permute-start.16 = (bf16[2,72,1280]{2,1,0:T(8,128)(2,1)S(1)}, bf16[2,72,1280]{2,1,0:T(8,128)(2,1)S(1)}, u32[]{:S(2)}, u32[]{:S(2)}) collective-permute-start(bf16[2,72,1280]{2,1,0:T(8,128)(2,1)S(1)} %get-tuple-element.47), channel_id=1, source_target_pairs={{0,1},{1,0},{2,3},{3,2},{4,5},{5,4},{6,7},{7,6},{8,9},{9,8},{10,11... | collective-permute-start | bytes 1105928 | tf_op jit(solution)/shard_map/ppermute | solution.py:46
  66.6 6.8 %collective-permute-start.17 = (bf16[2,72,640]{2,1,0:T(8,128)(2,1)S(1)}, bf16[2,72,640]{2,1,0:T(8,128)(2,1)S(1)}, u32[]{:S(2)}, u32[]{:S(2)}) collective-permute-start(bf16[2,72,640]{2,1,0:T(8,128)(2,1)S(1)} %get-tuple-element.49), channel_id=1, source_target_pairs={{0,2},{1,3},{2,0},{3,1},{4,6},{5,7},{6,4},{7,5},{8,10},{9,11},{10,... | collective-permute-start | bytes 552968 | tf_op jit(solution)/shard_map/ppermute | solution.py:46
  73.5 7.3 %collective-permute-start.18 = (bf16[2,40,640]{2,1,0:T(8,128)(2,1)S(1)}, bf16[2,40,640]{2,1,0:T(8,128)(2,1)S(1)}, u32[]{:S(2)}, u32[]{:S(2)}) collective-permute-start(bf16[2,40,640]{2,1,0:T(8,128)(2,1)S(1)} %get-tuple-element.51), channel_id=1, source_target_pairs={{0,4},{1,5},{2,6},{3,7},{4,0},{5,1},{6,2},{7,3},{8,12},{9,13},{10,... | collective-permute-start | bytes 307208 | tf_op jit(solution)/shard_map/ppermute | solution.py:46
  80.9 5.2 %collective-permute-start.19 = (bf16[1,32,640]{2,1,0:T(8,128)(2,1)S(1)}, bf16[1,32,640]{2,1,0:T(8,128)(2,1)S(1)}, u32[]{:S(2)}, u32[]{:S(2)}) collective-permute-start(bf16[1,32,640]{2,1,0:T(8,128)(2,1)S(1)} %get-tuple-element.53), channel_id=1, source_target_pairs={{0,4},{1,5},{2,6},{3,7},{4,0},{5,1},{6,2},{7,3},{8,12},{9,13},{10,... | collective-permute-start | bytes 122888 | tf_op jit(solution)/shard_map/ppermute | solution.py:46
  86.2 4.5 %collective-permute-start.20 = (bf16[2,32,640]{2,1,0:T(8,128)(2,1)S(1)}, bf16[2,32,640]{2,1,0:T(8,128)(2,1)S(1)}, u32[]{:S(2)}, u32[]{:S(2)}) collective-permute-start(bf16[2,32,640]{2,1,0:T(8,128)(2,1)S(1)} %pad_maximum_fusion.2), channel_id=1, source_target_pairs={{0,2},{1,3},{2,0},{3,1},{4,6},{5,7},{6,4},{7,5},{8,10},{9,11},{10,... | collective-permute-start | bytes 245768 | tf_op jit(solution)/shard_map/ppermute | solution.py:46
  90.7 1.5 %collective-permute-start.21 = (bf16[4,32,640]{2,1,0:T(8,128)(2,1)S(1)}, bf16[4,32,640]{2,1,0:T(8,128)(2,1)S(1)}, u32[]{:S(2)}, u32[]{:S(2)}) collective-permute-start(bf16[4,32,640]{2,1,0:T(8,128)(2,1)S(1)} %pad_maximum_fusion.1), channel_id=1, source_target_pairs={{0,1},{1,0},{2,3},{3,2},{4,5},{5,4},{6,7},{7,6},{8,9},{9,8},{10,11... | collective-permute-start | bytes 491528 | tf_op jit(solution)/shard_map/ppermute | solution.py:46
  93.7 3.8 %collective-permute-start.22 = (bf16[16,512]{1,0:T(8,128)(2,1)S(1)}, bf16[16,512]{1,0:T(8,128)(2,1)S(1)}, u32[]{:S(2)}, u32[]{:S(2)}) collective-permute-start(bf16[16,512]{1,0:T(8,128)(2,1)S(1)} %get-tuple-element.58), channel_id=1, source_target_pairs={{0,8},{8,0},{16,24},{24,16},{1,9},{9,1},{17,25},{25,17},{2,10},{10... | collective-permute-start | bytes 49160 | tf_op jit(solution)/shard_map/ppermute | solution.py:46
  95.7 3.7 %collective-permute-start.23 = (bf16[16,512]{1,0:T(8,128)(2,1)S(1)}, bf16[16,512]{1,0:T(8,128)(2,1)S(1)}, u32[]{:S(2)}, u32[]{:S(2)}) collective-permute-start(bf16[16,512]{1,0:T(8,128)(2,1)S(1)} %get-tuple-element.59), channel_id=1, source_target_pairs={{0,16},{8,24},{16,0},{24,8},{1,17},{9,25},{17,1},{25,9},{2,18},{10... | collective-permute-start | bytes 49160 | tf_op jit(solution)/shard_map/ppermute | solution.py:46
  96.5 4.6 %collective-permute-start.24 = (bf16[16,512]{1,0:T(8,128)(2,1)S(1)}, bf16[16,512]{1,0:T(8,128)(2,1)S(1)}, u32[]{:S(2)}, u32[]{:S(2)}) collective-permute-start(bf16[16,512]{1,0:T(8,128)(2,1)S(1)} %get-tuple-element.60), channel_id=1, source_target_pairs={{0,24},{8,16},{16,8},{24,0},{1,25},{9,17},{17,9},{25,1},{2,26},{10... | collective-permute-start | bytes 49160 | tf_op jit(solution)/shard_map/ppermute | solution.py:46
  101.2 1.2 %collective-permute-start.25 = (f32[8,128]{1,0:T(8,128)S(1)}, f32[8,128]{1,0:T(8,128)S(1)}, u32[]{:S(2)}, u32[]{:S(2)}) collective-permute-start(f32[8,128]{1,0:T(8,128)S(1)} %get-tuple-element.62), channel_id=1, source_target_pairs={{0,1},{1,0},{2,3},{3,2},{4,5},{5,4},{6,7},{7,6},{8,9},{9,8},{10,11... | collective-permute-start | bytes 12296 | tf_op jit(solution)/shard_map/ppermute | solution.py:46
  102.5 3.6 %collective-permute-start.26 = (f32[8,128]{1,0:T(8,128)S(1)}, f32[8,128]{1,0:T(8,128)S(1)}, u32[]{:S(2)}, u32[]{:S(2)}) collective-permute-start(f32[8,128]{1,0:T(8,128)S(1)} %add.6), channel_id=1, source_target_pairs={{0,2},{1,3},{2,0},{3,1},{4,6},{5,7},{6,4},{7,5},{8,10},{9,11},{10,... | collective-permute-start | bytes 12296 | tf_op jit(solution)/shard_map/ppermute | solution.py:46
  106.1 4.5 %collective-permute-start.27 = (f32[8,128]{1,0:T(8,128)S(1)}, f32[8,128]{1,0:T(8,128)S(1)}, u32[]{:S(2)}, u32[]{:S(2)}) collective-permute-start(f32[8,128]{1,0:T(8,128)S(1)} %add.7.refs_2_), channel_id=1, source_target_pairs={{0,4},{1,5},{2,6},{3,7},{4,0},{5,1},{6,2},{7,3},{8,12},{9,13},{10,... | collective-permute-start | bytes 12296 | tf_op jit(solution)/shard_map/ppermute | solution.py:46

commit v3 on v2

--- a/solution.py
+++ b/solution.py
@@ -1,8 +1,8 @@
 import functools
+import math
 
 import jax
 import jax.numpy as jnp
-import numpy as np
 from jax import lax
 from jax.experimental import pallas as pl
 from jax.experimental.pallas import tpu as pltpu
@@ -26,11 +26,13 @@
 F32 = jnp.float32
 BF16 = jnp.bfloat16
 
+OVERLAP = 20_000_000_000
+
 IN_VMEM = pl.BlockSpec(memory_space=pltpu.VMEM)
 IN_SMEM = pl.BlockSpec(memory_space=pltpu.SMEM)
 
 
-def call(kernel, name, outs, args, scalars=0, scratch=(), mib=4, **sizes):
+def call(kernel, name, outs, args, scalars=0, scratch=(), mib=4, cost=0, **sizes):
     return pl.pallas_call(
         functools.partial(kernel, **sizes),
         out_shape=[jax.ShapeDtypeStruct(shape, dtype) for shape, dtype in outs],
@@ -38,6 +40,7 @@
         out_specs=[IN_VMEM] * len(outs),
         scratch_shapes=[pltpu.VMEM(shape, dtype) for shape, dtype in scratch],
         compiler_params=pltpu.CompilerParams(vmem_limit_bytes=mib * 1024 * 1024),
+        cost_estimate=pl.CostEstimate(flops=cost, bytes_accessed=cost, transcendentals=0) if cost else None,
         name=name,
     )(*args)
 
@@ -48,6 +51,14 @@
 
 def xor_all(arrays, axis, count):
     return [xor_permute(arrays[d - 1], axis, count, d) for d in range(1, count)]
+
+
+def places_all(arrays, tp_count):
+    got = {}
+    order = sorted(range(1, tp_count // 2), key=lambda d: (d != 1, -d))
+    for d in order:
+        got[d] = xor_permute(arrays[d - 1], "tp", tp_count, 2 * d)
+    return [got[d] for d in range(1, tp_count // 2)]
 
 
 def aligned(index, size):
@@ -83,7 +94,7 @@
 MEAN_LANE = WEIGHT_LANE + 3 * TOPK
 
 
-def prepare_kernel(lengths, tokens, ids, weights, frequency, *outs, ep_count):
+def prepare_kernel(tokens, ids, weights, *outs, ep_count):
     seq_count, width = tokens.shape
     block = width // ep_count
     ep = lax.axis_index("ep")
@@ -104,15 +115,21 @@
     for d in range(ep_count):
         outs[d][:, :block] = tokens[:, aligned(ep ^ d, block)]
         outs[d][:, block:] = extra
+
+
+def tables_kernel(lengths, cos_ref, sin_ref):
+    seq_count = cos_ref.shape[0]
+    lane = iota((seq_count, LANES), 1)
     row = iota((seq_count, LANES), 0)
     position = jnp.zeros((seq_count, LANES), F32)
     for s in range(seq_count):
         position = jnp.where(row == s, lengths[s].astype(F32), position)
-    angle = position * frequency[...]
+    rate = (lane % (SUB // 2)).astype(F32) * (-2.0 / SUB * math.log(theta_base))
+    angle = position * jnp.exp(rate)
     low_half = (lane % SUB) < (SUB // 2)
     sine = jnp.sin(angle)
-    outs[ep_count][...] = jnp.cos(angle)
-    outs[ep_count + 1][...] = jnp.where(low_half, -sine, sine)
+    cos_ref[...] = jnp.cos(angle)
+    sin_ref[...] = jnp.where(low_half, -sine, sine)
 
 
 def project_kernel(*refs, ep_count):
@@ -396,30 +413,45 @@
     kept[...] = full[:, :, aligned(side, half)]
 
 
-def columns_kernel(kept_in, got, sent, kept, full, *, bit):
-    full[...] = kept_in[...] + got[...].astype(F32)
-    half = full.shape[2] // 2
-    side = (lax.axis_index("tp") >> bit) & 1
-    send_part(sent, full[:, :, aligned(1 - side, half)])
-    kept[...] = full[:, :, aligned(side, half)]
-
-
-def rows_kernel(kept_in, got, sent, kept, full, *, bit):
-    full[...] = kept_in[...] + got[...].astype(F32)
-    half = (full.shape[1] - TAIL) // 2
-    side = (lax.axis_index("tp") >> bit) & 1
-    tail = full[:, 2 * half :, :]
-    other = full[:, pl.ds(pl.multiple_of((1 - side) * half, 8), half), :]
-    send_part(sent, jnp.concatenate([other, tail], axis=1))
-    kept[:, :half, :] = full[:, pl.ds(pl.multiple_of(side * half, 8), half), :]
-    kept[:, half:, :] = tail
+def piece_at(index, bits, rows, width):
+    row, column = 0, 0
+    for bit, splits_columns in enumerate(bits):
+        up = (index >> bit) & 1
+        if splits_columns:
+            width //= 2
+            column = column + up * width
+        else:
+            rows //= 2
+            row = row + up * rows
+    return row, column
+
+
+def spread_kernel(kept, got, *refs, bits):
+    outs, full = refs[:-1], refs[-1]
+    full[...] = kept[...] + got[...].astype(F32)
+    rows = full.shape[1] - TAIL
+    piece_rows = outs[0].shape[1] - TAIL
+    width = outs[0].shape[2]
+    place = lax.axis_index("tp") >> 1
+    for d, out in enumerate(outs):
+        row, column = piece_at(place ^ d, bits, rows, full.shape[2])
+        lanes = pl.ds(pl.multiple_of(column, LANES), width)
+        main = full[:, pl.ds(pl.multiple_of(row, 8), piece_rows), lanes]
+        tail = full[:, rows:, lanes]
+        if d == 0:
+            out[:, :piece_rows, :] = main
+            out[:, piece_rows:, :] = tail
+        else:
+            send_part(out, jnp.concatenate([main, tail], axis=1))
 
 
 def act_kernel(
-    kept, got, placed, act, stats, *, model_width, expert_width, dense_width, expert_rows, bits
+    *refs, model_width, expert_width, dense_width, expert_rows, bits
 ):
-    column_bits, row_bits = bits
-    total = kept[...] + got[...].astype(F32)
+    placed, act, stats = refs[-3:]
+    total = refs[0][...]
+    for ref in refs[1:-3]:
+        total = total + ref[...].astype(F32)
     rows = total.shape[1] - TAIL
     width = total.shape[2]
     slot_count, total_rows = placed.shape
@@ -433,16 +465,9 @@
     stats[0:1, :] = mean
     stats[1:2, :] = scale
     stats[2:3, :] = gate
-    first_row = 0
-    size = slot_count
-    for bit in row_bits:
-        size //= 2
-        first_row = first_row + ((tp >> bit) & 1) * size
-    first_column = 0
-    size = expert_width + dense_width * (total_rows // slot_count)
-    for bit in column_bits:
-        size //= 2
-        first_column = first_column + ((tp >> bit) & 1) * size
+    whole = expert_width + dense_width * (total_rows // slot_count)
+    first_row, first_column = piece_at(tp >> 1, bits, slot_count, whole // 2)
+    first_column = first_column + (tp & 1) * (whole // 2)
     mine = placed[pl.ds(pl.multiple_of(first_row, 8), rows), :]
     scale_used = jnp.sum(mine * scale, axis=1, keepdims=True)
     mean_used = jnp.sum(mine * mean, axis=1, keepdims=True)
@@ -480,7 +505,7 @@
     tp = lax.axis_index("tp")
     piece_rows, piece_width = acts.shape[1:]
     for index, (row, column) in enumerate(places):
-        block = acts[index ^ reverse_bits(tp, len(places))]
+        block = acts[index ^ ((tp & 1) * (len(places) // 2) + (tp >> 1))]
         joined[row : row + piece_rows, column : column + piece_width] = block
     local_experts, expert_width, size = expert_down.shape
     dense_width = dense_down.shape[0]
@@ -515,14 +540,6 @@
     outs[0][...] = mixed[:seq_count] + residual_scale * hidden
     for d in range(1, ep_count):
         outs[d][...] = mixed[d * seq_count : (d + 1) * seq_count].astype(BF16)
-
-
-def reverse_bits(index, count):
-    steps = count.bit_length() - 1
-    total = 0
-    for step in range(steps):
-        total = total + (((index >> step) & 1) << (steps - 1 - step))
-    return total
 
 
 def combine_kernel(*refs):
@@ -587,18 +604,20 @@
     heads = head_lambda.shape[0]
     cache, kv_local = key_cache.shape[1:3]
 
-    frequency = theta_base ** (-(np.arange(SUB // 2, dtype=np.float64) * (2.0 / SUB)))
-    frequency = np.tile(frequency, LANES // (SUB // 2)).astype(np.float32)[None, :]
     piece = ((seq_count, block_width + LANES), BF16)
     table = ((seq_count, LANES), F32)
-    *pieces, cosine, sine = call(
+    pieces = call(
         prepare_kernel,
         "prepare",
-        [piece] * ep_count + [table] * 2,
-        [lengths, tokens, expert_ids.T, route_weights.T, jnp.asarray(frequency)],
-        scalars=1,
+        [piece] * ep_count,
+        [
+            pltpu.with_memory_space_constraint(array, pltpu.HBM)
+            for array in (tokens, expert_ids.T, route_weights.T)
+        ],
+        cost=OVERLAP,
         ep_count=ep_count,
     )
+    cosine, sine = call(tables_kernel, "tables", [table] * 2, [lengths], scalars=1)
     pieces = [pieces[0]] + xor_all(pieces[1:], "ep", ep_count)
     qkv_width = (heads + 2 * kv_local) * LANES
     sums = call(
@@ -625,6 +644,7 @@
         ],
         scalars=2,
         scratch=[rows_scratch] * 4,
+        cost=OVERLAP,
         ep_count=ep_count,
         group=min(8, seq_count),
     )
@@ -667,15 +687,16 @@
     ]
 
     width = expert_width + dense_width * (total_rows // slot_count)
-    column_bits, row_bits = [], []
-    piece_width, piece_rows = width, slot_count
-    for bit in range(tp_count.bit_length() - 1):
-        if piece_width % (2 * LANES) == 0 and not row_bits:
-            column_bits.append(bit)
+    place_count = tp_count // 2
+    bits = []
+    piece_width, piece_rows = width // 2, slot_count
+    for _ in range(place_count.bit_length() - 1):
+        bits.append(piece_width % (2 * LANES) == 0)
+        if bits[-1]:
             piece_width //= 2
         else:
-            row_bits.append(bit)
             piece_rows //= 2
+    bits = tuple(bits)
     full_rows = slot_count + TAIL
     half = (2, full_rows, width // 2)
     sent, kept, placed, info, own_rows = call(
@@ -705,51 +726,34 @@
         ratio=ratio,
         width=piece_width,
     )
-    shape = list(half)
-    for bit in range(1, tp_count.bit_length() - 1):
-        got = xor_permute(sent, "tp", tp_count, 1 << (bit - 1))
-        before = tuple(shape)
-        if bit in column_bits:
-            shape[2] //= 2
-        else:
-            shape[1] = (shape[1] - TAIL) // 2 + TAIL
-        sent, kept = call(
-            columns_kernel if bit in column_bits else rows_kernel,
-            "fold%d" % bit,
-            [(tuple(shape), BF16), (tuple(shape), F32)],
-            [kept, got],
-            scratch=[(before, F32)],
-            bit=bit,
-        )
-    got = xor_permute(sent, "tp", tp_count, tp_count // 2)
+    got = xor_permute(sent, "tp", tp_count, 1)
+    piece = (2, piece_rows + TAIL, piece_width)
+    parts = call(
+        spread_kernel,
+        "spread",
+        [(piece, F32)] + [(piece, BF16)] * (place_count - 1),
+        [kept, got],
+        scratch=[(half, F32)],
+        bits=bits,
+    )
+    parts = [parts[0]] + places_all(parts[1:], tp_count)
     act, stats = call(
         act_kernel,
         "act",
         [((1, piece_rows, piece_width), BF16), ((8, total_rows), F32)],
-        [kept, got, placed],
+        parts + [placed],
         model_width=model_width,
         expert_width=expert_width,
         dense_width=dense_width,
         expert_rows=expert_rows,
-        bits=(column_bits, row_bits),
-    )
-    distance = tp_count // 2
-    while distance:
-        act = jnp.concatenate([act, xor_permute(act, "tp", tp_count, distance)], axis=0)
-        distance //= 2
-    steps = tp_count.bit_length() - 1
+        bits=bits,
+    )
+    act = jnp.concatenate([act] + places_all([act] * (place_count - 1), tp_count), axis=0)
+    act = jnp.concatenate([act, xor_permute(act, "tp", tp_count, 1)], axis=0)
     places = []
     for index in range(tp_count):
-        row, column, rows, columns = 0, 0, slot_count, width
-        for bit in range(steps):
-            up = (index >> (steps - 1 - bit)) & 1
-            if bit in column_bits:
-                columns //= 2
-                column += up * columns
-            else:
-                rows //= 2
-                row += up * rows
-        places.append((row, column))
+        row, column = piece_at(index % place_count, bits, slot_count, width // 2)
+        places.append((row, column + index // place_count * (width // 2)))
     mixed = call(
         down_kernel,
         "down",
@@ -767,17 +771,13 @@
         [((seq_count, slice_width), F32), ((8, LANES), F32)],
         mixed,
     )
-    distance = 1
-    while distance < tp_count:
-        other = xor_permute(moments, "tp", tp_count, distance)
-        distance *= 2
-        if distance < tp_count:
-            moments = moments + other
+    moments = moments + xor_permute(moments, "tp", tp_count, 1)
+    others = places_all([moments] * (place_count - 1), tp_count)
     (layer_out,) = call(
         norm_kernel,
         "norm",
         [((seq_count, slice_width), BF16)],
-        [combined, second_gain[None, :], moments, other],
+        [combined, second_gain[None, :], moments] + others,
         model_width=model_width,
     )
     return layer_out

time: 112 us -> 92.1 us (0.82)
  local copies, waits for them, and re-layouts: 15 us -> 0.19 us
  waiting for transfers between devices: 54.1 us -> 40.7 us
  starting transfers between devices: 29.5 us -> 37.2 us
    unnamed x46, local copies, waits for them, and re-layouts: 15 us -> 0.15 us
    ppermute x22 -> x25, waiting for transfers between devices: 45.5 us -> 32.1 us  [xor_permute(): return lax.ppermute(array, axis, [(i, i ^ distance) for i in range(count)])]
    ppermute x22 -> x25, starting transfers between devices: 21.8 us -> 29.5 us  [xor_permute(): return lax.ppermute(array, axis, [(i, i ^ distance) for i in range(count)])]
  transfers between devices with their start and end apart: 28 -> 31, of which waited for: 26 -> 26; matrix products, arithmetic and copies ran while one was open for 0% -> 0% of each run, Pallas kernels for 0% -> 1%
where the time goes in v3:
time: 92.1 us; the launch traced here: 91.9 us
  waiting for transfers between devices  40.7 us (44%)
  starting transfers between devices  37.2 us (40%)
  Pallas kernels  13.3 us (14%)
    ppermute x25, waiting for transfers between devices, xor_permute(): return lax.ppermute(array, axis, [(i, i ^ distance) for i in range(count)])  32.1 us
    ppermute x25, starting transfers between devices, xor_permute(): return lax.ppermute(array, axis, [(i, i ^ distance) for i in range(count)])  29.5 us
    pallas_call x13, Pallas kernels, call(): pl.pallas_call(functools.partial(kernel, **sizes), out_shape=[jax.ShapeDt...  13.3 us
    ppermute x3, waiting for transfers between devices, on_device(): lax.ppermute(part_sum, both, [(device(c, c ^ d, h), device(c, c, h)) for...  6.75 us
    ppermute x3, starting transfers between devices, on_device(): lax.ppermute(residual, both, [(device(c, c, h), device(c ^ d, c, h)) for...  3.88 us
    ppermute x3, starting transfers between devices, on_device(): lax.ppermute(part_sum, both, [(device(c, c ^ d, h), device(c, c, h)) for...  3.88 us
    ppermute x3, waiting for transfers between devices, on_device(): lax.ppermute(residual, both, [(device(c, c, h), device(c ^ d, c, h)) for...  1.85 us
  transfers between devices with their start and end apart: 31, of which 26 were waited for; matrix products, arithmetic and copies ran while one was open for 0% of the time, Pallas kernels for 1%

profile of v3, /device:TPU:0, one launch (start us, length us, event | category | flops | bytes accessed | tf_op | source)
XLA Modules:
  0.0 91.9 jit_solution(1235675611243847504)
XLA Ops:
  0.0 1.2 %prepare.1 = (bf16[16,1152]{1,0:T(8,128)(2,1)S(1)}, bf16[16,1152]{1,0:T(8,128)(2,1)S(1)}, bf16[16,1152]{1,0:T(8,128)(2,1)S(1)}, bf16[16,1152]{1,0:T(8,128)(2,1)S(1)}) custom-call(bf16[16,4096]{1,0:T(8,128)(2,1)} %tokens.1, s32[2,16]{1,0:T(2,128)} %bitcast.19, f32[2,16]{1,0:T(2,128)} %bitcast.20), custom_call_target="tpu_custom_call" | custom-call | flops 20000000000 | bytes 20000000000 | tf_op jit(solution)/shard_map/prepare/pallas_call | solution.py:36
  1.2 3.0 %collective-permute-start = (bf16[16,1152]{1,0:T(8,128)(2,1)S(1)}, bf16[16,1152]{1,0:T(8,128)(2,1)S(1)}, u32[]{:S(2)}, u32[]{:S(2)}) collective-permute-start(bf16[16,1152]{1,0:T(8,128)(2,1)S(1)} %get-tuple-element.35), channel_id=1, source_target_pairs={{0,8},{8,0},{16,24},{24,16},{1,9},{9,1},{17,25},{25,17},{2,10},{10... | collective-permute-start | bytes 110600 | tf_op jit(solution)/shard_map/ppermute | solution.py:49
  4.3 1.5 %collective-permute-start.1 = (bf16[16,1152]{1,0:T(8,128)(2,1)S(1)}, bf16[16,1152]{1,0:T(8,128)(2,1)S(1)}, u32[]{:S(2)}, u32[]{:S(2)}) collective-permute-start(bf16[16,1152]{1,0:T(8,128)(2,1)S(1)} %get-tuple-element.36), channel_id=1, source_target_pairs={{0,16},{8,24},{16,0},{24,8},{1,17},{9,25},{17,1},{25,9},{2,18},{10... | collective-permute-start | bytes 110600 | tf_op jit(solution)/shard_map/ppermute | solution.py:49
  5.8 0.4 collective-permute-done.refs_1_.refs_5_
  6.2 2.0 %collective-permute-done.1.refs_2_.refs_6_ = bf16[16,1152]{1,0:T(8,128)(2,1)S(1)} collective-permute-done((bf16[16,1152]{1,0:T(8,128)(2,1)S(1)}, bf16[16,1152]{1,0:T(8,128)(2,1)S(1)}, u32[]{:S(2)}, u32[]{:S(2)}) %collective-permute-start.1) | collective-permute-done | bytes 36896 | tf_op jit(solution)/shard_map/ppermute | solution.py:49
  8.2 2.4 %collective-permute-done.2.refs_3_.refs_7_ = bf16[16,1152]{1,0:T(8,128)(2,1)S(1)} collective-permute-done((bf16[16,1152]{1,0:T(8,128)(2,1)S(1)}, bf16[16,1152]{1,0:T(8,128)(2,1)S(1)}, u32[]{:S(2)}, u32[]{:S(2)}) %collective-permute-start.2) | collective-permute-done | bytes 36896 | tf_op jit(solution)/shard_map/ppermute | solution.py:49
  10.7 0.5 project.1
  11.2 0.6 collective-permute-start.3
  11.8 2.9 %collective-permute-start.5 = (bf16[16,1024]{1,0:T(8,128)(2,1)S(1)}, bf16[16,1024]{1,0:T(8,128)(2,1)S(1)}, u32[]{:S(2)}, u32[]{:S(2)}) collective-permute-start(bf16[16,1024]{1,0:T(8,128)(2,1)S(1)} %get-tuple-element.41), channel_id=1, source_target_pairs={{0,24},{8,16},{16,8},{24,0},{1,25},{9,17},{17,9},{25,1},{2,26},{10... | collective-permute-start | bytes 98312 | tf_op jit(solution)/shard_map/ppermute | solution.py:49
  14.7 0.6 tables.1
  15.4 0.3 collective-permute-done.4.refs_2_
  15.7 0.9 %collective-permute-done.5.refs_3_ = bf16[16,1024]{1,0:T(8,128)(2,1)S(1)} collective-permute-done((bf16[16,1024]{1,0:T(8,128)(2,1)S(1)}, bf16[16,1024]{1,0:T(8,128)(2,1)S(1)}, u32[]{:S(2)}, u32[]{:S(2)}) %collective-permute-start.5) | collective-permute-done | bytes 32800 | tf_op jit(solution)/shard_map/ppermute | solution.py:49
  16.8 4.4 %attend.1.refs_0_ = bf16[16,512]{1,0:T(8,128)(2,1)S(1)} custom-call(s32[16]{0:T(128)S(1)} %copy-done.11, f32[4]{0:T(128)S(1)} %copy-done.12, f32[16,1024]{1,0:T(8,128)S(1)} %get-tuple-element.38.refs_0_, bf16[16,1024]{1,0:T(8,128)(2,1)S(1)} %collective-permute-done.3.refs_1_, bf16[16,1024]{1,0:T(8,128)(2,1)S(1)} %collective-permute-done.4.refs_2_, ...), custom_call_target="tpu_custom_call" | custom-call | flops 20000000000 | bytes 20000000000 | tf_op jit(solution)/shard_map/attend/pallas_call | solution.py:36
  21.1 3.0 %collective-permute-start.8 = (bf16[16,512]{1,0:T(8,128)(2,1)S(1)}, bf16[16,512]{1,0:T(8,128)(2,1)S(1)}, u32[]{:S(2)}, u32[]{:S(2)}) collective-permute-start(bf16[16,512]{1,0:T(8,128)(2,1)S(1)} %attend.1.refs_0_), channel_id=1, source_target_pairs={{0,24},{8,16},{16,8},{24,0},{1,25},{9,17},{17,9},{25,1},{2,26},{10... | collective-permute-start | bytes 49160 | tf_op jit(solution)/shard_map/ppermute | solution.py:49
  24.1 0.5 collective-permute-start.7
  24.6 0.1 collective-permute-start.6
  24.7 1.1 %collective-permute-done.8.refs_3_ = bf16[16,512]{1,0:T(8,128)(2,1)S(1)} collective-permute-done((bf16[16,512]{1,0:T(8,128)(2,1)S(1)}, bf16[16,512]{1,0:T(8,128)(2,1)S(1)}, u32[]{:S(2)}, u32[]{:S(2)}) %collective-permute-start.8) | collective-permute-done | bytes 16416 | tf_op jit(solution)/shard_map/ppermute | solution.py:49
  25.8 2.0 %collective-permute-done.7.refs_2_ = bf16[16,512]{1,0:T(8,128)(2,1)S(1)} collective-permute-done((bf16[16,512]{1,0:T(8,128)(2,1)S(1)}, bf16[16,512]{1,0:T(8,128)(2,1)S(1)}, u32[]{:S(2)}, u32[]{:S(2)}) %collective-permute-start.7) | collective-permute-done | bytes 16416 | tf_op jit(solution)/shard_map/ppermute | solution.py:49
  27.8 0.5 collective-permute-done.6.refs_1_
  28.3 0.3 outproj.1
  28.7 0.1 collective-permute-start.9
  28.7 1.2 %collective-permute-done.9.refs_1_ = bf16[64,512]{1,0:T(8,128)(2,1)S(1)} collective-permute-done((bf16[64,512]{1,0:T(8,128)(2,1)S(1)}, bf16[64,512]{1,0:T(8,128)(2,1)S(1)}, u32[]{:S(2)}, u32[]{:S(2)}) %collective-permute-start.9) | collective-permute-done | bytes 65568 | tf_op jit(solution)/shard_map/ppermute | solution.py:49
  30.0 1.3 %collective-permute-start.12 = (bf16[64,512]{1,0:T(8,128)(2,1)S(1)}, bf16[64,512]{1,0:T(8,128)(2,1)S(1)}, u32[]{:S(2)}, u32[]{:S(2)}) collective-permute-start(bf16[64,512]{1,0:T(8,128)(2,1)S(1)} %pairsum.1.refs_0_), channel_id=1, source_target_pairs={{6,0},{7,1},{12,10},{13,11},{18,20},{19,21},{24,30},{25,31}} | collective-permute-start | bytes 196616 | tf_op jit(solution)/shard_map/ppermute | solution.py:673
  31.3 1.3 %collective-permute-start.11 = (bf16[64,512]{1,0:T(8,128)(2,1)S(1)}, bf16[64,512]{1,0:T(8,128)(2,1)S(1)}, u32[]{:S(2)}, u32[]{:S(2)}) collective-permute-start(bf16[64,512]{1,0:T(8,128)(2,1)S(1)} %pairsum.1.refs_0_), channel_id=1, source_target_pairs={{4,0},{5,1},{14,10},{15,11},{16,20},{17,21},{26,30},{27,31}} | collective-permute-start | bytes 196616 | tf_op jit(solution)/shard_map/ppermute | solution.py:673
  32.6 1.3 %collective-permute-start.10 = (bf16[64,512]{1,0:T(8,128)(2,1)S(1)}, bf16[64,512]{1,0:T(8,128)(2,1)S(1)}, u32[]{:S(2)}, u32[]{:S(2)}) collective-permute-start(bf16[64,512]{1,0:T(8,128)(2,1)S(1)} %pairsum.1.refs_0_), channel_id=1, source_target_pairs={{2,0},{3,1},{8,10},{9,11},{22,20},{23,21},{28,30},{29,31}} | collective-permute-start | bytes 196616 | tf_op jit(solution)/shard_map/ppermute | solution.py:673
  33.9 4.1 %collective-permute-done.12.refs_3_ = bf16[64,512]{1,0:T(8,128)(2,1)S(1)} collective-permute-done((bf16[64,512]{1,0:T(8,128)(2,1)S(1)}, bf16[64,512]{1,0:T(8,128)(2,1)S(1)}, u32[]{:S(2)}, u32[]{:S(2)}) %collective-permute-start.12) | collective-permute-done | bytes 65568 | tf_op jit(solution)/shard_map/ppermute | solution.py:673
  38.0 1.3 %collective-permute-done.11.refs_2_ = bf16[64,512]{1,0:T(8,128)(2,1)S(1)} collective-permute-done((bf16[64,512]{1,0:T(8,128)(2,1)S(1)}, bf16[64,512]{1,0:T(8,128)(2,1)S(1)}, u32[]{:S(2)}, u32[]{:S(2)}) %collective-permute-start.11) | collective-permute-done | bytes 65568 | tf_op jit(solution)/shard_map/ppermute | solution.py:673
  39.4 1.3 %collective-permute-done.10.refs_1_ = bf16[64,512]{1,0:T(8,128)(2,1)S(1)} collective-permute-done((bf16[64,512]{1,0:T(8,128)(2,1)S(1)}, bf16[64,512]{1,0:T(8,128)(2,1)S(1)}, u32[]{:S(2)}, u32[]{:S(2)}) %collective-permute-start.10) | collective-permute-done | bytes 65568 | tf_op jit(solution)/shard_map/ppermute | solution.py:673
  40.7 0.2 residual.1.refs_0_
  40.8 1.3 %collective-permute-start.15 = (bf16[64,512]{1,0:T(8,128)(2,1)S(1)}, bf16[64,512]{1,0:T(8,128)(2,1)S(1)}, u32[]{:S(2)}, u32[]{:S(2)}) collective-permute-start(bf16[64,512]{1,0:T(8,128)(2,1)S(1)} %residual.1.refs_0_), channel_id=1, source_target_pairs={{0,24},{1,25},{10,18},{11,19},{20,12},{21,13},{30,6},{31,7}} | collective-permute-start | bytes 196616 | tf_op jit(solution)/shard_map/ppermute | solution.py:685
  42.1 1.3 %collective-permute-start.14 = (bf16[64,512]{1,0:T(8,128)(2,1)S(1)}, bf16[64,512]{1,0:T(8,128)(2,1)S(1)}, u32[]{:S(2)}, u32[]{:S(2)}) collective-permute-start(bf16[64,512]{1,0:T(8,128)(2,1)S(1)} %residual.1.refs_0_), channel_id=1, source_target_pairs={{0,16},{1,17},{10,26},{11,27},{20,4},{21,5},{30,14},{31,15}} | collective-permute-start | bytes 196616 | tf_op jit(solution)/shard_map/ppermute | solution.py:685
  43.4 1.3 %collective-permute-start.13 = (bf16[64,512]{1,0:T(8,128)(2,1)S(1)}, bf16[64,512]{1,0:T(8,128)(2,1)S(1)}, u32[]{:S(2)}, u32[]{:S(2)}) collective-permute-start(bf16[64,512]{1,0:T(8,128)(2,1)S(1)} %residual.1.refs_0_), channel_id=1, source_target_pairs={{0,8},{1,9},{10,2},{11,3},{20,28},{21,29},{30,22},{31,23}} | collective-permute-start | bytes 196616 | tf_op jit(solution)/shard_map/ppermute | solution.py:685
  44.8 0.5 collective-permute-done.14.refs_2_
  45.3 1.3 %collective-permute-done.13.refs_1_ = bf16[64,512]{1,0:T(8,128)(2,1)S(1)} collective-permute-done((bf16[64,512]{1,0:T(8,128)(2,1)S(1)}, bf16[64,512]{1,0:T(8,128)(2,1)S(1)}, u32[]{:S(2)}, u32[]{:S(2)}) %collective-permute-start.13) | collective-permute-done | bytes 65568 | tf_op jit(solution)/shard_map/ppermute | solution.py:685
  46.7 3.7 %experts.1 = (bf16[2,72,1280]{2,1,0:T(8,128)(2,1)S(1)}, f32[2,72,1280]{2,1,0:T(8,128)S(1)}, f32[64,64]{1,0:T(8,128)S(1)}, f32[64,128]{1,0:T(8,128)S(1)}, f32[16,512]{1,0:T(8,128)S(1)}) custom-call(bf16[64,512]{1,0:T(8,128)(2,1)S(1)} %residual.1.refs_0_, bf16[64,512]{1,0:T(8,128)(2,1)S(1)} %collective-permute-done.13.refs_1_, ...), custom_call_target="tpu_custom_call" | custom-call | tf_op jit(solution)/shard_map/experts/pallas_call | solution.py:36
  50.5 1.7 %collective-permute-done.16.got = bf16[2,72,1280]{2,1,0:T(8,128)(2,1)S(1)} collective-permute-done((bf16[2,72,1280]{2,1,0:T(8,128)(2,1)S(1)}, bf16[2,72,1280]{2,1,0:T(8,128)(2,1)S(1)}, u32[]{:S(2)}, u32[]{:S(2)}) %collective-permute-start.16) | collective-permute-done | bytes 368672 | tf_op jit(solution)/shard_map/ppermute | solution.py:49
  52.1 0.2 spread.1
  52.3 1.9 %collective-permute-start.17 = (bf16[2,40,640]{2,1,0:T(8,128)(2,1)S(1)}, bf16[2,40,640]{2,1,0:T(8,128)(2,1)S(1)}, u32[]{:S(2)}, u32[]{:S(2)}) collective-permute-start(bf16[2,40,640]{2,1,0:T(8,128)(2,1)S(1)} %get-tuple-element.49), channel_id=1, source_target_pairs={{0,2},{1,3},{2,0},{3,1},{4,6},{5,7},{6,4},{7,5},{8,10},{9,11},{10,... | collective-permute-start | bytes 307208 | tf_op jit(solution)/shard_map/ppermute | solution.py:49
  54.2 1.7 %collective-permute-start.18 = (bf16[2,40,640]{2,1,0:T(8,128)(2,1)S(1)}, bf16[2,40,640]{2,1,0:T(8,128)(2,1)S(1)}, u32[]{:S(2)}, u32[]{:S(2)}) collective-permute-start(bf16[2,40,640]{2,1,0:T(8,128)(2,1)S(1)} %get-tuple-element.50), channel_id=1, source_target_pairs={{0,4},{1,5},{2,6},{3,7},{4,0},{5,1},{6,2},{7,3},{8,12},{9,13},{10,... | collective-permute-start | bytes 307208 | tf_op jit(solution)/shard_map/ppermute | solution.py:49
  55.8 0.9 collective-permute-start.19
  56.8 0.7 collective-permute-done.17.refs_1_
  57.4 7.4 %collective-permute-done.18.refs_2_ = bf16[2,40,640]{2,1,0:T(8,128)(2,1)S(1)} collective-permute-done((bf16[2,40,640]{2,1,0:T(8,128)(2,1)S(1)}, bf16[2,40,640]{2,1,0:T(8,128)(2,1)S(1)}, u32[]{:S(2)}, u32[]{:S(2)}) %collective-permute-start.18) | collective-permute-done | bytes 102432 | tf_op jit(solution)/shard_map/ppermute | solution.py:49
  64.9 0.2 act.1
  65.0 1.7 %collective-permute-start.22 = (bf16[1,32,640]{2,1,0:T(8,128)(2,1)S(1)}, bf16[1,32,640]{2,1,0:T(8,128)(2,1)S(1)}, u32[]{:S(2)}, u32[]{:S(2)}) collective-permute-start(bf16[1,32,640]{2,1,0:T(8,128)(2,1)S(1)} %get-tuple-element.53), channel_id=1, source_target_pairs={{0,6},{1,7},{2,4},{3,5},{4,2},{5,3},{6,0},{7,1},{8,14},{9,15},{10,... | collective-permute-start | bytes 122888 | tf_op jit(solution)/shard_map/ppermute | solution.py:49
  66.7 1.9 %collective-permute-start.21 = (bf16[1,32,640]{2,1,0:T(8,128)(2,1)S(1)}, bf16[1,32,640]{2,1,0:T(8,128)(2,1)S(1)}, u32[]{:S(2)}, u32[]{:S(2)}) collective-permute-start(bf16[1,32,640]{2,1,0:T(8,128)(2,1)S(1)} %get-tuple-element.53), channel_id=1, source_target_pairs={{0,4},{1,5},{2,6},{3,7},{4,0},{5,1},{6,2},{7,3},{8,12},{9,13},{10,... | collective-permute-start | bytes 122888 | tf_op jit(solution)/shard_map/ppermute | solution.py:49
  68.6 0.9 collective-permute-start.20
  69.5 1.5 %collective-permute-done.22 = bf16[1,32,640]{2,1,0:T(8,128)(2,1)S(1)} collective-permute-done((bf16[1,32,640]{2,1,0:T(8,128)(2,1)S(1)}, bf16[1,32,640]{2,1,0:T(8,128)(2,1)S(1)}, u32[]{:S(2)}, u32[]{:S(2)}) %collective-permute-start.22) | collective-permute-done | bytes 40992 | tf_op jit(solution)/shard_map/ppermute | solution.py:49
  71.0 0.6 collective-permute-done.21
  71.6 1.0 %collective-permute-done.20 = bf16[1,32,640]{2,1,0:T(8,128)(2,1)S(1)} collective-permute-done((bf16[1,32,640]{2,1,0:T(8,128)(2,1)S(1)}, bf16[1,32,640]{2,1,0:T(8,128)(2,1)S(1)}, u32[]{:S(2)}, u32[]{:S(2)}) %collective-permute-start.20) | collective-permute-done | bytes 40992 | tf_op jit(solution)/shard_map/ppermute | solution.py:49
  72.7 1.3 %collective-permute-done.23 = bf16[4,32,640]{2,1,0:T(8,128)(2,1)S(1)} collective-permute-done((bf16[4,32,640]{2,1,0:T(8,128)(2,1)S(1)}, bf16[4,32,640]{2,1,0:T(8,128)(2,1)S(1)}, u32[]{:S(2)}, u32[]{:S(2)}) %collective-permute-start.23) | collective-permute-done | bytes 163872 | tf_op jit(solution)/shard_map/ppermute | solution.py:49
  74.1 1.4 %down.1 = (f32[16,512]{1,0:T(8,128)S(1)}, bf16[16,512]{1,0:T(8,128)(2,1)S(1)}, bf16[16,512]{1,0:T(8,128)(2,1)S(1)}, bf16[16,512]{1,0:T(8,128)(2,1)S(1)}) custom-call(bf16[8,32,640]{2,1,0:T(8,128)(2,1)S(1)} %constant_dynamic-update-slice_fusion.acts, f32[8,64]{1,0:T(8,128)S(1)} %get-tuple-element.54.stats, f32[64,128]{1,0:T(8,128)S(1)} %get-tuple-element.55.info, ...), custom_call_target="tpu_custom_call" | custom-call | tf_op jit(solution)/shard_map/down/pallas_call | solution.py:36
  75.5 1.4 %collective-permute-start.24 = (bf16[16,512]{1,0:T(8,128)(2,1)S(1)}, bf16[16,512]{1,0:T(8,128)(2,1)S(1)}, u32[]{:S(2)}, u32[]{:S(2)}) collective-permute-start(bf16[16,512]{1,0:T(8,128)(2,1)S(1)} %get-tuple-element.58), channel_id=1, source_target_pairs={{0,8},{8,0},{16,24},{24,16},{1,9},{9,1},{17,25},{25,17},{2,10},{10... | collective-permute-start | bytes 49160 | tf_op jit(solution)/shard_map/ppermute | solution.py:49
  76.9 1.4 %collective-permute-start.25 = (bf16[16,512]{1,0:T(8,128)(2,1)S(1)}, bf16[16,512]{1,0:T(8,128)(2,1)S(1)}, u32[]{:S(2)}, u32[]{:S(2)}) collective-permute-start(bf16[16,512]{1,0:T(8,128)(2,1)S(1)} %get-tuple-element.59), channel_id=1, source_target_pairs={{0,16},{8,24},{16,0},{24,8},{1,17},{9,25},{17,1},{25,9},{2,18},{10... | collective-permute-start | bytes 49160 | tf_op jit(solution)/shard_map/ppermute | solution.py:49
  78.2 1.4 %collective-permute-start.26 = (bf16[16,512]{1,0:T(8,128)(2,1)S(1)}, bf16[16,512]{1,0:T(8,128)(2,1)S(1)}, u32[]{:S(2)}, u32[]{:S(2)}) collective-permute-start(bf16[16,512]{1,0:T(8,128)(2,1)S(1)} %get-tuple-element.60), channel_id=1, source_target_pairs={{0,24},{8,16},{16,8},{24,0},{1,25},{9,17},{17,9},{25,1},{2,26},{10... | collective-permute-start | bytes 49160 | tf_op jit(solution)/shard_map/ppermute | solution.py:49
  79.6 1.0 %collective-permute-done.25.refs_2_ = bf16[16,512]{1,0:T(8,128)(2,1)S(1)} collective-permute-done((bf16[16,512]{1,0:T(8,128)(2,1)S(1)}, bf16[16,512]{1,0:T(8,128)(2,1)S(1)}, u32[]{:S(2)}, u32[]{:S(2)}) %collective-permute-start.25) | collective-permute-done | bytes 16416 | tf_op jit(solution)/shard_map/ppermute | solution.py:49
  80.6 2.3 %collective-permute-done.26.refs_3_ = bf16[16,512]{1,0:T(8,128)(2,1)S(1)} collective-permute-done((bf16[16,512]{1,0:T(8,128)(2,1)S(1)}, bf16[16,512]{1,0:T(8,128)(2,1)S(1)}, u32[]{:S(2)}, u32[]{:S(2)}) %collective-permute-start.26) | collective-permute-done | bytes 16416 | tf_op jit(solution)/shard_map/ppermute | solution.py:49
  82.9 0.1 combine.1
  83.0 0.1 collective-permute-start.27
  83.1 1.2 %collective-permute-done.27 = f32[8,128]{1,0:T(8,128)S(1)} collective-permute-done((f32[8,128]{1,0:T(8,128)S(1)}, f32[8,128]{1,0:T(8,128)S(1)}, u32[]{:S(2)}, u32[]{:S(2)}) %collective-permute-start.27) | collective-permute-done | bytes 4128 | tf_op jit(solution)/shard_map/ppermute | solution.py:49
  84.2 2.5 %collective-permute-start.30 = (f32[8,128]{1,0:T(8,128)S(1)}, f32[8,128]{1,0:T(8,128)S(1)}, u32[]{:S(2)}, u32[]{:S(2)}) collective-permute-start(f32[8,128]{1,0:T(8,128)S(1)} %add.3.refs_2_), channel_id=1, source_target_pairs={{0,6},{1,7},{2,4},{3,5},{4,2},{5,3},{6,0},{7,1},{8,14},{9,15},{10,... | collective-permute-start | bytes 12296 | tf_op jit(solution)/shard_map/ppermute | solution.py:49
  86.7 1.9 %collective-permute-start.28 = (f32[8,128]{1,0:T(8,128)S(1)}, f32[8,128]{1,0:T(8,128)S(1)}, u32[]{:S(2)}, u32[]{:S(2)}) collective-permute-start(f32[8,128]{1,0:T(8,128)S(1)} %add.3.refs_2_), channel_id=1, source_target_pairs={{0,2},{1,3},{2,0},{3,1},{4,6},{5,7},{6,4},{7,5},{8,10},{9,11},{10,... | collective-permute-start | bytes 12296 | tf_op jit(solution)/shard_map/ppermute | solution.py:49
  88.6 1.0 %collective-permute-done.30.refs_5_ = f32[8,128]{1,0:T(8,128)S(1)} collective-permute-done((f32[8,128]{1,0:T(8,128)S(1)}, f32[8,128]{1,0:T(8,128)S(1)}, u32[]{:S(2)}, u32[]{:S(2)}) %collective-permute-start.30) | collective-permute-done | bytes 4128 | tf_op jit(solution)/shard_map/ppermute | solution.py:49
  89.6 1.6 %collective-permute-done.29.refs_4_ = f32[8,128]{1,0:T(8,128)S(1)} collective-permute-done((f32[8,128]{1,0:T(8,128)S(1)}, f32[8,128]{1,0:T(8,128)S(1)}, u32[]{:S(2)}, u32[]{:S(2)}) %collective-permute-start.29) | collective-permute-done | bytes 4128 | tf_op jit(solution)/shard_map/ppermute | solution.py:49
  91.2 0.7 norm.1
  (64 shorter events, 0.5 us)
Async XLA Ops:
  0.0 10.7 %copy-start = (bf16[1024,512]{1,0:T(8,128)(2,1)S(1)}, bf16[1024,512]{1,0:T(8,128)(2,1)}, u32[]{:S(2)}) copy-start(bf16[1024,512]{1,0:T(8,128)(2,1)} %refs_4_.2) | copy-start | bytes 3145732
  0.0 10.7 %copy-start.2 = (bf16[1024,256]{1,0:T(8,128)(2,1)S(1)}, bf16[1024,256]{1,0:T(8,128)(2,1)}, u32[]{:S(2)}) copy-start(bf16[1024,256]{1,0:T(8,128)(2,1)} %refs_5_.1) | copy-start | bytes 1572868
  0.0 10.7 %copy-start.3 = (bf16[1024,256]{1,0:T(8,128)(2,1)S(1)}, bf16[1024,256]{1,0:T(8,128)(2,1)}, u32[]{:S(2)}) copy-start(bf16[1024,256]{1,0:T(8,128)(2,1)} %refs_6_.1) | copy-start | bytes 1572868
  0.0 14.7 %copy-start.11 = (s32[16]{0:T(128)S(1)}, s32[16]{0:T(128)}, u32[]{:S(2)}) copy-start(s32[16]{0:T(128)} %lengths.3) | copy-start | bytes 196
  0.0 16.6 %copy-start.9 = (bf16[16,1024,2,128]{3,2,1,0:T(2,128)(2,1)S(1)}, bf16[16,1024,2,128]{3,2,1,0:T(2,128)(2,1)}, u32[]{:S(2)}) copy-start(bf16[16,1024,2,128]{3,2,1,0:T(2,128)(2,1)} %param.28) | copy-start | bytes 25165828
  0.0 16.6 %copy-start.10 = (bf16[16,1024,2,128]{3,2,1,0:T(2,128)(2,1)S(1)}, bf16[16,1024,2,128]{3,2,1,0:T(2,128)(2,1)}, u32[]{:S(2)}) copy-start(bf16[16,1024,2,128]{3,2,1,0:T(2,128)(2,1)} %param.29) | copy-start | bytes 25165828
  0.0 16.6 %copy-start.12 = (f32[4]{0:T(128)S(1)}, f32[4]{0:T(128)}, u32[]{:S(2)}) copy-start(f32[4]{0:T(128)} %lambdas.1) | copy-start | bytes 52
  0.0 16.6 %copy-start.13 = (f32[128]{0:T(128)S(1)}, f32[128]{0:T(128)}, u32[]{:S(2)}) copy-start(f32[128]{0:T(128)} %param.27) | copy-start | bytes 1540
  1.2 5.0 %collective-permute-start = (bf16[16,1152]{1,0:T(8,128)(2,1)S(1)}, bf16[16,1152]{1,0:T(8,128)(2,1)S(1)}, u32[]{:S(2)}, u32[]{:S(2)}) collective-permute-start(bf16[16,1152]{1,0:T(8,128)(2,1)S(1)} %get-tuple-element.35), channel_id=1, source_target_pairs={{0,8},{8,0},{16,24},{24,16},{1,9},{9,1},{17,25},{25,17},{2,10},{10... | collective-permute-start | bytes 110600 | tf_op jit(solution)/shard_map/ppermute | solution.py:49
  4.3 4.0 %collective-permute-start.1 = (bf16[16,1152]{1,0:T(8,128)(2,1)S(1)}, bf16[16,1152]{1,0:T(8,128)(2,1)S(1)}, u32[]{:S(2)}, u32[]{:S(2)}) collective-permute-start(bf16[16,1152]{1,0:T(8,128)(2,1)S(1)} %get-tuple-element.36), channel_id=1, source_target_pairs={{0,16},{8,24},{16,0},{24,8},{1,17},{9,25},{17,1},{25,9},{2,18},{10... | collective-permute-start | bytes 110600 | tf_op jit(solution)/shard_map/ppermute | solution.py:49
  5.8 4.9 %collective-permute-start.2 = (bf16[16,1152]{1,0:T(8,128)(2,1)S(1)}, bf16[16,1152]{1,0:T(8,128)(2,1)S(1)}, u32[]{:S(2)}, u32[]{:S(2)}) collective-permute-start(bf16[16,1152]{1,0:T(8,128)(2,1)S(1)} %get-tuple-element.37), channel_id=1, source_target_pairs={{0,24},{8,16},{16,8},{24,0},{1,25},{9,17},{17,9},{25,1},{2,26},{10... | collective-permute-start | bytes 110600 | tf_op jit(solution)/shard_map/ppermute | solution.py:49
  10.7 36.0 %slice-start.2 = ((s8[8388608]{0:T(1024)(128)(4,1)}), s8[4194304]{0:T(1024)(128)(4,1)S(1)}, s32[]{:S(2)}) async-start(s8[8388608]{0:T(1024)(128)(4,1)} %bitcast.9), calls=%async_computation.2 | async-start | bytes 8388608
  10.7 35.9 %slice-start.4 = ((s8[8388608]{0:T(1024)(128)(4,1)}), s8[4194304]{0:T(1024)(128)(4,1)S(1)}, s32[]{:S(2)}) async-start(s8[8388608]{0:T(1024)(128)(4,1)} %bitcast.11), calls=%async_computation.4 | async-start | bytes 8388608
  11.2 4.2 %collective-permute-start.3 = (bf16[16,1024]{1,0:T(8,128)(2,1)S(1)}, bf16[16,1024]{1,0:T(8,128)(2,1)S(1)}, u32[]{:S(2)}, u32[]{:S(2)}) collective-permute-start(bf16[16,1024]{1,0:T(8,128)(2,1)S(1)} %get-tuple-element.39), channel_id=1, source_target_pairs={{0,8},{8,0},{16,24},{24,16},{1,9},{9,1},{17,25},{25,17},{2,10},{10... | collective-permute-start | bytes 98312 | tf_op jit(solution)/shard_map/ppermute | solution.py:49
  11.8 3.9 %collective-permute-start.4 = (bf16[16,1024]{1,0:T(8,128)(2,1)S(1)}, bf16[16,1024]{1,0:T(8,128)(2,1)S(1)}, u32[]{:S(2)}, u32[]{:S(2)}) collective-permute-start(bf16[16,1024]{1,0:T(8,128)(2,1)S(1)} %get-tuple-element.40), channel_id=1, source_target_pairs={{0,16},{8,24},{16,0},{24,8},{1,17},{9,25},{17,1},{25,9},{2,18},{10... | collective-permute-start | bytes 98312 | tf_op jit(solution)/shard_map/ppermute | solution.py:49
  11.8 4.8 %collective-permute-start.5 = (bf16[16,1024]{1,0:T(8,128)(2,1)S(1)}, bf16[16,1024]{1,0:T(8,128)(2,1)S(1)}, u32[]{:S(2)}, u32[]{:S(2)}) collective-permute-start(bf16[16,1024]{1,0:T(8,128)(2,1)S(1)} %get-tuple-element.41), channel_id=1, source_target_pairs={{0,24},{8,16},{16,8},{24,0},{1,25},{9,17},{17,9},{25,1},{2,26},{10... | collective-permute-start | bytes 98312 | tf_op jit(solution)/shard_map/ppermute | solution.py:49
  16.7 11.7 %copy-start.1 = (bf16[512,1024]{1,0:T(8,128)(2,1)S(1)}, bf16[512,1024]{1,0:T(8,128)(2,1)}, u32[]{:S(2)}) copy-start(bf16[512,1024]{1,0:T(8,128)(2,1)} %refs_4_.3) | copy-start | bytes 3145732
  16.7 28.1 %copy-start.14 = (bf16[4096]{0:T(1024)(128)(2,1)S(1)}, bf16[4096]{0:T(1024)(128)(2,1)}, u32[]{:S(2)}) copy-start(bf16[4096]{0:T(1024)(128)(2,1)} %param.41) | copy-start | bytes 24580
  16.7 29.9 %slice-start.3 = ((s8[8388608]{0:T(1024)(128)(4,1)}), s8[4194304]{0:T(1024)(128)(4,1)S(1)}, s32[]{:S(2)}) async-start(s8[8388608]{0:T(1024)(128)(4,1)} %bitcast.9), calls=%async_computation.3 | async-start | bytes 8388608
  16.7 29.9 %slice-start.5 = ((s8[8388608]{0:T(1024)(128)(4,1)}), s8[4194304]{0:T(1024)(128)(4,1)S(1)}, s32[]{:S(2)}) async-start(s8[8388608]{0:T(1024)(128)(4,1)} %bitcast.11), calls=%async_computation.5 | async-start | bytes 8388608
  16.7 29.9 %copy-start.5 = (bf16[512,512]{1,0:T(8,128)(2,1)S(1)}, bf16[512,512]{1,0:T(8,128)(2,1)}, u32[]{:S(2)}) copy-start(bf16[512,512]{1,0:T(8,128)(2,1)} %refs_12_.1) | copy-start | bytes 1572868
  16.7 29.9 %copy-start.6 = (bf16[512,512]{1,0:T(8,128)(2,1)S(1)}, bf16[512,512]{1,0:T(8,128)(2,1)}, u32[]{:S(2)}) copy-start(bf16[512,512]{1,0:T(8,128)(2,1)} %refs_13_.1) | copy-start | bytes 1572868
  16.7 29.9 %copy-start.7 = (f32[4096]{0:T(1024)S(1)}, f32[4096]{0:T(1024)}, u32[]{:S(2)}) copy-start(f32[4096]{0:T(1024)} %param.31) | copy-start | bytes 49156
  21.1 4.7 %collective-permute-start.8 = (bf16[16,512]{1,0:T(8,128)(2,1)S(1)}, bf16[16,512]{1,0:T(8,128)(2,1)S(1)}, u32[]{:S(2)}, u32[]{:S(2)}) collective-permute-start(bf16[16,512]{1,0:T(8,128)(2,1)S(1)} %attend.1.refs_0_), channel_id=1, source_target_pairs={{0,24},{8,16},{16,8},{24,0},{1,25},{9,17},{17,9},{25,1},{2,26},{10... | collective-permute-start | bytes 49160 | tf_op jit(solution)/shard_map/ppermute | solution.py:49
  24.1 3.7 %collective-permute-start.7 = (bf16[16,512]{1,0:T(8,128)(2,1)S(1)}, bf16[16,512]{1,0:T(8,128)(2,1)S(1)}, u32[]{:S(2)}, u32[]{:S(2)}) collective-permute-start(bf16[16,512]{1,0:T(8,128)(2,1)S(1)} %attend.1.refs_0_), channel_id=1, source_target_pairs={{0,16},{8,24},{16,0},{24,8},{1,17},{9,25},{17,1},{25,9},{2,18},{10... | collective-permute-start | bytes 49160 | tf_op jit(solution)/shard_map/ppermute | solution.py:49
  24.6 3.7 %collective-permute-start.6 = (bf16[16,512]{1,0:T(8,128)(2,1)S(1)}, bf16[16,512]{1,0:T(8,128)(2,1)S(1)}, u32[]{:S(2)}, u32[]{:S(2)}) collective-permute-start(bf16[16,512]{1,0:T(8,128)(2,1)S(1)} %attend.1.refs_0_), channel_id=1, source_target_pairs={{0,8},{8,0},{16,24},{24,16},{1,9},{9,1},{17,25},{25,17},{2,10},{10... | collective-permute-start | bytes 49160 | tf_op jit(solution)/shard_map/ppermute | solution.py:49
  28.7 1.3 %collective-permute-start.9 = (bf16[64,512]{1,0:T(8,128)(2,1)S(1)}, bf16[64,512]{1,0:T(8,128)(2,1)S(1)}, u32[]{:S(2)}, u32[]{:S(2)}) collective-permute-start(bf16[64,512]{1,0:T(8,128)(2,1)S(1)} %get-tuple-element.45), channel_id=1, source_target_pairs={{0,1},{1,0},{2,3},{3,2},{4,5},{5,4},{6,7},{7,6},{8,9},{9,8},{10,11... | collective-permute-start | bytes 196616 | tf_op jit(solution)/shard_map/ppermute | solution.py:49
  30.0 8.0 %collective-permute-start.12 = (bf16[64,512]{1,0:T(8,128)(2,1)S(1)}, bf16[64,512]{1,0:T(8,128)(2,1)S(1)}, u32[]{:S(2)}, u32[]{:S(2)}) collective-permute-start(bf16[64,512]{1,0:T(8,128)(2,1)S(1)} %pairsum.1.refs_0_), channel_id=1, source_target_pairs={{6,0},{7,1},{12,10},{13,11},{18,20},{19,21},{24,30},{25,31}} | collective-permute-start | bytes 196616 | tf_op jit(solution)/shard_map/ppermute | solution.py:673
  31.3 8.1 %collective-permute-start.11 = (bf16[64,512]{1,0:T(8,128)(2,1)S(1)}, bf16[64,512]{1,0:T(8,128)(2,1)S(1)}, u32[]{:S(2)}, u32[]{:S(2)}) collective-permute-start(bf16[64,512]{1,0:T(8,128)(2,1)S(1)} %pairsum.1.refs_0_), channel_id=1, source_target_pairs={{4,0},{5,1},{14,10},{15,11},{16,20},{17,21},{26,30},{27,31}} | collective-permute-start | bytes 196616 | tf_op jit(solution)/shard_map/ppermute | solution.py:673
  32.6 8.1 %collective-permute-start.10 = (bf16[64,512]{1,0:T(8,128)(2,1)S(1)}, bf16[64,512]{1,0:T(8,128)(2,1)S(1)}, u32[]{:S(2)}, u32[]{:S(2)}) collective-permute-start(bf16[64,512]{1,0:T(8,128)(2,1)S(1)} %pairsum.1.refs_0_), channel_id=1, source_target_pairs={{2,0},{3,1},{8,10},{9,11},{22,20},{23,21},{28,30},{29,31}} | collective-permute-start | bytes 196616 | tf_op jit(solution)/shard_map/ppermute | solution.py:673
  40.8 3.9 %collective-permute-start.15 = (bf16[64,512]{1,0:T(8,128)(2,1)S(1)}, bf16[64,512]{1,0:T(8,128)(2,1)S(1)}, u32[]{:S(2)}, u32[]{:S(2)}) collective-permute-start(bf16[64,512]{1,0:T(8,128)(2,1)S(1)} %residual.1.refs_0_), channel_id=1, source_target_pairs={{0,24},{1,25},{10,18},{11,19},{20,12},{21,13},{30,6},{31,7}} | collective-permute-start | bytes 196616 | tf_op jit(solution)/shard_map/ppermute | solution.py:685
  42.1 3.2 %collective-permute-start.14 = (bf16[64,512]{1,0:T(8,128)(2,1)S(1)}, bf16[64,512]{1,0:T(8,128)(2,1)S(1)}, u32[]{:S(2)}, u32[]{:S(2)}) collective-permute-start(bf16[64,512]{1,0:T(8,128)(2,1)S(1)} %residual.1.refs_0_), channel_id=1, source_target_pairs={{0,16},{1,17},{10,26},{11,27},{20,4},{21,5},{30,14},{31,15}} | collective-permute-start | bytes 196616 | tf_op jit(solution)/shard_map/ppermute | solution.py:685
  43.4 3.2 %collective-permute-start.13 = (bf16[64,512]{1,0:T(8,128)(2,1)S(1)}, bf16[64,512]{1,0:T(8,128)(2,1)S(1)}, u32[]{:S(2)}, u32[]{:S(2)}) collective-permute-start(bf16[64,512]{1,0:T(8,128)(2,1)S(1)} %residual.1.refs_0_), channel_id=1, source_target_pairs={{0,8},{1,9},{10,2},{11,3},{20,28},{21,29},{30,22},{31,23}} | collective-permute-start | bytes 196616 | tf_op jit(solution)/shard_map/ppermute | solution.py:685
  46.6 27.5 %slice-start = ((s8[8388608]{0:T(1024)(128)(4,1)}), s8[4194304]{0:T(1024)(128)(4,1)S(1)}, s32[]{:S(2)}) async-start(s8[8388608]{0:T(1024)(128)(4,1)} %bitcast.7), calls=%async_computation | async-start | bytes 8388608
  46.7 27.4 %slice-start.1 = ((s8[8388608]{0:T(1024)(128)(4,1)}), s8[4194304]{0:T(1024)(128)(4,1)S(1)}, s32[]{:S(2)}) async-start(s8[8388608]{0:T(1024)(128)(4,1)} %bitcast.7), calls=%async_computation.1 | async-start | bytes 8388608
  46.7 27.4 %copy-start.4 = (bf16[512,512]{1,0:T(8,128)(2,1)S(1)}, bf16[512,512]{1,0:T(8,128)(2,1)}, u32[]{:S(2)}) copy-start(bf16[512,512]{1,0:T(8,128)(2,1)} %dense_down.1) | copy-start | bytes 1572868
  50.4 40.8 %copy-start.8 = (f32[512]{0:T(512)S(1)}, f32[512]{0:T(512)}, u32[]{:S(2)}) copy-start(f32[512]{0:T(512)} %param.32) | copy-start | bytes 6148
  50.4 1.8 %collective-permute-start.16 = (bf16[2,72,1280]{2,1,0:T(8,128)(2,1)S(1)}, bf16[2,72,1280]{2,1,0:T(8,128)(2,1)S(1)}, u32[]{:S(2)}, u32[]{:S(2)}) collective-permute-start(bf16[2,72,1280]{2,1,0:T(8,128)(2,1)S(1)} %get-tuple-element.47), channel_id=1, source_target_pairs={{0,1},{1,0},{2,3},{3,2},{4,5},{5,4},{6,7},{7,6},{8,9},{9,8},{10,11... | collective-permute-start | bytes 1105928 | tf_op jit(solution)/shard_map/ppermute | solution.py:49
  52.3 5.1 %collective-permute-start.17 = (bf16[2,40,640]{2,1,0:T(8,128)(2,1)S(1)}, bf16[2,40,640]{2,1,0:T(8,128)(2,1)S(1)}, u32[]{:S(2)}, u32[]{:S(2)}) collective-permute-start(bf16[2,40,640]{2,1,0:T(8,128)(2,1)S(1)} %get-tuple-element.49), channel_id=1, source_target_pairs={{0,2},{1,3},{2,0},{3,1},{4,6},{5,7},{6,4},{7,5},{8,10},{9,11},{10,... | collective-permute-start | bytes 307208 | tf_op jit(solution)/shard_map/ppermute | solution.py:49
  54.2 10.7 %collective-permute-start.18 = (bf16[2,40,640]{2,1,0:T(8,128)(2,1)S(1)}, bf16[2,40,640]{2,1,0:T(8,128)(2,1)S(1)}, u32[]{:S(2)}, u32[]{:S(2)}) collective-permute-start(bf16[2,40,640]{2,1,0:T(8,128)(2,1)S(1)} %get-tuple-element.50), channel_id=1, source_target_pairs={{0,4},{1,5},{2,6},{3,7},{4,0},{5,1},{6,2},{7,3},{8,12},{9,13},{10,... | collective-permute-start | bytes 307208 | tf_op jit(solution)/shard_map/ppermute | solution.py:49
  55.8 9.0 %collective-permute-start.19 = (bf16[2,40,640]{2,1,0:T(8,128)(2,1)S(1)}, bf16[2,40,640]{2,1,0:T(8,128)(2,1)S(1)}, u32[]{:S(2)}, u32[]{:S(2)}) collective-permute-start(bf16[2,40,640]{2,1,0:T(8,128)(2,1)S(1)} %get-tuple-element.51), channel_id=1, source_target_pairs={{0,6},{1,7},{2,4},{3,5},{4,2},{5,3},{6,0},{7,1},{8,14},{9,15},{10,... | collective-permute-start | bytes 307208 | tf_op jit(solution)/shard_map/ppermute | solution.py:49
  65.0 6.0 %collective-permute-start.22 = (bf16[1,32,640]{2,1,0:T(8,128)(2,1)S(1)}, bf16[1,32,640]{2,1,0:T(8,128)(2,1)S(1)}, u32[]{:S(2)}, u32[]{:S(2)}) collective-permute-start(bf16[1,32,640]{2,1,0:T(8,128)(2,1)S(1)} %get-tuple-element.53), channel_id=1, source_target_pairs={{0,6},{1,7},{2,4},{3,5},{4,2},{5,3},{6,0},{7,1},{8,14},{9,15},{10,... | collective-permute-start | bytes 122888 | tf_op jit(solution)/shard_map/ppermute | solution.py:49
  66.7 4.9 %collective-permute-start.21 = (bf16[1,32,640]{2,1,0:T(8,128)(2,1)S(1)}, bf16[1,32,640]{2,1,0:T(8,128)(2,1)S(1)}, u32[]{:S(2)}, u32[]{:S(2)}) collective-permute-start(bf16[1,32,640]{2,1,0:T(8,128)(2,1)S(1)} %get-tuple-element.53), channel_id=1, source_target_pairs={{0,4},{1,5},{2,6},{3,7},{4,0},{5,1},{6,2},{7,3},{8,12},{9,13},{10,... | collective-permute-start | bytes 122888 | tf_op jit(solution)/shard_map/ppermute | solution.py:49
  68.6 4.0 %collective-permute-start.20 = (bf16[1,32,640]{2,1,0:T(8,128)(2,1)S(1)}, bf16[1,32,640]{2,1,0:T(8,128)(2,1)S(1)}, u32[]{:S(2)}, u32[]{:S(2)}) collective-permute-start(bf16[1,32,640]{2,1,0:T(8,128)(2,1)S(1)} %get-tuple-element.53), channel_id=1, source_target_pairs={{0,2},{1,3},{2,0},{3,1},{4,6},{5,7},{6,4},{7,5},{8,10},{9,11},{10,... | collective-permute-start | bytes 122888 | tf_op jit(solution)/shard_map/ppermute | solution.py:49
  72.6 1.5 %collective-permute-start.23 = (bf16[4,32,640]{2,1,0:T(8,128)(2,1)S(1)}, bf16[4,32,640]{2,1,0:T(8,128)(2,1)S(1)}, u32[]{:S(2)}, u32[]{:S(2)}) collective-permute-start(bf16[4,32,640]{2,1,0:T(8,128)(2,1)S(1)} %pad_maximum_fusion), channel_id=1, source_target_pairs={{0,1},{1,0},{2,3},{3,2},{4,5},{5,4},{6,7},{7,6},{8,9},{9,8},{10,11... | collective-permute-start | bytes 491528 | tf_op jit(solution)/shard_map/ppermute | solution.py:49
  75.5 4.1 %collective-permute-start.24 = (bf16[16,512]{1,0:T(8,128)(2,1)S(1)}, bf16[16,512]{1,0:T(8,128)(2,1)S(1)}, u32[]{:S(2)}, u32[]{:S(2)}) collective-permute-start(bf16[16,512]{1,0:T(8,128)(2,1)S(1)} %get-tuple-element.58), channel_id=1, source_target_pairs={{0,8},{8,0},{16,24},{24,16},{1,9},{9,1},{17,25},{25,17},{2,10},{10... | collective-permute-start | bytes 49160 | tf_op jit(solution)/shard_map/ppermute | solution.py:49
  76.9 3.7 %collective-permute-start.25 = (bf16[16,512]{1,0:T(8,128)(2,1)S(1)}, bf16[16,512]{1,0:T(8,128)(2,1)S(1)}, u32[]{:S(2)}, u32[]{:S(2)}) collective-permute-start(bf16[16,512]{1,0:T(8,128)(2,1)S(1)} %get-tuple-element.59), channel_id=1, source_target_pairs={{0,16},{8,24},{16,0},{24,8},{1,17},{9,25},{17,1},{25,9},{2,18},{10... | collective-permute-start | bytes 49160 | tf_op jit(solution)/shard_map/ppermute | solution.py:49
  78.2 4.6 %collective-permute-start.26 = (bf16[16,512]{1,0:T(8,128)(2,1)S(1)}, bf16[16,512]{1,0:T(8,128)(2,1)S(1)}, u32[]{:S(2)}, u32[]{:S(2)}) collective-permute-start(bf16[16,512]{1,0:T(8,128)(2,1)S(1)} %get-tuple-element.60), channel_id=1, source_target_pairs={{0,24},{8,16},{16,8},{24,0},{1,25},{9,17},{17,9},{25,1},{2,26},{10... | collective-permute-start | bytes 49160 | tf_op jit(solution)/shard_map/ppermute | solution.py:49
  83.0 1.2 %collective-permute-start.27 = (f32[8,128]{1,0:T(8,128)S(1)}, f32[8,128]{1,0:T(8,128)S(1)}, u32[]{:S(2)}, u32[]{:S(2)}) collective-permute-start(f32[8,128]{1,0:T(8,128)S(1)} %get-tuple-element.62), channel_id=1, source_target_pairs={{0,1},{1,0},{2,3},{3,2},{4,5},{5,4},{6,7},{7,6},{8,9},{9,8},{10,11... | collective-permute-start | bytes 12296 | tf_op jit(solution)/shard_map/ppermute | solution.py:49
  84.2 5.4 %collective-permute-start.30 = (f32[8,128]{1,0:T(8,128)S(1)}, f32[8,128]{1,0:T(8,128)S(1)}, u32[]{:S(2)}, u32[]{:S(2)}) collective-permute-start(f32[8,128]{1,0:T(8,128)S(1)} %add.3.refs_2_), channel_id=1, source_target_pairs={{0,6},{1,7},{2,4},{3,5},{4,2},{5,3},{6,0},{7,1},{8,14},{9,15},{10,... | collective-permute-start | bytes 12296 | tf_op jit(solution)/shard_map/ppermute | solution.py:49
  86.7 4.5 %collective-permute-start.29 = (f32[8,128]{1,0:T(8,128)S(1)}, f32[8,128]{1,0:T(8,128)S(1)}, u32[]{:S(2)}, u32[]{:S(2)}) collective-permute-start(f32[8,128]{1,0:T(8,128)S(1)} %add.3.refs_2_), channel_id=1, source_target_pairs={{0,4},{1,5},{2,6},{3,7},{4,0},{5,1},{6,2},{7,3},{8,12},{9,13},{10,... | collective-permute-start | bytes 12296 | tf_op jit(solution)/shard_map/ppermute | solution.py:49
  86.7 4.5 %collective-permute-start.28 = (f32[8,128]{1,0:T(8,128)S(1)}, f32[8,128]{1,0:T(8,128)S(1)}, u32[]{:S(2)}, u32[]{:S(2)}) collective-permute-start(f32[8,128]{1,0:T(8,128)S(1)} %add.3.refs_2_), channel_id=1, source_target_pairs={{0,2},{1,3},{2,0},{3,1},{4,6},{5,7},{6,4},{7,5},{8,10},{9,11},{10,... | collective-permute-start | bytes 12296 | tf_op jit(solution)/shard_map/ppermute | solution.py:49

commit v4 on v3

--- a/solution.py
+++ b/solution.py
@@ -286,46 +286,12 @@
     sent[1, rows - STATS :, :] = (sums - high.astype(F32)).astype(BF16)
 
 
-def experts_kernel(*refs, ep_count, ratio, width):
-    own = refs[0]
-    arrivals = refs[1:ep_count]
-    pieces = refs[ep_count : 2 * ep_count]
-    (
-        gain_ref,
-        mix_ref,
-        expert_gate,
-        expert_up,
-        dense_gate,
-        dense_up,
-        sent,
-        kept,
-        placed_out,
-        info_out,
-        own_out,
-        full,
-    ) = refs[2 * ep_count :]
+def routing_kernel(*refs, ep_count, local_experts):
+    pieces, placed_out, info_out = refs[:ep_count], refs[-2], refs[-1]
     ep = lax.axis_index("ep")
-    tp = lax.axis_index("tp")
     seq_count = pieces[0].shape[0]
-    total_rows, size = own.shape
-    local_experts = expert_gate.shape[0]
+    slot_count, total_rows = placed_out.shape
     expert_rows = ep_count * CAP
-    slot_count = local_experts * expert_rows
-    distance = ep ^ (tp // ratio)
-    blocks = []
-    for i in range(ep_count):
-        rows = own[i * seq_count : (i + 1) * seq_count, :].astype(F32)
-        rows = jnp.where(distance == 0, rows, 0.0)
-        for d in range(1, ep_count):
-            j = i ^ d
-            rows = rows + arrivals[d - 1][j * seq_count : (j + 1) * seq_count, :].astype(F32)
-        blocks.append(rows)
-    own_out[...] = blocks[0]
-    rows = jnp.concatenate(blocks, axis=0)
-    gain = gain_ref[:, aligned(tp, size)]
-    mix = mix_ref[:, aligned(tp, size)].astype(F32)
-    scaled = rows * gain
-    hidden = scaled.astype(BF16)
 
     block = pieces[0].shape[1] - LANES
     extra = jnp.concatenate([piece[:, block:] for piece in pieces], axis=0).astype(F32)
@@ -364,7 +330,48 @@
         info = jnp.where(info_lane == TOPK + k, weights[k] / weight_sum, info)
     info_out[...] = info
     placed_out[...] = placed
-    routed = jnp.dot(placed.astype(BF16), hidden, preferred_element_type=F32).astype(BF16)
+
+
+def experts_kernel(*refs, ep_count, ratio, width):
+    own = refs[0]
+    arrivals = refs[1:ep_count]
+    (
+        placed,
+        gain_ref,
+        mix_ref,
+        expert_gate,
+        expert_up,
+        dense_gate,
+        dense_up,
+        sent,
+        kept,
+        own_out,
+        full,
+    ) = refs[ep_count:]
+    ep = lax.axis_index("ep")
+    tp = lax.axis_index("tp")
+    total_rows, size = own.shape
+    seq_count = total_rows // ep_count
+    local_experts = expert_gate.shape[0]
+    expert_rows = ep_count * CAP
+    slot_count = local_experts * expert_rows
+    distance = ep ^ (tp // ratio)
+    blocks = []
+    for i in range(ep_count):
+        rows = own[i * seq_count : (i + 1) * seq_count, :].astype(F32)
+        rows = jnp.where(distance == 0, rows, 0.0)
+        for d in range(1, ep_count):
+            j = i ^ d
+            rows = rows + arrivals[d - 1][j * seq_count : (j + 1) * seq_count, :].astype(F32)
+        blocks.append(rows)
+    own_out[...] = blocks[0]
+    rows = jnp.concatenate(blocks, axis=0)
+    gain = gain_ref[:, aligned(tp, size)]
+    mix = mix_ref[:, aligned(tp, size)].astype(F32)
+    scaled = rows * gain
+    hidden = scaled.astype(BF16)
+
+    routed = jnp.dot(placed[...].astype(BF16), hidden, preferred_element_type=F32).astype(BF16)
 
     sums = [
         jnp.sum(rows, axis=1, keepdims=True),
@@ -426,23 +433,40 @@
     return row, column
 
 
-def spread_kernel(kept, got, *refs, bits):
-    outs, full = refs[:-1], refs[-1]
+def low_lane(total_rows):
+    return -(-total_rows // LANES) * LANES
+
+
+def spread_kernel(kept, got, *refs, bits, expert_rows, total_rows):
+    outs, full, tail = refs[:-2], refs[-2], refs[-1]
     full[...] = kept[...] + got[...].astype(F32)
-    rows = full.shape[1] - TAIL
-    piece_rows = outs[0].shape[1] - TAIL
-    width = outs[0].shape[2]
+    slot_count = full.shape[1] - TAIL
+    width = outs[0].shape[1]
+    piece_rows = (outs[0].shape[0] - tail.shape[0]) // 2
+    experts = max(1, piece_rows // expert_rows)
     place = lax.axis_index("tp") >> 1
+    low = low_lane(total_rows)
     for d, out in enumerate(outs):
-        row, column = piece_at(place ^ d, bits, rows, full.shape[2])
+        row, column = piece_at(place ^ d, bits, slot_count, full.shape[2])
         lanes = pl.ds(pl.multiple_of(column, LANES), width)
-        main = full[:, pl.ds(pl.multiple_of(row, 8), piece_rows), lanes]
-        tail = full[:, rows:, lanes]
-        if d == 0:
-            out[:, :piece_rows, :] = main
-            out[:, piece_rows:, :] = tail
+        first = slot_count + row // expert_rows
+        tail[...] = jnp.zeros(tail.shape, F32)
+        for plane in range(2):
+            main = full[plane, pl.ds(pl.multiple_of(row, 8), piece_rows), lanes]
+            out[plane * piece_rows : (plane + 1) * piece_rows, :] = main.astype(out.dtype)
+            for i in range(experts):
+                at = plane * experts + i
+                tail[at : at + 1, :] = full[plane, pl.ds(first + i, 1), lanes]
+        sums = full[:, slot_count + TAIL - STATS :, lanes]
+        sums = (sums[0] + sums[1])[:, :total_rows]
+        rows = slice(2 * experts, 2 * experts + STATS)
+        if d:
+            high = sums.astype(BF16).astype(F32)
+            tail[rows, :total_rows] = high
+            tail[rows, low : low + total_rows] = sums - high
         else:
-            send_part(out, jnp.concatenate([main, tail], axis=1))
+            tail[rows, :total_rows] = sums
+        out[2 * piece_rows :, :] = tail[...].astype(out.dtype)
 
 
 def act_kernel(
@@ -452,12 +476,13 @@
     total = refs[0][...]
     for ref in refs[1:-3]:
         total = total + ref[...].astype(F32)
-    rows = total.shape[1] - TAIL
-    width = total.shape[2]
+    rows, width = act.shape[1:]
     slot_count, total_rows = placed.shape
+    experts = max(1, rows // expert_rows)
     tp = lax.axis_index("tp")
-    sums = total[0, rows + TAIL - STATS :, :] + total[1, rows + TAIL - STATS :, :]
-    sums = sums[:, :total_rows]
+    low = low_lane(total_rows)
+    sums = total[2 * (rows + experts) : 2 * (rows + experts) + STATS, :]
+    sums = sums[:, :total_rows] + sums[:, low : low + total_rows]
     mean = sums[0:1] * (1.0 / model_width)
     variance = sums[1:2] * (1.0 / model_width) - mean * mean
     scale = lax.rsqrt(variance + layer_epsilon)
@@ -479,13 +504,15 @@
         start = first_row + f * slot_count
         scale_used = jnp.where(dense, column_of(scale, start, rows), scale_used)
         mean_used = jnp.where(dense, column_of(mean, start, rows), mean_used)
-    expert = (iota((rows, width), 0) + first_row) // expert_rows
+    expert = iota((rows, width), 0) // expert_rows
     pre = []
     for plane in range(2):
         gain_sum = jnp.zeros((rows, width), F32)
-        for e in range(slot_count // expert_rows):
-            gain_sum = jnp.where(expert == e, total[plane, rows + e : rows + e + 1, :], gain_sum)
-        pre.append(scale_used * (total[plane, :rows, :] - mean_used * gain_sum))
+        for i in range(experts):
+            at = 2 * rows + plane * experts + i
+            gain_sum = jnp.where(expert == i, total[at : at + 1, :], gain_sum)
+        main = total[plane * rows : (plane + 1) * rows, :]
+        pre.append(scale_used * (main - mean_used * gain_sum))
     act[0] = (pre[0] / (1.0 + jnp.exp(-pre[0])) * pre[1]).astype(BF16)
 
 
@@ -699,20 +726,26 @@
     bits = tuple(bits)
     full_rows = slot_count + TAIL
     half = (2, full_rows, width // 2)
-    sent, kept, placed, info, own_rows = call(
+    placed, info = call(
+        routing_kernel,
+        "routing",
+        [((slot_count, total_rows), F32), ((total_rows, LANES), F32)],
+        pieces,
+        ep_count=ep_count,
+        local_experts=local_experts,
+    )
+    sent, kept, own_rows = call(
         experts_kernel,
         "experts",
         [
             (half, BF16),
             (half, F32),
-            ((slot_count, total_rows), F32),
-            ((total_rows, LANES), F32),
             ((seq_count, slice_width), F32),
         ],
         [residual]
         + arrivals
-        + pieces
         + [
+            placed,
             first_gain[None, :],
             dense_mix[None, :],
             expert_gate,
@@ -727,14 +760,17 @@
         width=piece_width,
     )
     got = xor_permute(sent, "tp", tp_count, 1)
-    piece = (2, piece_rows + TAIL, piece_width)
+    piece_tail = -(-(2 * max(1, piece_rows // expert_rows) + STATS) // 8) * 8
+    piece = (2 * piece_rows + piece_tail, piece_width)
     parts = call(
         spread_kernel,
         "spread",
         [(piece, F32)] + [(piece, BF16)] * (place_count - 1),
         [kept, got],
-        scratch=[(half, F32)],
+        scratch=[(half, F32), ((piece_tail, piece_width), F32)],
         bits=bits,
+        expert_rows=expert_rows,
+        total_rows=total_rows,
     )
     parts = [parts[0]] + places_all(parts[1:], tp_count)
     act, stats = call(

time: 92.1 us -> 91.2 us (level)
  waiting for transfers between devices: 40.7 us -> 39.6 us
    pallas_call x13 -> x14, Pallas kernels: 13.3 us -> 13.3 us  [call(): pl.pallas_call(functools.partial(kernel, **sizes), out_shape=[jax.ShapeDt...]
where the time goes in v4:
time: 91.2 us; the launch traced here: 90.9 us
  waiting for transfers between devices  39.6 us (43%)
  starting transfers between devices  37.3 us (41%)
  Pallas kernels  13.3 us (15%)
    ppermute x25, waiting for transfers between devices, xor_permute(): return lax.ppermute(array, axis, [(i, i ^ distance) for i in range(count)])  31.3 us
    ppermute x25, starting transfers between devices, xor_permute(): return lax.ppermute(array, axis, [(i, i ^ distance) for i in range(count)])  29.6 us
    pallas_call x14, Pallas kernels, call(): pl.pallas_call(functools.partial(kernel, **sizes), out_shape=[jax.ShapeDt...  13.3 us
    ppermute x3, waiting for transfers between devices, on_device(): lax.ppermute(part_sum, both, [(device(c, c ^ d, h), device(c, c, h)) for...  6.75 us
    ppermute x3, starting transfers between devices, on_device(): lax.ppermute(residual, both, [(device(c, c, h), device(c ^ d, c, h)) for...  3.88 us
    ppermute x3, starting transfers between devices, on_device(): lax.ppermute(part_sum, both, [(device(c, c ^ d, h), device(c, c, h)) for...  3.88 us
  transfers between devices with their start and end apart: 31, of which 26 were waited for; matrix products, arithmetic and copies ran while one was open for 0% of the time, Pallas kernels for 1%

profile of v4, /device:TPU:0, one launch (start us, length us, event | category | flops | bytes accessed | tf_op | source)
XLA Modules:
  0.0 90.9 jit_solution(17429440180166699992)
XLA Ops:
  0.0 1.2 %prepare.1 = (bf16[16,1152]{1,0:T(8,128)(2,1)S(1)}, bf16[16,1152]{1,0:T(8,128)(2,1)S(1)}, bf16[16,1152]{1,0:T(8,128)(2,1)S(1)}, bf16[16,1152]{1,0:T(8,128)(2,1)S(1)}) custom-call(bf16[16,4096]{1,0:T(8,128)(2,1)} %tokens.1, s32[2,16]{1,0:T(2,128)} %bitcast.19, f32[2,16]{1,0:T(2,128)} %bitcast.20), custom_call_target="tpu_custom_call" | custom-call | flops 20000000000 | bytes 20000000000 | tf_op jit(solution)/shard_map/prepare/pallas_call | solution.py:36
  1.2 3.0 %collective-permute-start = (bf16[16,1152]{1,0:T(8,128)(2,1)S(1)}, bf16[16,1152]{1,0:T(8,128)(2,1)S(1)}, u32[]{:S(2)}, u32[]{:S(2)}) collective-permute-start(bf16[16,1152]{1,0:T(8,128)(2,1)S(1)} %get-tuple-element.35), channel_id=1, source_target_pairs={{0,8},{8,0},{16,24},{24,16},{1,9},{9,1},{17,25},{25,17},{2,10},{10... | collective-permute-start | bytes 110600 | tf_op jit(solution)/shard_map/ppermute | solution.py:49
  4.3 1.5 %collective-permute-start.1 = (bf16[16,1152]{1,0:T(8,128)(2,1)S(1)}, bf16[16,1152]{1,0:T(8,128)(2,1)S(1)}, u32[]{:S(2)}, u32[]{:S(2)}) collective-permute-start(bf16[16,1152]{1,0:T(8,128)(2,1)S(1)} %get-tuple-element.36), channel_id=1, source_target_pairs={{0,16},{8,24},{16,0},{24,8},{1,17},{9,25},{17,1},{25,9},{2,18},{10... | collective-permute-start | bytes 110600 | tf_op jit(solution)/shard_map/ppermute | solution.py:49
  5.8 0.4 collective-permute-done.refs_1_.refs_5_
  6.2 2.0 %collective-permute-done.1.refs_2_.refs_6_ = bf16[16,1152]{1,0:T(8,128)(2,1)S(1)} collective-permute-done((bf16[16,1152]{1,0:T(8,128)(2,1)S(1)}, bf16[16,1152]{1,0:T(8,128)(2,1)S(1)}, u32[]{:S(2)}, u32[]{:S(2)}) %collective-permute-start.1) | collective-permute-done | bytes 36896 | tf_op jit(solution)/shard_map/ppermute | solution.py:49
  8.2 2.4 %collective-permute-done.2.refs_3_.refs_7_ = bf16[16,1152]{1,0:T(8,128)(2,1)S(1)} collective-permute-done((bf16[16,1152]{1,0:T(8,128)(2,1)S(1)}, bf16[16,1152]{1,0:T(8,128)(2,1)S(1)}, u32[]{:S(2)}, u32[]{:S(2)}) %collective-permute-start.2) | collective-permute-done | bytes 36896 | tf_op jit(solution)/shard_map/ppermute | solution.py:49
  10.7 0.5 project.1
  11.2 0.6 collective-permute-start.3
  11.8 2.9 %collective-permute-start.5 = (bf16[16,1024]{1,0:T(8,128)(2,1)S(1)}, bf16[16,1024]{1,0:T(8,128)(2,1)S(1)}, u32[]{:S(2)}, u32[]{:S(2)}) collective-permute-start(bf16[16,1024]{1,0:T(8,128)(2,1)S(1)} %get-tuple-element.41), channel_id=1, source_target_pairs={{0,24},{8,16},{16,8},{24,0},{1,25},{9,17},{17,9},{25,1},{2,26},{10... | collective-permute-start | bytes 98312 | tf_op jit(solution)/shard_map/ppermute | solution.py:49
  14.7 0.6 tables.1
  15.4 0.3 collective-permute-done.4.refs_2_
  15.7 0.9 %collective-permute-done.5.refs_3_ = bf16[16,1024]{1,0:T(8,128)(2,1)S(1)} collective-permute-done((bf16[16,1024]{1,0:T(8,128)(2,1)S(1)}, bf16[16,1024]{1,0:T(8,128)(2,1)S(1)}, u32[]{:S(2)}, u32[]{:S(2)}) %collective-permute-start.5) | collective-permute-done | bytes 32800 | tf_op jit(solution)/shard_map/ppermute | solution.py:49
  16.8 4.4 %attend.1.refs_0_ = bf16[16,512]{1,0:T(8,128)(2,1)S(1)} custom-call(s32[16]{0:T(128)S(1)} %copy-done.11, f32[4]{0:T(128)S(1)} %copy-done.12, f32[16,1024]{1,0:T(8,128)S(1)} %get-tuple-element.38.refs_0_, bf16[16,1024]{1,0:T(8,128)(2,1)S(1)} %collective-permute-done.3.refs_1_, bf16[16,1024]{1,0:T(8,128)(2,1)S(1)} %collective-permute-done.4.refs_2_, ...), custom_call_target="tpu_custom_call" | custom-call | flops 20000000000 | bytes 20000000000 | tf_op jit(solution)/shard_map/attend/pallas_call | solution.py:36
  21.1 3.0 %collective-permute-start.8 = (bf16[16,512]{1,0:T(8,128)(2,1)S(1)}, bf16[16,512]{1,0:T(8,128)(2,1)S(1)}, u32[]{:S(2)}, u32[]{:S(2)}) collective-permute-start(bf16[16,512]{1,0:T(8,128)(2,1)S(1)} %attend.1.refs_0_), channel_id=1, source_target_pairs={{0,24},{8,16},{16,8},{24,0},{1,25},{9,17},{17,9},{25,1},{2,26},{10... | collective-permute-start | bytes 49160 | tf_op jit(solution)/shard_map/ppermute | solution.py:49
  24.1 0.5 collective-permute-start.7
  24.6 0.1 collective-permute-start.6
  24.7 1.1 %collective-permute-done.8.refs_3_ = bf16[16,512]{1,0:T(8,128)(2,1)S(1)} collective-permute-done((bf16[16,512]{1,0:T(8,128)(2,1)S(1)}, bf16[16,512]{1,0:T(8,128)(2,1)S(1)}, u32[]{:S(2)}, u32[]{:S(2)}) %collective-permute-start.8) | collective-permute-done | bytes 16416 | tf_op jit(solution)/shard_map/ppermute | solution.py:49
  25.8 2.0 %collective-permute-done.7.refs_2_ = bf16[16,512]{1,0:T(8,128)(2,1)S(1)} collective-permute-done((bf16[16,512]{1,0:T(8,128)(2,1)S(1)}, bf16[16,512]{1,0:T(8,128)(2,1)S(1)}, u32[]{:S(2)}, u32[]{:S(2)}) %collective-permute-start.7) | collective-permute-done | bytes 16416 | tf_op jit(solution)/shard_map/ppermute | solution.py:49
  27.8 0.5 collective-permute-done.6.refs_1_
  28.3 0.3 outproj.1
  28.7 1.2 %collective-permute-done.9.refs_1_ = bf16[64,512]{1,0:T(8,128)(2,1)S(1)} collective-permute-done((bf16[64,512]{1,0:T(8,128)(2,1)S(1)}, bf16[64,512]{1,0:T(8,128)(2,1)S(1)}, u32[]{:S(2)}, u32[]{:S(2)}) %collective-permute-start.9) | collective-permute-done | bytes 65568 | tf_op jit(solution)/shard_map/ppermute | solution.py:49
  30.0 1.3 %collective-permute-start.12 = (bf16[64,512]{1,0:T(8,128)(2,1)S(1)}, bf16[64,512]{1,0:T(8,128)(2,1)S(1)}, u32[]{:S(2)}, u32[]{:S(2)}) collective-permute-start(bf16[64,512]{1,0:T(8,128)(2,1)S(1)} %pairsum.1.refs_0_), channel_id=1, source_target_pairs={{6,0},{7,1},{12,10},{13,11},{18,20},{19,21},{24,30},{25,31}} | collective-permute-start | bytes 196616 | tf_op jit(solution)/shard_map/ppermute | solution.py:700
  31.3 1.3 %collective-permute-start.11 = (bf16[64,512]{1,0:T(8,128)(2,1)S(1)}, bf16[64,512]{1,0:T(8,128)(2,1)S(1)}, u32[]{:S(2)}, u32[]{:S(2)}) collective-permute-start(bf16[64,512]{1,0:T(8,128)(2,1)S(1)} %pairsum.1.refs_0_), channel_id=1, source_target_pairs={{4,0},{5,1},{14,10},{15,11},{16,20},{17,21},{26,30},{27,31}} | collective-permute-start | bytes 196616 | tf_op jit(solution)/shard_map/ppermute | solution.py:700
  32.6 1.3 %collective-permute-start.10 = (bf16[64,512]{1,0:T(8,128)(2,1)S(1)}, bf16[64,512]{1,0:T(8,128)(2,1)S(1)}, u32[]{:S(2)}, u32[]{:S(2)}) collective-permute-start(bf16[64,512]{1,0:T(8,128)(2,1)S(1)} %pairsum.1.refs_0_), channel_id=1, source_target_pairs={{2,0},{3,1},{8,10},{9,11},{22,20},{23,21},{28,30},{29,31}} | collective-permute-start | bytes 196616 | tf_op jit(solution)/shard_map/ppermute | solution.py:700
  33.9 4.1 %collective-permute-done.12.refs_3_ = bf16[64,512]{1,0:T(8,128)(2,1)S(1)} collective-permute-done((bf16[64,512]{1,0:T(8,128)(2,1)S(1)}, bf16[64,512]{1,0:T(8,128)(2,1)S(1)}, u32[]{:S(2)}, u32[]{:S(2)}) %collective-permute-start.12) | collective-permute-done | bytes 65568 | tf_op jit(solution)/shard_map/ppermute | solution.py:700
  38.0 1.3 %collective-permute-done.11.refs_2_ = bf16[64,512]{1,0:T(8,128)(2,1)S(1)} collective-permute-done((bf16[64,512]{1,0:T(8,128)(2,1)S(1)}, bf16[64,512]{1,0:T(8,128)(2,1)S(1)}, u32[]{:S(2)}, u32[]{:S(2)}) %collective-permute-start.11) | collective-permute-done | bytes 65568 | tf_op jit(solution)/shard_map/ppermute | solution.py:700
  39.4 1.3 %collective-permute-done.10.refs_1_ = bf16[64,512]{1,0:T(8,128)(2,1)S(1)} collective-permute-done((bf16[64,512]{1,0:T(8,128)(2,1)S(1)}, bf16[64,512]{1,0:T(8,128)(2,1)S(1)}, u32[]{:S(2)}, u32[]{:S(2)}) %collective-permute-start.10) | collective-permute-done | bytes 65568 | tf_op jit(solution)/shard_map/ppermute | solution.py:700
  40.7 0.2 residual.1.refs_0_
  40.8 1.3 %collective-permute-start.15 = (bf16[64,512]{1,0:T(8,128)(2,1)S(1)}, bf16[64,512]{1,0:T(8,128)(2,1)S(1)}, u32[]{:S(2)}, u32[]{:S(2)}) collective-permute-start(bf16[64,512]{1,0:T(8,128)(2,1)S(1)} %residual.1.refs_0_), channel_id=1, source_target_pairs={{0,24},{1,25},{10,18},{11,19},{20,12},{21,13},{30,6},{31,7}} | collective-permute-start | bytes 196616 | tf_op jit(solution)/shard_map/ppermute | solution.py:712
  42.1 1.3 %collective-permute-start.14 = (bf16[64,512]{1,0:T(8,128)(2,1)S(1)}, bf16[64,512]{1,0:T(8,128)(2,1)S(1)}, u32[]{:S(2)}, u32[]{:S(2)}) collective-permute-start(bf16[64,512]{1,0:T(8,128)(2,1)S(1)} %residual.1.refs_0_), channel_id=1, source_target_pairs={{0,16},{1,17},{10,26},{11,27},{20,4},{21,5},{30,14},{31,15}} | collective-permute-start | bytes 196616 | tf_op jit(solution)/shard_map/ppermute | solution.py:712
  43.4 1.3 %collective-permute-start.13 = (bf16[64,512]{1,0:T(8,128)(2,1)S(1)}, bf16[64,512]{1,0:T(8,128)(2,1)S(1)}, u32[]{:S(2)}, u32[]{:S(2)}) collective-permute-start(bf16[64,512]{1,0:T(8,128)(2,1)S(1)} %residual.1.refs_0_), channel_id=1, source_target_pairs={{0,8},{1,9},{10,2},{11,3},{20,28},{21,29},{30,22},{31,23}} | collective-permute-start | bytes 196616 | tf_op jit(solution)/shard_map/ppermute | solution.py:712
  44.8 0.3 routing.1
  45.1 0.2 collective-permute-done.14.refs_2_
  45.3 1.3 %collective-permute-done.13.refs_1_ = bf16[64,512]{1,0:T(8,128)(2,1)S(1)} collective-permute-done((bf16[64,512]{1,0:T(8,128)(2,1)S(1)}, bf16[64,512]{1,0:T(8,128)(2,1)S(1)}, u32[]{:S(2)}, u32[]{:S(2)}) %collective-permute-start.13) | collective-permute-done | bytes 65568 | tf_op jit(solution)/shard_map/ppermute | solution.py:712
  46.7 3.4 %experts.1 = (bf16[2,72,1280]{2,1,0:T(8,128)(2,1)S(1)}, f32[2,72,1280]{2,1,0:T(8,128)S(1)}, f32[16,512]{1,0:T(8,128)S(1)}) custom-call(bf16[64,512]{1,0:T(8,128)(2,1)S(1)} %residual.1.refs_0_, bf16[64,512]{1,0:T(8,128)(2,1)S(1)} %collective-permute-done.13.refs_1_, bf16[64,512]{1,0:T(8,128)(2,1)S(1)} %collective-permute-done.14.refs_2_, ...), custom_call_target="tpu_custom_call" | custom-call | tf_op jit(solution)/shard_map/experts/pallas_call | solution.py:36
  50.1 0.1 collective-permute-start.16
  50.2 1.7 %collective-permute-done.16.got = bf16[2,72,1280]{2,1,0:T(8,128)(2,1)S(1)} collective-permute-done((bf16[2,72,1280]{2,1,0:T(8,128)(2,1)S(1)}, bf16[2,72,1280]{2,1,0:T(8,128)(2,1)S(1)}, u32[]{:S(2)}, u32[]{:S(2)}) %collective-permute-start.16) | collective-permute-done | bytes 368672 | tf_op jit(solution)/shard_map/ppermute | solution.py:49
  51.9 0.2 spread.1
  52.1 1.9 %collective-permute-start.17 = (bf16[72,640]{1,0:T(8,128)(2,1)S(1)}, bf16[72,640]{1,0:T(8,128)(2,1)S(1)}, u32[]{:S(2)}, u32[]{:S(2)}) collective-permute-start(bf16[72,640]{1,0:T(8,128)(2,1)S(1)} %get-tuple-element.50), channel_id=1, source_target_pairs={{0,2},{1,3},{2,0},{3,1},{4,6},{5,7},{6,4},{7,5},{8,10},{9,11},{10,... | collective-permute-start | bytes 276488 | tf_op jit(solution)/shard_map/ppermute | solution.py:49
  54.0 1.7 %collective-permute-start.18 = (bf16[72,640]{1,0:T(8,128)(2,1)S(1)}, bf16[72,640]{1,0:T(8,128)(2,1)S(1)}, u32[]{:S(2)}, u32[]{:S(2)}) collective-permute-start(bf16[72,640]{1,0:T(8,128)(2,1)S(1)} %get-tuple-element.51), channel_id=1, source_target_pairs={{0,4},{1,5},{2,6},{3,7},{4,0},{5,1},{6,2},{7,3},{8,12},{9,13},{10,... | collective-permute-start | bytes 276488 | tf_op jit(solution)/shard_map/ppermute | solution.py:49
  55.6 0.9 %collective-permute-start.19 = (bf16[72,640]{1,0:T(8,128)(2,1)S(1)}, bf16[72,640]{1,0:T(8,128)(2,1)S(1)}, u32[]{:S(2)}, u32[]{:S(2)}) collective-permute-start(bf16[72,640]{1,0:T(8,128)(2,1)S(1)} %get-tuple-element.52), channel_id=1, source_target_pairs={{0,6},{1,7},{2,4},{3,5},{4,2},{5,3},{6,0},{7,1},{8,14},{9,15},{10,... | collective-permute-start | bytes 276488 | tf_op jit(solution)/shard_map/ppermute | solution.py:49
  56.5 0.4 collective-permute-done.17.refs_1_
  56.9 6.9 %collective-permute-done.18.refs_2_ = bf16[72,640]{1,0:T(8,128)(2,1)S(1)} collective-permute-done((bf16[72,640]{1,0:T(8,128)(2,1)S(1)}, bf16[72,640]{1,0:T(8,128)(2,1)S(1)}, u32[]{:S(2)}, u32[]{:S(2)}) %collective-permute-start.18) | collective-permute-done | bytes 92192 | tf_op jit(solution)/shard_map/ppermute | solution.py:49
  63.9 0.1 act.1
  64.0 1.8 %collective-permute-start.22 = (bf16[1,32,640]{2,1,0:T(8,128)(2,1)S(1)}, bf16[1,32,640]{2,1,0:T(8,128)(2,1)S(1)}, u32[]{:S(2)}, u32[]{:S(2)}) collective-permute-start(bf16[1,32,640]{2,1,0:T(8,128)(2,1)S(1)} %get-tuple-element.53), channel_id=1, source_target_pairs={{0,6},{1,7},{2,4},{3,5},{4,2},{5,3},{6,0},{7,1},{8,14},{9,15},{10,... | collective-permute-start | bytes 122888 | tf_op jit(solution)/shard_map/ppermute | solution.py:49
  65.8 1.7 %collective-permute-start.21 = (bf16[1,32,640]{2,1,0:T(8,128)(2,1)S(1)}, bf16[1,32,640]{2,1,0:T(8,128)(2,1)S(1)}, u32[]{:S(2)}, u32[]{:S(2)}) collective-permute-start(bf16[1,32,640]{2,1,0:T(8,128)(2,1)S(1)} %get-tuple-element.53), channel_id=1, source_target_pairs={{0,4},{1,5},{2,6},{3,7},{4,0},{5,1},{6,2},{7,3},{8,12},{9,13},{10,... | collective-permute-start | bytes 122888 | tf_op jit(solution)/shard_map/ppermute | solution.py:49
  67.4 1.0 %collective-permute-start.20 = (bf16[1,32,640]{2,1,0:T(8,128)(2,1)S(1)}, bf16[1,32,640]{2,1,0:T(8,128)(2,1)S(1)}, u32[]{:S(2)}, u32[]{:S(2)}) collective-permute-start(bf16[1,32,640]{2,1,0:T(8,128)(2,1)S(1)} %get-tuple-element.53), channel_id=1, source_target_pairs={{0,2},{1,3},{2,0},{3,1},{4,6},{5,7},{6,4},{7,5},{8,10},{9,11},{10,... | collective-permute-start | bytes 122888 | tf_op jit(solution)/shard_map/ppermute | solution.py:49
  68.5 1.4 %collective-permute-done.22 = bf16[1,32,640]{2,1,0:T(8,128)(2,1)S(1)} collective-permute-done((bf16[1,32,640]{2,1,0:T(8,128)(2,1)S(1)}, bf16[1,32,640]{2,1,0:T(8,128)(2,1)S(1)}, u32[]{:S(2)}, u32[]{:S(2)}) %collective-permute-start.22) | collective-permute-done | bytes 40992 | tf_op jit(solution)/shard_map/ppermute | solution.py:49
  69.9 1.3 %collective-permute-done.21 = bf16[1,32,640]{2,1,0:T(8,128)(2,1)S(1)} collective-permute-done((bf16[1,32,640]{2,1,0:T(8,128)(2,1)S(1)}, bf16[1,32,640]{2,1,0:T(8,128)(2,1)S(1)}, u32[]{:S(2)}, u32[]{:S(2)}) %collective-permute-start.21) | collective-permute-done | bytes 40992 | tf_op jit(solution)/shard_map/ppermute | solution.py:49
  71.2 0.3 collective-permute-done.20
  71.7 1.3 %collective-permute-done.23 = bf16[4,32,640]{2,1,0:T(8,128)(2,1)S(1)} collective-permute-done((bf16[4,32,640]{2,1,0:T(8,128)(2,1)S(1)}, bf16[4,32,640]{2,1,0:T(8,128)(2,1)S(1)}, u32[]{:S(2)}, u32[]{:S(2)}) %collective-permute-start.23) | collective-permute-done | bytes 163872 | tf_op jit(solution)/shard_map/ppermute | solution.py:49
  73.1 1.4 %down.1 = (f32[16,512]{1,0:T(8,128)S(1)}, bf16[16,512]{1,0:T(8,128)(2,1)S(1)}, bf16[16,512]{1,0:T(8,128)(2,1)S(1)}, bf16[16,512]{1,0:T(8,128)(2,1)S(1)}) custom-call(bf16[8,32,640]{2,1,0:T(8,128)(2,1)S(1)} %constant_dynamic-update-slice_fusion.acts, f32[8,64]{1,0:T(8,128)S(1)} %get-tuple-element.54.stats, f32[64,128]{1,0:T(8,128)S(1)} %get-tuple-element.55.info, ...), custom_call_target="tpu_custom_call" | custom-call | tf_op jit(solution)/shard_map/down/pallas_call | solution.py:36
  74.5 1.5 %collective-permute-start.24 = (bf16[16,512]{1,0:T(8,128)(2,1)S(1)}, bf16[16,512]{1,0:T(8,128)(2,1)S(1)}, u32[]{:S(2)}, u32[]{:S(2)}) collective-permute-start(bf16[16,512]{1,0:T(8,128)(2,1)S(1)} %get-tuple-element.58), channel_id=1, source_target_pairs={{0,8},{8,0},{16,24},{24,16},{1,9},{9,1},{17,25},{25,17},{2,10},{10... | collective-permute-start | bytes 49160 | tf_op jit(solution)/shard_map/ppermute | solution.py:49
  76.0 1.4 %collective-permute-start.25 = (bf16[16,512]{1,0:T(8,128)(2,1)S(1)}, bf16[16,512]{1,0:T(8,128)(2,1)S(1)}, u32[]{:S(2)}, u32[]{:S(2)}) collective-permute-start(bf16[16,512]{1,0:T(8,128)(2,1)S(1)} %get-tuple-element.59), channel_id=1, source_target_pairs={{0,16},{8,24},{16,0},{24,8},{1,17},{9,25},{17,1},{25,9},{2,18},{10... | collective-permute-start | bytes 49160 | tf_op jit(solution)/shard_map/ppermute | solution.py:49
  77.3 1.4 %collective-permute-start.26 = (bf16[16,512]{1,0:T(8,128)(2,1)S(1)}, bf16[16,512]{1,0:T(8,128)(2,1)S(1)}, u32[]{:S(2)}, u32[]{:S(2)}) collective-permute-start(bf16[16,512]{1,0:T(8,128)(2,1)S(1)} %get-tuple-element.60), channel_id=1, source_target_pairs={{0,24},{8,16},{16,8},{24,0},{1,25},{9,17},{17,9},{25,1},{2,26},{10... | collective-permute-start | bytes 49160 | tf_op jit(solution)/shard_map/ppermute | solution.py:49
  78.7 1.0 %collective-permute-done.25.refs_2_ = bf16[16,512]{1,0:T(8,128)(2,1)S(1)} collective-permute-done((bf16[16,512]{1,0:T(8,128)(2,1)S(1)}, bf16[16,512]{1,0:T(8,128)(2,1)S(1)}, u32[]{:S(2)}, u32[]{:S(2)}) %collective-permute-start.25) | collective-permute-done | bytes 16416 | tf_op jit(solution)/shard_map/ppermute | solution.py:49
  79.7 2.3 %collective-permute-done.26.refs_3_ = bf16[16,512]{1,0:T(8,128)(2,1)S(1)} collective-permute-done((bf16[16,512]{1,0:T(8,128)(2,1)S(1)}, bf16[16,512]{1,0:T(8,128)(2,1)S(1)}, u32[]{:S(2)}, u32[]{:S(2)}) %collective-permute-start.26) | collective-permute-done | bytes 16416 | tf_op jit(solution)/shard_map/ppermute | solution.py:49
  82.0 0.1 combine.1
  82.2 1.2 %collective-permute-done.27 = f32[8,128]{1,0:T(8,128)S(1)} collective-permute-done((f32[8,128]{1,0:T(8,128)S(1)}, f32[8,128]{1,0:T(8,128)S(1)}, u32[]{:S(2)}, u32[]{:S(2)}) %collective-permute-start.27) | collective-permute-done | bytes 4128 | tf_op jit(solution)/shard_map/ppermute | solution.py:49
  83.3 2.4 %collective-permute-start.30 = (f32[8,128]{1,0:T(8,128)S(1)}, f32[8,128]{1,0:T(8,128)S(1)}, u32[]{:S(2)}, u32[]{:S(2)}) collective-permute-start(f32[8,128]{1,0:T(8,128)S(1)} %add.3.refs_2_), channel_id=1, source_target_pairs={{0,6},{1,7},{2,4},{3,5},{4,2},{5,3},{6,0},{7,1},{8,14},{9,15},{10,... | collective-permute-start | bytes 12296 | tf_op jit(solution)/shard_map/ppermute | solution.py:49
  85.7 2.0 %collective-permute-start.28 = (f32[8,128]{1,0:T(8,128)S(1)}, f32[8,128]{1,0:T(8,128)S(1)}, u32[]{:S(2)}, u32[]{:S(2)}) collective-permute-start(f32[8,128]{1,0:T(8,128)S(1)} %add.3.refs_2_), channel_id=1, source_target_pairs={{0,2},{1,3},{2,0},{3,1},{4,6},{5,7},{6,4},{7,5},{8,10},{9,11},{10,... | collective-permute-start | bytes 12296 | tf_op jit(solution)/shard_map/ppermute | solution.py:49
  87.7 1.0 %collective-permute-done.30.refs_5_ = f32[8,128]{1,0:T(8,128)S(1)} collective-permute-done((f32[8,128]{1,0:T(8,128)S(1)}, f32[8,128]{1,0:T(8,128)S(1)}, u32[]{:S(2)}, u32[]{:S(2)}) %collective-permute-start.30) | collective-permute-done | bytes 4128 | tf_op jit(solution)/shard_map/ppermute | solution.py:49
  88.7 1.5 %collective-permute-done.29.refs_4_ = f32[8,128]{1,0:T(8,128)S(1)} collective-permute-done((f32[8,128]{1,0:T(8,128)S(1)}, f32[8,128]{1,0:T(8,128)S(1)}, u32[]{:S(2)}, u32[]{:S(2)}) %collective-permute-start.29) | collective-permute-done | bytes 4128 | tf_op jit(solution)/shard_map/ppermute | solution.py:49
  90.2 0.7 norm.1
  (65 shorter events, 0.5 us)
Async XLA Ops:
  0.0 10.7 %copy-start = (bf16[1024,512]{1,0:T(8,128)(2,1)S(1)}, bf16[1024,512]{1,0:T(8,128)(2,1)}, u32[]{:S(2)}) copy-start(bf16[1024,512]{1,0:T(8,128)(2,1)} %refs_4_.2) | copy-start | bytes 3145732
  0.0 10.7 %copy-start.2 = (bf16[1024,256]{1,0:T(8,128)(2,1)S(1)}, bf16[1024,256]{1,0:T(8,128)(2,1)}, u32[]{:S(2)}) copy-start(bf16[1024,256]{1,0:T(8,128)(2,1)} %refs_5_.1) | copy-start | bytes 1572868
  0.0 10.7 %copy-start.3 = (bf16[1024,256]{1,0:T(8,128)(2,1)S(1)}, bf16[1024,256]{1,0:T(8,128)(2,1)}, u32[]{:S(2)}) copy-start(bf16[1024,256]{1,0:T(8,128)(2,1)} %refs_6_.1) | copy-start | bytes 1572868
  0.0 14.7 %copy-start.11 = (s32[16]{0:T(128)S(1)}, s32[16]{0:T(128)}, u32[]{:S(2)}) copy-start(s32[16]{0:T(128)} %lengths.3) | copy-start | bytes 196
  0.0 16.6 %copy-start.9 = (bf16[16,1024,2,128]{3,2,1,0:T(2,128)(2,1)S(1)}, bf16[16,1024,2,128]{3,2,1,0:T(2,128)(2,1)}, u32[]{:S(2)}) copy-start(bf16[16,1024,2,128]{3,2,1,0:T(2,128)(2,1)} %param.28) | copy-start | bytes 25165828
  0.0 16.6 %copy-start.10 = (bf16[16,1024,2,128]{3,2,1,0:T(2,128)(2,1)S(1)}, bf16[16,1024,2,128]{3,2,1,0:T(2,128)(2,1)}, u32[]{:S(2)}) copy-start(bf16[16,1024,2,128]{3,2,1,0:T(2,128)(2,1)} %param.29) | copy-start | bytes 25165828
  0.0 16.6 %copy-start.12 = (f32[4]{0:T(128)S(1)}, f32[4]{0:T(128)}, u32[]{:S(2)}) copy-start(f32[4]{0:T(128)} %lambdas.1) | copy-start | bytes 52
  0.0 16.6 %copy-start.13 = (f32[128]{0:T(128)S(1)}, f32[128]{0:T(128)}, u32[]{:S(2)}) copy-start(f32[128]{0:T(128)} %param.27) | copy-start | bytes 1540
  1.2 5.0 %collective-permute-start = (bf16[16,1152]{1,0:T(8,128)(2,1)S(1)}, bf16[16,1152]{1,0:T(8,128)(2,1)S(1)}, u32[]{:S(2)}, u32[]{:S(2)}) collective-permute-start(bf16[16,1152]{1,0:T(8,128)(2,1)S(1)} %get-tuple-element.35), channel_id=1, source_target_pairs={{0,8},{8,0},{16,24},{24,16},{1,9},{9,1},{17,25},{25,17},{2,10},{10... | collective-permute-start | bytes 110600 | tf_op jit(solution)/shard_map/ppermute | solution.py:49
  4.3 4.0 %collective-permute-start.1 = (bf16[16,1152]{1,0:T(8,128)(2,1)S(1)}, bf16[16,1152]{1,0:T(8,128)(2,1)S(1)}, u32[]{:S(2)}, u32[]{:S(2)}) collective-permute-start(bf16[16,1152]{1,0:T(8,128)(2,1)S(1)} %get-tuple-element.36), channel_id=1, source_target_pairs={{0,16},{8,24},{16,0},{24,8},{1,17},{9,25},{17,1},{25,9},{2,18},{10... | collective-permute-start | bytes 110600 | tf_op jit(solution)/shard_map/ppermute | solution.py:49
  5.8 4.9 %collective-permute-start.2 = (bf16[16,1152]{1,0:T(8,128)(2,1)S(1)}, bf16[16,1152]{1,0:T(8,128)(2,1)S(1)}, u32[]{:S(2)}, u32[]{:S(2)}) collective-permute-start(bf16[16,1152]{1,0:T(8,128)(2,1)S(1)} %get-tuple-element.37), channel_id=1, source_target_pairs={{0,24},{8,16},{16,8},{24,0},{1,25},{9,17},{17,9},{25,1},{2,26},{10... | collective-permute-start | bytes 110600 | tf_op jit(solution)/shard_map/ppermute | solution.py:49
  10.7 35.9 %slice-start = ((s8[8388608]{0:T(1024)(128)(4,1)}), s8[4194304]{0:T(1024)(128)(4,1)S(1)}, s32[]{:S(2)}) async-start(s8[8388608]{0:T(1024)(128)(4,1)} %bitcast.7), calls=%async_computation | async-start | bytes 8388608
  10.7 35.9 %slice-start.2 = ((s8[8388608]{0:T(1024)(128)(4,1)}), s8[4194304]{0:T(1024)(128)(4,1)S(1)}, s32[]{:S(2)}) async-start(s8[8388608]{0:T(1024)(128)(4,1)} %bitcast.9), calls=%async_computation.2 | async-start | bytes 8388608
  11.2 4.2 %collective-permute-start.3 = (bf16[16,1024]{1,0:T(8,128)(2,1)S(1)}, bf16[16,1024]{1,0:T(8,128)(2,1)S(1)}, u32[]{:S(2)}, u32[]{:S(2)}) collective-permute-start(bf16[16,1024]{1,0:T(8,128)(2,1)S(1)} %get-tuple-element.39), channel_id=1, source_target_pairs={{0,8},{8,0},{16,24},{24,16},{1,9},{9,1},{17,25},{25,17},{2,10},{10... | collective-permute-start | bytes 98312 | tf_op jit(solution)/shard_map/ppermute | solution.py:49
  11.8 3.9 %collective-permute-start.4 = (bf16[16,1024]{1,0:T(8,128)(2,1)S(1)}, bf16[16,1024]{1,0:T(8,128)(2,1)S(1)}, u32[]{:S(2)}, u32[]{:S(2)}) collective-permute-start(bf16[16,1024]{1,0:T(8,128)(2,1)S(1)} %get-tuple-element.40), channel_id=1, source_target_pairs={{0,16},{8,24},{16,0},{24,8},{1,17},{9,25},{17,1},{25,9},{2,18},{10... | collective-permute-start | bytes 98312 | tf_op jit(solution)/shard_map/ppermute | solution.py:49
  11.8 4.8 %collective-permute-start.5 = (bf16[16,1024]{1,0:T(8,128)(2,1)S(1)}, bf16[16,1024]{1,0:T(8,128)(2,1)S(1)}, u32[]{:S(2)}, u32[]{:S(2)}) collective-permute-start(bf16[16,1024]{1,0:T(8,128)(2,1)S(1)} %get-tuple-element.41), channel_id=1, source_target_pairs={{0,24},{8,16},{16,8},{24,0},{1,25},{9,17},{17,9},{25,1},{2,26},{10... | collective-permute-start | bytes 98312 | tf_op jit(solution)/shard_map/ppermute | solution.py:49
  16.7 11.7 %copy-start.1 = (bf16[512,1024]{1,0:T(8,128)(2,1)S(1)}, bf16[512,1024]{1,0:T(8,128)(2,1)}, u32[]{:S(2)}) copy-start(bf16[512,1024]{1,0:T(8,128)(2,1)} %refs_4_.3) | copy-start | bytes 3145732
  16.7 28.1 %copy-start.14 = (bf16[4096]{0:T(1024)(128)(2,1)S(1)}, bf16[4096]{0:T(1024)(128)(2,1)}, u32[]{:S(2)}) copy-start(bf16[4096]{0:T(1024)(128)(2,1)} %param.41) | copy-start | bytes 24580
  16.7 29.9 %slice-start.1 = ((s8[8388608]{0:T(1024)(128)(4,1)}), s8[4194304]{0:T(1024)(128)(4,1)S(1)}, s32[]{:S(2)}) async-start(s8[8388608]{0:T(1024)(128)(4,1)} %bitcast.7), calls=%async_computation.1 | async-start | bytes 8388608
  16.7 29.9 %slice-start.3 = ((s8[8388608]{0:T(1024)(128)(4,1)}), s8[4194304]{0:T(1024)(128)(4,1)S(1)}, s32[]{:S(2)}) async-start(s8[8388608]{0:T(1024)(128)(4,1)} %bitcast.9), calls=%async_computation.3 | async-start | bytes 8388608
  16.7 29.9 %copy-start.4 = (bf16[512,512]{1,0:T(8,128)(2,1)S(1)}, bf16[512,512]{1,0:T(8,128)(2,1)}, u32[]{:S(2)}) copy-start(bf16[512,512]{1,0:T(8,128)(2,1)} %refs_9_.1) | copy-start | bytes 1572868
  16.7 29.9 %copy-start.5 = (bf16[512,512]{1,0:T(8,128)(2,1)S(1)}, bf16[512,512]{1,0:T(8,128)(2,1)}, u32[]{:S(2)}) copy-start(bf16[512,512]{1,0:T(8,128)(2,1)} %refs_10_.1) | copy-start | bytes 1572868
  16.7 29.9 %copy-start.7 = (f32[4096]{0:T(1024)S(1)}, f32[4096]{0:T(1024)}, u32[]{:S(2)}) copy-start(f32[4096]{0:T(1024)} %param.31) | copy-start | bytes 49156
  21.1 4.7 %collective-permute-start.8 = (bf16[16,512]{1,0:T(8,128)(2,1)S(1)}, bf16[16,512]{1,0:T(8,128)(2,1)S(1)}, u32[]{:S(2)}, u32[]{:S(2)}) collective-permute-start(bf16[16,512]{1,0:T(8,128)(2,1)S(1)} %attend.1.refs_0_), channel_id=1, source_target_pairs={{0,24},{8,16},{16,8},{24,0},{1,25},{9,17},{17,9},{25,1},{2,26},{10... | collective-permute-start | bytes 49160 | tf_op jit(solution)/shard_map/ppermute | solution.py:49
  24.1 3.7 %collective-permute-start.7 = (bf16[16,512]{1,0:T(8,128)(2,1)S(1)}, bf16[16,512]{1,0:T(8,128)(2,1)S(1)}, u32[]{:S(2)}, u32[]{:S(2)}) collective-permute-start(bf16[16,512]{1,0:T(8,128)(2,1)S(1)} %attend.1.refs_0_), channel_id=1, source_target_pairs={{0,16},{8,24},{16,0},{24,8},{1,17},{9,25},{17,1},{25,9},{2,18},{10... | collective-permute-start | bytes 49160 | tf_op jit(solution)/shard_map/ppermute | solution.py:49
  24.6 3.7 %collective-permute-start.6 = (bf16[16,512]{1,0:T(8,128)(2,1)S(1)}, bf16[16,512]{1,0:T(8,128)(2,1)S(1)}, u32[]{:S(2)}, u32[]{:S(2)}) collective-permute-start(bf16[16,512]{1,0:T(8,128)(2,1)S(1)} %attend.1.refs_0_), channel_id=1, source_target_pairs={{0,8},{8,0},{16,24},{24,16},{1,9},{9,1},{17,25},{25,17},{2,10},{10... | collective-permute-start | bytes 49160 | tf_op jit(solution)/shard_map/ppermute | solution.py:49
  28.3 44.7 %slice-start.4 = ((s8[8388608]{0:T(1024)(128)(4,1)}), s8[4194304]{0:T(1024)(128)(4,1)S(1)}, s32[]{:S(2)}) async-start(s8[8388608]{0:T(1024)(128)(4,1)} %bitcast.11), calls=%async_computation.4 | async-start | bytes 8388608
  28.7 1.3 %collective-permute-start.9 = (bf16[64,512]{1,0:T(8,128)(2,1)S(1)}, bf16[64,512]{1,0:T(8,128)(2,1)S(1)}, u32[]{:S(2)}, u32[]{:S(2)}) collective-permute-start(bf16[64,512]{1,0:T(8,128)(2,1)S(1)} %get-tuple-element.45), channel_id=1, source_target_pairs={{0,1},{1,0},{2,3},{3,2},{4,5},{5,4},{6,7},{7,6},{8,9},{9,8},{10,11... | collective-permute-start | bytes 196616 | tf_op jit(solution)/shard_map/ppermute | solution.py:49
  30.0 8.0 %collective-permute-start.12 = (bf16[64,512]{1,0:T(8,128)(2,1)S(1)}, bf16[64,512]{1,0:T(8,128)(2,1)S(1)}, u32[]{:S(2)}, u32[]{:S(2)}) collective-permute-start(bf16[64,512]{1,0:T(8,128)(2,1)S(1)} %pairsum.1.refs_0_), channel_id=1, source_target_pairs={{6,0},{7,1},{12,10},{13,11},{18,20},{19,21},{24,30},{25,31}} | collective-permute-start | bytes 196616 | tf_op jit(solution)/shard_map/ppermute | solution.py:700
  31.3 8.1 %collective-permute-start.11 = (bf16[64,512]{1,0:T(8,128)(2,1)S(1)}, bf16[64,512]{1,0:T(8,128)(2,1)S(1)}, u32[]{:S(2)}, u32[]{:S(2)}) collective-permute-start(bf16[64,512]{1,0:T(8,128)(2,1)S(1)} %pairsum.1.refs_0_), channel_id=1, source_target_pairs={{4,0},{5,1},{14,10},{15,11},{16,20},{17,21},{26,30},{27,31}} | collective-permute-start | bytes 196616 | tf_op jit(solution)/shard_map/ppermute | solution.py:700
  32.6 8.1 %collective-permute-start.10 = (bf16[64,512]{1,0:T(8,128)(2,1)S(1)}, bf16[64,512]{1,0:T(8,128)(2,1)S(1)}, u32[]{:S(2)}, u32[]{:S(2)}) collective-permute-start(bf16[64,512]{1,0:T(8,128)(2,1)S(1)} %pairsum.1.refs_0_), channel_id=1, source_target_pairs={{2,0},{3,1},{8,10},{9,11},{22,20},{23,21},{28,30},{29,31}} | collective-permute-start | bytes 196616 | tf_op jit(solution)/shard_map/ppermute | solution.py:700
  40.8 4.2 %collective-permute-start.15 = (bf16[64,512]{1,0:T(8,128)(2,1)S(1)}, bf16[64,512]{1,0:T(8,128)(2,1)S(1)}, u32[]{:S(2)}, u32[]{:S(2)}) collective-permute-start(bf16[64,512]{1,0:T(8,128)(2,1)S(1)} %residual.1.refs_0_), channel_id=1, source_target_pairs={{0,24},{1,25},{10,18},{11,19},{20,12},{21,13},{30,6},{31,7}} | collective-permute-start | bytes 196616 | tf_op jit(solution)/shard_map/ppermute | solution.py:712
  42.1 3.2 %collective-permute-start.14 = (bf16[64,512]{1,0:T(8,128)(2,1)S(1)}, bf16[64,512]{1,0:T(8,128)(2,1)S(1)}, u32[]{:S(2)}, u32[]{:S(2)}) collective-permute-start(bf16[64,512]{1,0:T(8,128)(2,1)S(1)} %residual.1.refs_0_), channel_id=1, source_target_pairs={{0,16},{1,17},{10,26},{11,27},{20,4},{21,5},{30,14},{31,15}} | collective-permute-start | bytes 196616 | tf_op jit(solution)/shard_map/ppermute | solution.py:712
  43.4 3.2 %collective-permute-start.13 = (bf16[64,512]{1,0:T(8,128)(2,1)S(1)}, bf16[64,512]{1,0:T(8,128)(2,1)S(1)}, u32[]{:S(2)}, u32[]{:S(2)}) collective-permute-start(bf16[64,512]{1,0:T(8,128)(2,1)S(1)} %residual.1.refs_0_), channel_id=1, source_target_pairs={{0,8},{1,9},{10,2},{11,3},{20,28},{21,29},{30,22},{31,23}} | collective-permute-start | bytes 196616 | tf_op jit(solution)/shard_map/ppermute | solution.py:712
  46.7 26.4 %slice-start.5 = ((s8[8388608]{0:T(1024)(128)(4,1)}), s8[4194304]{0:T(1024)(128)(4,1)S(1)}, s32[]{:S(2)}) async-start(s8[8388608]{0:T(1024)(128)(4,1)} %bitcast.11), calls=%async_computation.5 | async-start | bytes 8388608
  46.7 26.4 %copy-start.6 = (bf16[512,512]{1,0:T(8,128)(2,1)S(1)}, bf16[512,512]{1,0:T(8,128)(2,1)}, u32[]{:S(2)}) copy-start(bf16[512,512]{1,0:T(8,128)(2,1)} %dense_down.1) | copy-start | bytes 1572868
  50.1 40.1 %copy-start.8 = (f32[512]{0:T(512)S(1)}, f32[512]{0:T(512)}, u32[]{:S(2)}) copy-start(f32[512]{0:T(512)} %param.32) | copy-start | bytes 6148
  50.1 1.8 %collective-permute-start.16 = (bf16[2,72,1280]{2,1,0:T(8,128)(2,1)S(1)}, bf16[2,72,1280]{2,1,0:T(8,128)(2,1)S(1)}, u32[]{:S(2)}, u32[]{:S(2)}) collective-permute-start(bf16[2,72,1280]{2,1,0:T(8,128)(2,1)S(1)} %get-tuple-element.48), channel_id=1, source_target_pairs={{0,1},{1,0},{2,3},{3,2},{4,5},{5,4},{6,7},{7,6},{8,9},{9,8},{10,11... | collective-permute-start | bytes 1105928 | tf_op jit(solution)/shard_map/ppermute | solution.py:49
  52.1 4.8 %collective-permute-start.17 = (bf16[72,640]{1,0:T(8,128)(2,1)S(1)}, bf16[72,640]{1,0:T(8,128)(2,1)S(1)}, u32[]{:S(2)}, u32[]{:S(2)}) collective-permute-start(bf16[72,640]{1,0:T(8,128)(2,1)S(1)} %get-tuple-element.50), channel_id=1, source_target_pairs={{0,2},{1,3},{2,0},{3,1},{4,6},{5,7},{6,4},{7,5},{8,10},{9,11},{10,... | collective-permute-start | bytes 276488 | tf_op jit(solution)/shard_map/ppermute | solution.py:49
  54.0 9.9 %collective-permute-start.18 = (bf16[72,640]{1,0:T(8,128)(2,1)S(1)}, bf16[72,640]{1,0:T(8,128)(2,1)S(1)}, u32[]{:S(2)}, u32[]{:S(2)}) collective-permute-start(bf16[72,640]{1,0:T(8,128)(2,1)S(1)} %get-tuple-element.51), channel_id=1, source_target_pairs={{0,4},{1,5},{2,6},{3,7},{4,0},{5,1},{6,2},{7,3},{8,12},{9,13},{10,... | collective-permute-start | bytes 276488 | tf_op jit(solution)/shard_map/ppermute | solution.py:49
  55.6 8.3 %collective-permute-start.19 = (bf16[72,640]{1,0:T(8,128)(2,1)S(1)}, bf16[72,640]{1,0:T(8,128)(2,1)S(1)}, u32[]{:S(2)}, u32[]{:S(2)}) collective-permute-start(bf16[72,640]{1,0:T(8,128)(2,1)S(1)} %get-tuple-element.52), channel_id=1, source_target_pairs={{0,6},{1,7},{2,4},{3,5},{4,2},{5,3},{6,0},{7,1},{8,14},{9,15},{10,... | collective-permute-start | bytes 276488 | tf_op jit(solution)/shard_map/ppermute | solution.py:49
  64.0 5.9 %collective-permute-start.22 = (bf16[1,32,640]{2,1,0:T(8,128)(2,1)S(1)}, bf16[1,32,640]{2,1,0:T(8,128)(2,1)S(1)}, u32[]{:S(2)}, u32[]{:S(2)}) collective-permute-start(bf16[1,32,640]{2,1,0:T(8,128)(2,1)S(1)} %get-tuple-element.53), channel_id=1, source_target_pairs={{0,6},{1,7},{2,4},{3,5},{4,2},{5,3},{6,0},{7,1},{8,14},{9,15},{10,... | collective-permute-start | bytes 122888 | tf_op jit(solution)/shard_map/ppermute | solution.py:49
  65.8 5.4 %collective-permute-start.21 = (bf16[1,32,640]{2,1,0:T(8,128)(2,1)S(1)}, bf16[1,32,640]{2,1,0:T(8,128)(2,1)S(1)}, u32[]{:S(2)}, u32[]{:S(2)}) collective-permute-start(bf16[1,32,640]{2,1,0:T(8,128)(2,1)S(1)} %get-tuple-element.53), channel_id=1, source_target_pairs={{0,4},{1,5},{2,6},{3,7},{4,0},{5,1},{6,2},{7,3},{8,12},{9,13},{10,... | collective-permute-start | bytes 122888 | tf_op jit(solution)/shard_map/ppermute | solution.py:49
  67.4 4.1 %collective-permute-start.20 = (bf16[1,32,640]{2,1,0:T(8,128)(2,1)S(1)}, bf16[1,32,640]{2,1,0:T(8,128)(2,1)S(1)}, u32[]{:S(2)}, u32[]{:S(2)}) collective-permute-start(bf16[1,32,640]{2,1,0:T(8,128)(2,1)S(1)} %get-tuple-element.53), channel_id=1, source_target_pairs={{0,2},{1,3},{2,0},{3,1},{4,6},{5,7},{6,4},{7,5},{8,10},{9,11},{10,... | collective-permute-start | bytes 122888 | tf_op jit(solution)/shard_map/ppermute | solution.py:49
  71.6 1.5 %collective-permute-start.23 = (bf16[4,32,640]{2,1,0:T(8,128)(2,1)S(1)}, bf16[4,32,640]{2,1,0:T(8,128)(2,1)S(1)}, u32[]{:S(2)}, u32[]{:S(2)}) collective-permute-start(bf16[4,32,640]{2,1,0:T(8,128)(2,1)S(1)} %pad_maximum_fusion), channel_id=1, source_target_pairs={{0,1},{1,0},{2,3},{3,2},{4,5},{5,4},{6,7},{7,6},{8,9},{9,8},{10,11... | collective-permute-start | bytes 491528 | tf_op jit(solution)/shard_map/ppermute | solution.py:49
  74.5 4.3 %collective-permute-start.24 = (bf16[16,512]{1,0:T(8,128)(2,1)S(1)}, bf16[16,512]{1,0:T(8,128)(2,1)S(1)}, u32[]{:S(2)}, u32[]{:S(2)}) collective-permute-start(bf16[16,512]{1,0:T(8,128)(2,1)S(1)} %get-tuple-element.58), channel_id=1, source_target_pairs={{0,8},{8,0},{16,24},{24,16},{1,9},{9,1},{17,25},{25,17},{2,10},{10... | collective-permute-start | bytes 49160 | tf_op jit(solution)/shard_map/ppermute | solution.py:49
  76.0 3.7 %collective-permute-start.25 = (bf16[16,512]{1,0:T(8,128)(2,1)S(1)}, bf16[16,512]{1,0:T(8,128)(2,1)S(1)}, u32[]{:S(2)}, u32[]{:S(2)}) collective-permute-start(bf16[16,512]{1,0:T(8,128)(2,1)S(1)} %get-tuple-element.59), channel_id=1, source_target_pairs={{0,16},{8,24},{16,0},{24,8},{1,17},{9,25},{17,1},{25,9},{2,18},{10... | collective-permute-start | bytes 49160 | tf_op jit(solution)/shard_map/ppermute | solution.py:49
  77.3 4.6 %collective-permute-start.26 = (bf16[16,512]{1,0:T(8,128)(2,1)S(1)}, bf16[16,512]{1,0:T(8,128)(2,1)S(1)}, u32[]{:S(2)}, u32[]{:S(2)}) collective-permute-start(bf16[16,512]{1,0:T(8,128)(2,1)S(1)} %get-tuple-element.60), channel_id=1, source_target_pairs={{0,24},{8,16},{16,8},{24,0},{1,25},{9,17},{17,9},{25,1},{2,26},{10... | collective-permute-start | bytes 49160 | tf_op jit(solution)/shard_map/ppermute | solution.py:49
  82.1 1.2 %collective-permute-start.27 = (f32[8,128]{1,0:T(8,128)S(1)}, f32[8,128]{1,0:T(8,128)S(1)}, u32[]{:S(2)}, u32[]{:S(2)}) collective-permute-start(f32[8,128]{1,0:T(8,128)S(1)} %get-tuple-element.62), channel_id=1, source_target_pairs={{0,1},{1,0},{2,3},{3,2},{4,5},{5,4},{6,7},{7,6},{8,9},{9,8},{10,11... | collective-permute-start | bytes 12296 | tf_op jit(solution)/shard_map/ppermute | solution.py:49
  83.3 5.4 %collective-permute-start.30 = (f32[8,128]{1,0:T(8,128)S(1)}, f32[8,128]{1,0:T(8,128)S(1)}, u32[]{:S(2)}, u32[]{:S(2)}) collective-permute-start(f32[8,128]{1,0:T(8,128)S(1)} %add.3.refs_2_), channel_id=1, source_target_pairs={{0,6},{1,7},{2,4},{3,5},{4,2},{5,3},{6,0},{7,1},{8,14},{9,15},{10,... | collective-permute-start | bytes 12296 | tf_op jit(solution)/shard_map/ppermute | solution.py:49
  85.7 4.5 %collective-permute-start.29 = (f32[8,128]{1,0:T(8,128)S(1)}, f32[8,128]{1,0:T(8,128)S(1)}, u32[]{:S(2)}, u32[]{:S(2)}) collective-permute-start(f32[8,128]{1,0:T(8,128)S(1)} %add.3.refs_2_), channel_id=1, source_target_pairs={{0,4},{1,5},{2,6},{3,7},{4,0},{5,1},{6,2},{7,3},{8,12},{9,13},{10,... | collective-permute-start | bytes 12296 | tf_op jit(solution)/shard_map/ppermute | solution.py:49
  85.7 4.5 %collective-permute-start.28 = (f32[8,128]{1,0:T(8,128)S(1)}, f32[8,128]{1,0:T(8,128)S(1)}, u32[]{:S(2)}, u32[]{:S(2)}) collective-permute-start(f32[8,128]{1,0:T(8,128)S(1)} %add.3.refs_2_), channel_id=1, source_target_pairs={{0,2},{1,3},{2,0},{3,1},{4,6},{5,7},{6,4},{7,5},{8,10},{9,11},{10,... | collective-permute-start | bytes 12296 | tf_op jit(solution)/shard_map/ppermute | solution.py:49

commit v5 on v4

--- a/solution.py
+++ b/solution.py
@@ -275,15 +275,6 @@
             mean = mean + extra[:, MEAN_LANE + i : MEAN_LANE + i + 1]
         own = pieces[d][:, aligned(side, size)].astype(F32)
         out[place, :] = (residual_scale * (own - mean) + total).astype(BF16)
-
-
-def send_part(sent, value):
-    rows = value.shape[1]
-    sent[:, : rows - STATS, :] = value[:, : rows - STATS, :].astype(BF16)
-    sums = value[0, rows - STATS :, :] + value[1, rows - STATS :, :]
-    high = sums.astype(BF16)
-    sent[0, rows - STATS :, :] = high
-    sent[1, rows - STATS :, :] = (sums - high.astype(F32)).astype(BF16)
 
 
 def routing_kernel(*refs, ep_count, local_experts):
@@ -332,27 +323,25 @@
     placed_out[...] = placed
 
 
-def experts_kernel(*refs, ep_count, ratio, width):
+def experts_kernel(*refs, ep_count, ratio, width, plane):
     own = refs[0]
     arrivals = refs[1:ep_count]
     (
         placed,
         gain_ref,
         mix_ref,
-        expert_gate,
-        expert_up,
-        dense_gate,
-        dense_up,
+        expert_weight_ref,
+        dense_weight,
         sent,
         kept,
-        own_out,
+        *own_out,
         full,
     ) = refs[ep_count:]
     ep = lax.axis_index("ep")
     tp = lax.axis_index("tp")
     total_rows, size = own.shape
     seq_count = total_rows // ep_count
-    local_experts = expert_gate.shape[0]
+    local_experts = expert_weight_ref.shape[0]
     expert_rows = ep_count * CAP
     slot_count = local_experts * expert_rows
     distance = ep ^ (tp // ratio)
@@ -364,7 +353,8 @@
             j = i ^ d
             rows = rows + arrivals[d - 1][j * seq_count : (j + 1) * seq_count, :].astype(F32)
         blocks.append(rows)
-    own_out[...] = blocks[0]
+    if own_out:
+        own_out[0][...] = blocks[0]
     rows = jnp.concatenate(blocks, axis=0)
     gain = gain_ref[:, aligned(tp, size)]
     mix = mix_ref[:, aligned(tp, size)].astype(F32)
@@ -384,40 +374,43 @@
     gain_rows = jnp.where(
         gain_row == 0, gain_high, jnp.where(gain_row == 1, gain - gain_high, 0.0)
     ).astype(BF16)
-    expert_width = expert_gate.shape[2]
-    dense_width = dense_gate.shape[1]
+    expert_width = expert_weight_ref.shape[2]
+    dense_width = dense_weight.shape[1]
     fold = total_rows // slot_count
-    full[:, slot_count:, :] = jnp.zeros((2, TAIL, full.shape[2]), F32)
+    full[slot_count:, :] = jnp.zeros((TAIL, full.shape[1]), F32)
     dense_rows = jnp.concatenate([hidden, gain_rows], axis=0)
-    for plane, (expert_weight, dense_weight) in enumerate(
-        ((expert_gate, dense_gate), (expert_up, dense_up))
-    ):
+    for e in range(local_experts):
+        lhs = jnp.concatenate(
+            [routed[e * expert_rows : (e + 1) * expert_rows], gain_rows], axis=0
+        )
+        part = jnp.dot(lhs, expert_weight_ref[e], preferred_element_type=F32)
+        full[e * expert_rows : (e + 1) * expert_rows, :expert_width] = part[
+            :expert_rows
+        ]
+        full[slot_count + e : slot_count + e + 1, :expert_width] = (
+            part[expert_rows : expert_rows + 1] + part[expert_rows + 1 : expert_rows + 2]
+        )
+    part = jnp.dot(dense_rows, dense_weight[...], preferred_element_type=F32)
+    gain_part = part[total_rows : total_rows + 1] + part[total_rows + 1 : total_rows + 2]
+    for f in range(fold):
+        place = slice(expert_width + f * dense_width, expert_width + (f + 1) * dense_width)
+        full[:slot_count, place] = part[f * slot_count : (f + 1) * slot_count]
         for e in range(local_experts):
-            lhs = jnp.concatenate(
-                [routed[e * expert_rows : (e + 1) * expert_rows], gain_rows], axis=0
-            )
-            part = jnp.dot(lhs, expert_weight[e], preferred_element_type=F32)
-            full[plane, e * expert_rows : (e + 1) * expert_rows, :expert_width] = part[
-                :expert_rows
-            ]
-            full[plane, slot_count + e : slot_count + e + 1, :expert_width] = (
-                part[expert_rows : expert_rows + 1] + part[expert_rows + 1 : expert_rows + 2]
-            )
-        part = jnp.dot(dense_rows, dense_weight[...], preferred_element_type=F32)
-        gain_part = part[total_rows : total_rows + 1] + part[total_rows + 1 : total_rows + 2]
-        for f in range(fold):
-            place = slice(expert_width + f * dense_width, expert_width + (f + 1) * dense_width)
-            full[plane, :slot_count, place] = part[f * slot_count : (f + 1) * slot_count]
-            for e in range(local_experts):
-                full[plane, slot_count + e : slot_count + e + 1, place] = gain_part
-    for start in range(0, full.shape[2], width):
-        for i in range(STATS):
-            at = slot_count + TAIL - STATS + i
-            full[0, at : at + 1, start : start + total_rows] = row_of(sums[i])
-    half = full.shape[2] // 2
+            full[slot_count + e : slot_count + e + 1, place] = gain_part
+    half = full.shape[1] // 2
     side = tp & 1
-    send_part(sent, full[:, :, aligned(1 - side, half)])
-    kept[...] = full[:, :, aligned(side, half)]
+    sent[...] = full[:, aligned(1 - side, half)].astype(BF16)
+    kept[...] = full[:, aligned(side, half)]
+    sums = jnp.concatenate([row_of(column) for column in sums], axis=0)
+    high = sums.astype(BF16)
+    rows = slice(slot_count + TAIL - STATS, slot_count + TAIL)
+    for start in range(0, half, width):
+        place = slice(start, start + total_rows)
+        if plane == 0:
+            sent[rows, place] = high
+            kept[rows, place] = sums
+        else:
+            sent[rows, place] = (sums - high.astype(F32)).astype(BF16)
 
 
 def piece_at(index, bits, rows, width):
@@ -437,9 +430,10 @@
     return -(-total_rows // LANES) * LANES
 
 
-def spread_kernel(kept, got, *refs, bits, expert_rows, total_rows):
-    outs, full, tail = refs[:-2], refs[-2], refs[-1]
-    full[...] = kept[...] + got[...].astype(F32)
+def spread_kernel(*refs, bits, expert_rows, total_rows):
+    outs, full, tail = refs[4:-2], refs[-2], refs[-1]
+    for plane in range(2):
+        full[plane] = refs[plane][...] + refs[2 + plane][...].astype(F32)
     slot_count = full.shape[1] - TAIL
     width = outs[0].shape[1]
     piece_rows = (outs[0].shape[0] - tail.shape[0]) // 2
@@ -725,7 +719,7 @@
             piece_rows //= 2
     bits = tuple(bits)
     full_rows = slot_count + TAIL
-    half = (2, full_rows, width // 2)
+    half = (full_rows, width // 2)
     placed, info = call(
         routing_kernel,
         "routing",
@@ -734,40 +728,39 @@
         ep_count=ep_count,
         local_experts=local_experts,
     )
-    sent, kept, own_rows = call(
-        experts_kernel,
-        "experts",
-        [
-            (half, BF16),
-            (half, F32),
-            ((seq_count, slice_width), F32),
-        ],
-        [residual]
-        + arrivals
-        + [
-            placed,
-            first_gain[None, :],
-            dense_mix[None, :],
-            expert_gate,
-            expert_up,
-            dense_gate,
-            dense_up,
-        ],
-        scratch=[((2, full_rows, width), F32)],
-        mib=8,
-        ep_count=ep_count,
-        ratio=ratio,
-        width=piece_width,
-    )
-    got = xor_permute(sent, "tp", tp_count, 1)
+    kept, got = [], []
+    for plane, (name, expert_weight, dense_weight) in enumerate(
+        (("gates", expert_gate, dense_gate), ("ups", expert_up, dense_up))
+    ):
+        outs = [(half, BF16), (half, F32)]
+        if plane == 0:
+            outs.append(((seq_count, slice_width), F32))
+        result = call(
+            experts_kernel,
+            name,
+            outs,
+            [residual]
+            + arrivals
+            + [placed, first_gain[None, :], dense_mix[None, :], expert_weight, dense_weight],
+            scratch=[((full_rows, width), F32)],
+            mib=8,
+            ep_count=ep_count,
+            ratio=ratio,
+            width=piece_width,
+            plane=plane,
+        )
+        if plane == 0:
+            own_rows = result[2]
+        kept.append(result[1])
+        got.append(xor_permute(result[0], "tp", tp_count, 1))
     piece_tail = -(-(2 * max(1, piece_rows // expert_rows) + STATS) // 8) * 8
     piece = (2 * piece_rows + piece_tail, piece_width)
     parts = call(
         spread_kernel,
         "spread",
         [(piece, F32)] + [(piece, BF16)] * (place_count - 1),
-        [kept, got],
-        scratch=[(half, F32), ((piece_tail, piece_width), F32)],
+        kept + got,
+        scratch=[((2,) + half, F32), ((piece_tail, piece_width), F32)],
         bits=bits,
         expert_rows=expert_rows,
         total_rows=total_rows,

time: 91.2 us -> 91.5 us (level)
    ppermute x25 -> x26, starting transfers between devices: 29.6 us -> 30 us  [xor_permute(): return lax.ppermute(array, axis, [(i, i ^ distance) for i in range(count)])]
    ppermute x25 -> x26, waiting for transfers between devices: 31.3 us -> 31.1 us  [xor_permute(): return lax.ppermute(array, axis, [(i, i ^ distance) for i in range(count)])]
    pallas_call x14 -> x15, Pallas kernels: 13.3 us -> 13.6 us  [call(): pl.pallas_call(functools.partial(kernel, **sizes), out_shape=[jax.ShapeDt...]
  transfers between devices with their start and end apart: 31 -> 32, of which waited for: 26 -> 26; matrix products, arithmetic and copies ran while one was open for 0% -> 0% of each run, Pallas kernels for 1% -> 3%
where the time goes in v5:
time: 91.5 us; the launch traced here: 91.3 us
  waiting for transfers between devices  39.4 us (43%)
  starting transfers between devices  37.7 us (41%)
  Pallas kernels  13.6 us (15%)
    ppermute x26, waiting for transfers between devices, xor_permute(): return lax.ppermute(array, axis, [(i, i ^ distance) for i in range(count)])  31.1 us
    ppermute x26, starting transfers between devices, xor_permute(): return lax.ppermute(array, axis, [(i, i ^ distance) for i in range(count)])  30 us
    pallas_call x15, Pallas kernels, call(): pl.pallas_call(functools.partial(kernel, **sizes), out_shape=[jax.ShapeDt...  13.6 us
    ppermute x3, waiting for transfers between devices, on_device(): lax.ppermute(part_sum, both, [(device(c, c ^ d, h), device(c, c, h)) for...  6.75 us
    ppermute x3, starting transfers between devices, on_device(): lax.ppermute(residual, both, [(device(c, c, h), device(c ^ d, c, h)) for...  3.88 us
    ppermute x3, starting transfers between devices, on_device(): lax.ppermute(part_sum, both, [(device(c, c ^ d, h), device(c, c, h)) for...  3.88 us
  transfers between devices with their start and end apart: 32, of which 26 were waited for; matrix products, arithmetic and copies ran while one was open for 0% of the time, Pallas kernels for 3%

profile of v5, /device:TPU:0, one launch (start us, length us, event | category | flops | bytes accessed | tf_op | source)
XLA Modules:
  0.0 91.3 jit_solution(17873962466635849461)
XLA Ops:
  0.0 1.2 %prepare.1 = (bf16[16,1152]{1,0:T(8,128)(2,1)S(1)}, bf16[16,1152]{1,0:T(8,128)(2,1)S(1)}, bf16[16,1152]{1,0:T(8,128)(2,1)S(1)}, bf16[16,1152]{1,0:T(8,128)(2,1)S(1)}) custom-call(bf16[16,4096]{1,0:T(8,128)(2,1)} %tokens.1, s32[2,16]{1,0:T(2,128)} %bitcast.20, f32[2,16]{1,0:T(2,128)} %bitcast.21), custom_call_target="tpu_custom_call" | custom-call | flops 20000000000 | bytes 20000000000 | tf_op jit(solution)/shard_map/prepare/pallas_call | solution.py:36
  1.2 3.0 %collective-permute-start = (bf16[16,1152]{1,0:T(8,128)(2,1)S(1)}, bf16[16,1152]{1,0:T(8,128)(2,1)S(1)}, u32[]{:S(2)}, u32[]{:S(2)}) collective-permute-start(bf16[16,1152]{1,0:T(8,128)(2,1)S(1)} %get-tuple-element.37), channel_id=1, source_target_pairs={{0,8},{8,0},{16,24},{24,16},{1,9},{9,1},{17,25},{25,17},{2,10},{10... | collective-permute-start | bytes 110600 | tf_op jit(solution)/shard_map/ppermute | solution.py:49
  4.3 1.5 %collective-permute-start.1 = (bf16[16,1152]{1,0:T(8,128)(2,1)S(1)}, bf16[16,1152]{1,0:T(8,128)(2,1)S(1)}, u32[]{:S(2)}, u32[]{:S(2)}) collective-permute-start(bf16[16,1152]{1,0:T(8,128)(2,1)S(1)} %get-tuple-element.38), channel_id=1, source_target_pairs={{0,16},{8,24},{16,0},{24,8},{1,17},{9,25},{17,1},{25,9},{2,18},{10... | collective-permute-start | bytes 110600 | tf_op jit(solution)/shard_map/ppermute | solution.py:49
  5.8 0.4 collective-permute-done.refs_1_.refs_5_
  6.2 2.0 %collective-permute-done.1.refs_2_.refs_6_ = bf16[16,1152]{1,0:T(8,128)(2,1)S(1)} collective-permute-done((bf16[16,1152]{1,0:T(8,128)(2,1)S(1)}, bf16[16,1152]{1,0:T(8,128)(2,1)S(1)}, u32[]{:S(2)}, u32[]{:S(2)}) %collective-permute-start.1) | collective-permute-done | bytes 36896 | tf_op jit(solution)/shard_map/ppermute | solution.py:49
  8.2 2.4 %collective-permute-done.2.refs_3_.refs_7_ = bf16[16,1152]{1,0:T(8,128)(2,1)S(1)} collective-permute-done((bf16[16,1152]{1,0:T(8,128)(2,1)S(1)}, bf16[16,1152]{1,0:T(8,128)(2,1)S(1)}, u32[]{:S(2)}, u32[]{:S(2)}) %collective-permute-start.2) | collective-permute-done | bytes 36896 | tf_op jit(solution)/shard_map/ppermute | solution.py:49
  10.7 0.5 project.1
  11.2 0.6 collective-permute-start.3
  11.8 2.9 %collective-permute-start.5 = (bf16[16,1024]{1,0:T(8,128)(2,1)S(1)}, bf16[16,1024]{1,0:T(8,128)(2,1)S(1)}, u32[]{:S(2)}, u32[]{:S(2)}) collective-permute-start(bf16[16,1024]{1,0:T(8,128)(2,1)S(1)} %get-tuple-element.43), channel_id=1, source_target_pairs={{0,24},{8,16},{16,8},{24,0},{1,25},{9,17},{17,9},{25,1},{2,26},{10... | collective-permute-start | bytes 98312 | tf_op jit(solution)/shard_map/ppermute | solution.py:49
  14.7 0.6 tables.1
  15.3 0.3 collective-permute-done.4.refs_2_
  15.7 0.9 %collective-permute-done.5.refs_3_ = bf16[16,1024]{1,0:T(8,128)(2,1)S(1)} collective-permute-done((bf16[16,1024]{1,0:T(8,128)(2,1)S(1)}, bf16[16,1024]{1,0:T(8,128)(2,1)S(1)}, u32[]{:S(2)}, u32[]{:S(2)}) %collective-permute-start.5) | collective-permute-done | bytes 32800 | tf_op jit(solution)/shard_map/ppermute | solution.py:49
  16.7 4.4 %attend.1.refs_0_ = bf16[16,512]{1,0:T(8,128)(2,1)S(1)} custom-call(s32[16]{0:T(128)S(1)} %copy-done.11, f32[4]{0:T(128)S(1)} %copy-done.12, f32[16,1024]{1,0:T(8,128)S(1)} %get-tuple-element.40.refs_0_, bf16[16,1024]{1,0:T(8,128)(2,1)S(1)} %collective-permute-done.3.refs_1_, bf16[16,1024]{1,0:T(8,128)(2,1)S(1)} %collective-permute-done.4.refs_2_, ...), custom_call_target="tpu_custom_call" | custom-call | flops 20000000000 | bytes 20000000000 | tf_op jit(solution)/shard_map/attend/pallas_call | solution.py:36
  21.1 3.0 %collective-permute-start.8 = (bf16[16,512]{1,0:T(8,128)(2,1)S(1)}, bf16[16,512]{1,0:T(8,128)(2,1)S(1)}, u32[]{:S(2)}, u32[]{:S(2)}) collective-permute-start(bf16[16,512]{1,0:T(8,128)(2,1)S(1)} %attend.1.refs_0_), channel_id=1, source_target_pairs={{0,24},{8,16},{16,8},{24,0},{1,25},{9,17},{17,9},{25,1},{2,26},{10... | collective-permute-start | bytes 49160 | tf_op jit(solution)/shard_map/ppermute | solution.py:49
  24.1 0.5 collective-permute-start.7
  24.6 0.1 collective-permute-start.6
  24.7 1.1 %collective-permute-done.8.refs_3_ = bf16[16,512]{1,0:T(8,128)(2,1)S(1)} collective-permute-done((bf16[16,512]{1,0:T(8,128)(2,1)S(1)}, bf16[16,512]{1,0:T(8,128)(2,1)S(1)}, u32[]{:S(2)}, u32[]{:S(2)}) %collective-permute-start.8) | collective-permute-done | bytes 16416 | tf_op jit(solution)/shard_map/ppermute | solution.py:49
  25.8 2.0 %collective-permute-done.7.refs_2_ = bf16[16,512]{1,0:T(8,128)(2,1)S(1)} collective-permute-done((bf16[16,512]{1,0:T(8,128)(2,1)S(1)}, bf16[16,512]{1,0:T(8,128)(2,1)S(1)}, u32[]{:S(2)}, u32[]{:S(2)}) %collective-permute-start.7) | collective-permute-done | bytes 16416 | tf_op jit(solution)/shard_map/ppermute | solution.py:49
  27.8 0.5 collective-permute-done.6.refs_1_
  28.3 0.3 outproj.1
  28.7 1.2 %collective-permute-done.9.refs_1_ = bf16[64,512]{1,0:T(8,128)(2,1)S(1)} collective-permute-done((bf16[64,512]{1,0:T(8,128)(2,1)S(1)}, bf16[64,512]{1,0:T(8,128)(2,1)S(1)}, u32[]{:S(2)}, u32[]{:S(2)}) %collective-permute-start.9) | collective-permute-done | bytes 65568 | tf_op jit(solution)/shard_map/ppermute | solution.py:49
  30.0 1.3 %collective-permute-start.12 = (bf16[64,512]{1,0:T(8,128)(2,1)S(1)}, bf16[64,512]{1,0:T(8,128)(2,1)S(1)}, u32[]{:S(2)}, u32[]{:S(2)}) collective-permute-start(bf16[64,512]{1,0:T(8,128)(2,1)S(1)} %pairsum.1.refs_0_), channel_id=1, source_target_pairs={{6,0},{7,1},{12,10},{13,11},{18,20},{19,21},{24,30},{25,31}} | collective-permute-start | bytes 196616 | tf_op jit(solution)/shard_map/ppermute | solution.py:694
  31.3 1.3 %collective-permute-start.11 = (bf16[64,512]{1,0:T(8,128)(2,1)S(1)}, bf16[64,512]{1,0:T(8,128)(2,1)S(1)}, u32[]{:S(2)}, u32[]{:S(2)}) collective-permute-start(bf16[64,512]{1,0:T(8,128)(2,1)S(1)} %pairsum.1.refs_0_), channel_id=1, source_target_pairs={{4,0},{5,1},{14,10},{15,11},{16,20},{17,21},{26,30},{27,31}} | collective-permute-start | bytes 196616 | tf_op jit(solution)/shard_map/ppermute | solution.py:694
  32.6 1.3 %collective-permute-start.10 = (bf16[64,512]{1,0:T(8,128)(2,1)S(1)}, bf16[64,512]{1,0:T(8,128)(2,1)S(1)}, u32[]{:S(2)}, u32[]{:S(2)}) collective-permute-start(bf16[64,512]{1,0:T(8,128)(2,1)S(1)} %pairsum.1.refs_0_), channel_id=1, source_target_pairs={{2,0},{3,1},{8,10},{9,11},{22,20},{23,21},{28,30},{29,31}} | collective-permute-start | bytes 196616 | tf_op jit(solution)/shard_map/ppermute | solution.py:694
  33.9 4.1 %collective-permute-done.12.refs_3_ = bf16[64,512]{1,0:T(8,128)(2,1)S(1)} collective-permute-done((bf16[64,512]{1,0:T(8,128)(2,1)S(1)}, bf16[64,512]{1,0:T(8,128)(2,1)S(1)}, u32[]{:S(2)}, u32[]{:S(2)}) %collective-permute-start.12) | collective-permute-done | bytes 65568 | tf_op jit(solution)/shard_map/ppermute | solution.py:694
  38.0 1.3 %collective-permute-done.11.refs_2_ = bf16[64,512]{1,0:T(8,128)(2,1)S(1)} collective-permute-done((bf16[64,512]{1,0:T(8,128)(2,1)S(1)}, bf16[64,512]{1,0:T(8,128)(2,1)S(1)}, u32[]{:S(2)}, u32[]{:S(2)}) %collective-permute-start.11) | collective-permute-done | bytes 65568 | tf_op jit(solution)/shard_map/ppermute | solution.py:694
  39.3 1.3 %collective-permute-done.10.refs_1_ = bf16[64,512]{1,0:T(8,128)(2,1)S(1)} collective-permute-done((bf16[64,512]{1,0:T(8,128)(2,1)S(1)}, bf16[64,512]{1,0:T(8,128)(2,1)S(1)}, u32[]{:S(2)}, u32[]{:S(2)}) %collective-permute-start.10) | collective-permute-done | bytes 65568 | tf_op jit(solution)/shard_map/ppermute | solution.py:694
  40.6 0.2 residual.1.refs_0_
  40.8 1.3 %collective-permute-start.15 = (bf16[64,512]{1,0:T(8,128)(2,1)S(1)}, bf16[64,512]{1,0:T(8,128)(2,1)S(1)}, u32[]{:S(2)}, u32[]{:S(2)}) collective-permute-start(bf16[64,512]{1,0:T(8,128)(2,1)S(1)} %residual.1.refs_0_), channel_id=1, source_target_pairs={{0,24},{1,25},{10,18},{11,19},{20,12},{21,13},{30,6},{31,7}} | collective-permute-start | bytes 196616 | tf_op jit(solution)/shard_map/ppermute | solution.py:706
  42.1 1.3 %collective-permute-start.14 = (bf16[64,512]{1,0:T(8,128)(2,1)S(1)}, bf16[64,512]{1,0:T(8,128)(2,1)S(1)}, u32[]{:S(2)}, u32[]{:S(2)}) collective-permute-start(bf16[64,512]{1,0:T(8,128)(2,1)S(1)} %residual.1.refs_0_), channel_id=1, source_target_pairs={{0,16},{1,17},{10,26},{11,27},{20,4},{21,5},{30,14},{31,15}} | collective-permute-start | bytes 196616 | tf_op jit(solution)/shard_map/ppermute | solution.py:706
  43.4 1.3 %collective-permute-start.13 = (bf16[64,512]{1,0:T(8,128)(2,1)S(1)}, bf16[64,512]{1,0:T(8,128)(2,1)S(1)}, u32[]{:S(2)}, u32[]{:S(2)}) collective-permute-start(bf16[64,512]{1,0:T(8,128)(2,1)S(1)} %residual.1.refs_0_), channel_id=1, source_target_pairs={{0,8},{1,9},{10,2},{11,3},{20,28},{21,29},{30,22},{31,23}} | collective-permute-start | bytes 196616 | tf_op jit(solution)/shard_map/ppermute | solution.py:706
  44.7 0.3 routing.1
  45.1 0.2 collective-permute-done.14.refs_2_
  45.3 1.3 %collective-permute-done.13.refs_1_ = bf16[64,512]{1,0:T(8,128)(2,1)S(1)} collective-permute-done((bf16[64,512]{1,0:T(8,128)(2,1)S(1)}, bf16[64,512]{1,0:T(8,128)(2,1)S(1)}, u32[]{:S(2)}, u32[]{:S(2)}) %collective-permute-start.13) | collective-permute-done | bytes 65568 | tf_op jit(solution)/shard_map/ppermute | solution.py:706
  46.6 1.8 %ups.1 = (bf16[72,1280]{1,0:T(8,128)(2,1)S(1)}, f32[72,1280]{1,0:T(8,128)S(1)}) custom-call(bf16[64,512]{1,0:T(8,128)(2,1)S(1)} %residual.1.refs_0_, bf16[64,512]{1,0:T(8,128)(2,1)S(1)} %collective-permute-done.13.refs_1_, bf16[64,512]{1,0:T(8,128)(2,1)S(1)} %collective-permute-done.14.refs_2_, bf16[64,512]{1,0:T(8,128)(2,1)S(1)} %collective-permute-done.15.refs_3_, ...), custom_call_target="tpu_custom_call" | custom-call | tf_op jit(solution)/shard_map/ups/pallas_call | solution.py:36
  48.6 1.8 %gates.1 = (bf16[72,1280]{1,0:T(8,128)(2,1)S(1)}, f32[72,1280]{1,0:T(8,128)S(1)}, f32[16,512]{1,0:T(8,128)S(1)}) custom-call(bf16[64,512]{1,0:T(8,128)(2,1)S(1)} %residual.1.refs_0_, bf16[64,512]{1,0:T(8,128)(2,1)S(1)} %collective-permute-done.13.refs_1_, bf16[64,512]{1,0:T(8,128)(2,1)S(1)} %collective-permute-done.14.refs_2_, ...), custom_call_target="tpu_custom_call" | custom-call | tf_op jit(solution)/shard_map/gates/pallas_call | solution.py:36
  50.5 0.5 collective-permute-start.16
  51.0 1.1 %collective-permute-done.16.refs_2_ = bf16[72,1280]{1,0:T(8,128)(2,1)S(1)} collective-permute-done((bf16[72,1280]{1,0:T(8,128)(2,1)S(1)}, bf16[72,1280]{1,0:T(8,128)(2,1)S(1)}, u32[]{:S(2)}, u32[]{:S(2)}) %collective-permute-start.16) | collective-permute-done | bytes 184352 | tf_op jit(solution)/shard_map/ppermute | solution.py:49
  52.1 0.2 spread.1
  52.2 1.9 %collective-permute-start.18 = (bf16[72,640]{1,0:T(8,128)(2,1)S(1)}, bf16[72,640]{1,0:T(8,128)(2,1)S(1)}, u32[]{:S(2)}, u32[]{:S(2)}) collective-permute-start(bf16[72,640]{1,0:T(8,128)(2,1)S(1)} %get-tuple-element.54), channel_id=1, source_target_pairs={{0,2},{1,3},{2,0},{3,1},{4,6},{5,7},{6,4},{7,5},{8,10},{9,11},{10,... | collective-permute-start | bytes 276488 | tf_op jit(solution)/shard_map/ppermute | solution.py:49
  54.1 1.7 %collective-permute-start.19 = (bf16[72,640]{1,0:T(8,128)(2,1)S(1)}, bf16[72,640]{1,0:T(8,128)(2,1)S(1)}, u32[]{:S(2)}, u32[]{:S(2)}) collective-permute-start(bf16[72,640]{1,0:T(8,128)(2,1)S(1)} %get-tuple-element.55), channel_id=1, source_target_pairs={{0,4},{1,5},{2,6},{3,7},{4,0},{5,1},{6,2},{7,3},{8,12},{9,13},{10,... | collective-permute-start | bytes 276488 | tf_op jit(solution)/shard_map/ppermute | solution.py:49
  55.8 0.9 %collective-permute-start.20 = (bf16[72,640]{1,0:T(8,128)(2,1)S(1)}, bf16[72,640]{1,0:T(8,128)(2,1)S(1)}, u32[]{:S(2)}, u32[]{:S(2)}) collective-permute-start(bf16[72,640]{1,0:T(8,128)(2,1)S(1)} %get-tuple-element.56), channel_id=1, source_target_pairs={{0,6},{1,7},{2,4},{3,5},{4,2},{5,3},{6,0},{7,1},{8,14},{9,15},{10,... | collective-permute-start | bytes 276488 | tf_op jit(solution)/shard_map/ppermute | solution.py:49
  56.7 0.6 collective-permute-done.18.refs_1_
  57.3 6.9 %collective-permute-done.19.refs_2_ = bf16[72,640]{1,0:T(8,128)(2,1)S(1)} collective-permute-done((bf16[72,640]{1,0:T(8,128)(2,1)S(1)}, bf16[72,640]{1,0:T(8,128)(2,1)S(1)}, u32[]{:S(2)}, u32[]{:S(2)}) %collective-permute-start.19) | collective-permute-done | bytes 92192 | tf_op jit(solution)/shard_map/ppermute | solution.py:49
  64.2 0.1 act.1
  64.4 1.5 %collective-permute-start.23 = (bf16[1,32,640]{2,1,0:T(8,128)(2,1)S(1)}, bf16[1,32,640]{2,1,0:T(8,128)(2,1)S(1)}, u32[]{:S(2)}, u32[]{:S(2)}) collective-permute-start(bf16[1,32,640]{2,1,0:T(8,128)(2,1)S(1)} %get-tuple-element.57), channel_id=1, source_target_pairs={{0,6},{1,7},{2,4},{3,5},{4,2},{5,3},{6,0},{7,1},{8,14},{9,15},{10,... | collective-permute-start | bytes 122888 | tf_op jit(solution)/shard_map/ppermute | solution.py:49
  65.9 1.9 %collective-permute-start.22 = (bf16[1,32,640]{2,1,0:T(8,128)(2,1)S(1)}, bf16[1,32,640]{2,1,0:T(8,128)(2,1)S(1)}, u32[]{:S(2)}, u32[]{:S(2)}) collective-permute-start(bf16[1,32,640]{2,1,0:T(8,128)(2,1)S(1)} %get-tuple-element.57), channel_id=1, source_target_pairs={{0,4},{1,5},{2,6},{3,7},{4,0},{5,1},{6,2},{7,3},{8,12},{9,13},{10,... | collective-permute-start | bytes 122888 | tf_op jit(solution)/shard_map/ppermute | solution.py:49
  67.8 1.0 %collective-permute-start.21 = (bf16[1,32,640]{2,1,0:T(8,128)(2,1)S(1)}, bf16[1,32,640]{2,1,0:T(8,128)(2,1)S(1)}, u32[]{:S(2)}, u32[]{:S(2)}) collective-permute-start(bf16[1,32,640]{2,1,0:T(8,128)(2,1)S(1)} %get-tuple-element.57), channel_id=1, source_target_pairs={{0,2},{1,3},{2,0},{3,1},{4,6},{5,7},{6,4},{7,5},{8,10},{9,11},{10,... | collective-permute-start | bytes 122888 | tf_op jit(solution)/shard_map/ppermute | solution.py:49
  68.9 1.6 %collective-permute-done.23 = bf16[1,32,640]{2,1,0:T(8,128)(2,1)S(1)} collective-permute-done((bf16[1,32,640]{2,1,0:T(8,128)(2,1)S(1)}, bf16[1,32,640]{2,1,0:T(8,128)(2,1)S(1)}, u32[]{:S(2)}, u32[]{:S(2)}) %collective-permute-start.23) | collective-permute-done | bytes 40992 | tf_op jit(solution)/shard_map/ppermute | solution.py:49
  70.4 0.9 collective-permute-done.22
  71.3 0.5 collective-permute-done.21
  72.0 1.3 %collective-permute-done.24 = bf16[4,32,640]{2,1,0:T(8,128)(2,1)S(1)} collective-permute-done((bf16[4,32,640]{2,1,0:T(8,128)(2,1)S(1)}, bf16[4,32,640]{2,1,0:T(8,128)(2,1)S(1)}, u32[]{:S(2)}, u32[]{:S(2)}) %collective-permute-start.24) | collective-permute-done | bytes 163872 | tf_op jit(solution)/shard_map/ppermute | solution.py:49
  73.4 1.4 %down.1 = (f32[16,512]{1,0:T(8,128)S(1)}, bf16[16,512]{1,0:T(8,128)(2,1)S(1)}, bf16[16,512]{1,0:T(8,128)(2,1)S(1)}, bf16[16,512]{1,0:T(8,128)(2,1)S(1)}) custom-call(bf16[8,32,640]{2,1,0:T(8,128)(2,1)S(1)} %constant_dynamic-update-slice_fusion.acts, f32[8,64]{1,0:T(8,128)S(1)} %get-tuple-element.58.stats, f32[64,128]{1,0:T(8,128)S(1)} %get-tuple-element.59.info, ...), custom_call_target="tpu_custom_call" | custom-call | tf_op jit(solution)/shard_map/down/pallas_call | solution.py:36
  74.8 1.4 %collective-permute-start.25 = (bf16[16,512]{1,0:T(8,128)(2,1)S(1)}, bf16[16,512]{1,0:T(8,128)(2,1)S(1)}, u32[]{:S(2)}, u32[]{:S(2)}) collective-permute-start(bf16[16,512]{1,0:T(8,128)(2,1)S(1)} %get-tuple-element.62), channel_id=1, source_target_pairs={{0,8},{8,0},{16,24},{24,16},{1,9},{9,1},{17,25},{25,17},{2,10},{10... | collective-permute-start | bytes 49160 | tf_op jit(solution)/shard_map/ppermute | solution.py:49
  76.1 1.4 %collective-permute-start.26 = (bf16[16,512]{1,0:T(8,128)(2,1)S(1)}, bf16[16,512]{1,0:T(8,128)(2,1)S(1)}, u32[]{:S(2)}, u32[]{:S(2)}) collective-permute-start(bf16[16,512]{1,0:T(8,128)(2,1)S(1)} %get-tuple-element.63), channel_id=1, source_target_pairs={{0,16},{8,24},{16,0},{24,8},{1,17},{9,25},{17,1},{25,9},{2,18},{10... | collective-permute-start | bytes 49160 | tf_op jit(solution)/shard_map/ppermute | solution.py:49
  77.6 1.3 %collective-permute-start.27 = (bf16[16,512]{1,0:T(8,128)(2,1)S(1)}, bf16[16,512]{1,0:T(8,128)(2,1)S(1)}, u32[]{:S(2)}, u32[]{:S(2)}) collective-permute-start(bf16[16,512]{1,0:T(8,128)(2,1)S(1)} %get-tuple-element.64), channel_id=1, source_target_pairs={{0,24},{8,16},{16,8},{24,0},{1,25},{9,17},{17,9},{25,1},{2,26},{10... | collective-permute-start | bytes 49160 | tf_op jit(solution)/shard_map/ppermute | solution.py:49
  78.9 1.0 %collective-permute-done.26.refs_2_ = bf16[16,512]{1,0:T(8,128)(2,1)S(1)} collective-permute-done((bf16[16,512]{1,0:T(8,128)(2,1)S(1)}, bf16[16,512]{1,0:T(8,128)(2,1)S(1)}, u32[]{:S(2)}, u32[]{:S(2)}) %collective-permute-start.26) | collective-permute-done | bytes 16416 | tf_op jit(solution)/shard_map/ppermute | solution.py:49
  79.9 2.3 %collective-permute-done.27.refs_3_ = bf16[16,512]{1,0:T(8,128)(2,1)S(1)} collective-permute-done((bf16[16,512]{1,0:T(8,128)(2,1)S(1)}, bf16[16,512]{1,0:T(8,128)(2,1)S(1)}, u32[]{:S(2)}, u32[]{:S(2)}) %collective-permute-start.27) | collective-permute-done | bytes 16416 | tf_op jit(solution)/shard_map/ppermute | solution.py:49
  82.4 1.2 %collective-permute-done.28 = f32[8,128]{1,0:T(8,128)S(1)} collective-permute-done((f32[8,128]{1,0:T(8,128)S(1)}, f32[8,128]{1,0:T(8,128)S(1)}, u32[]{:S(2)}, u32[]{:S(2)}) %collective-permute-start.28) | collective-permute-done | bytes 4128 | tf_op jit(solution)/shard_map/ppermute | solution.py:49
  83.5 2.6 %collective-permute-start.31 = (f32[8,128]{1,0:T(8,128)S(1)}, f32[8,128]{1,0:T(8,128)S(1)}, u32[]{:S(2)}, u32[]{:S(2)}) collective-permute-start(f32[8,128]{1,0:T(8,128)S(1)} %add.3.refs_2_), channel_id=1, source_target_pairs={{0,6},{1,7},{2,4},{3,5},{4,2},{5,3},{6,0},{7,1},{8,14},{9,15},{10,... | collective-permute-start | bytes 12296 | tf_op jit(solution)/shard_map/ppermute | solution.py:49
  86.1 1.8 %collective-permute-start.29 = (f32[8,128]{1,0:T(8,128)S(1)}, f32[8,128]{1,0:T(8,128)S(1)}, u32[]{:S(2)}, u32[]{:S(2)}) collective-permute-start(f32[8,128]{1,0:T(8,128)S(1)} %add.3.refs_2_), channel_id=1, source_target_pairs={{0,2},{1,3},{2,0},{3,1},{4,6},{5,7},{6,4},{7,5},{8,10},{9,11},{10,... | collective-permute-start | bytes 12296 | tf_op jit(solution)/shard_map/ppermute | solution.py:49
  87.9 1.0 %collective-permute-done.31.refs_5_ = f32[8,128]{1,0:T(8,128)S(1)} collective-permute-done((f32[8,128]{1,0:T(8,128)S(1)}, f32[8,128]{1,0:T(8,128)S(1)}, u32[]{:S(2)}, u32[]{:S(2)}) %collective-permute-start.31) | collective-permute-done | bytes 4128 | tf_op jit(solution)/shard_map/ppermute | solution.py:49
  88.9 1.7 %collective-permute-done.30.refs_4_ = f32[8,128]{1,0:T(8,128)S(1)} collective-permute-done((f32[8,128]{1,0:T(8,128)S(1)}, f32[8,128]{1,0:T(8,128)S(1)}, u32[]{:S(2)}, u32[]{:S(2)}) %collective-permute-start.30) | collective-permute-done | bytes 4128 | tf_op jit(solution)/shard_map/ppermute | solution.py:49
  90.6 0.7 norm.1
  (68 shorter events, 0.7 us)
Async XLA Ops:
  0.0 10.7 %copy-start = (bf16[1024,512]{1,0:T(8,128)(2,1)S(1)}, bf16[1024,512]{1,0:T(8,128)(2,1)}, u32[]{:S(2)}) copy-start(bf16[1024,512]{1,0:T(8,128)(2,1)} %refs_4_.2) | copy-start | bytes 3145732
  0.0 10.7 %copy-start.2 = (bf16[1024,256]{1,0:T(8,128)(2,1)S(1)}, bf16[1024,256]{1,0:T(8,128)(2,1)}, u32[]{:S(2)}) copy-start(bf16[1024,256]{1,0:T(8,128)(2,1)} %refs_5_.1) | copy-start | bytes 1572868
  0.0 10.7 %copy-start.3 = (bf16[1024,256]{1,0:T(8,128)(2,1)S(1)}, bf16[1024,256]{1,0:T(8,128)(2,1)}, u32[]{:S(2)}) copy-start(bf16[1024,256]{1,0:T(8,128)(2,1)} %refs_6_.1) | copy-start | bytes 1572868
  0.0 14.7 %copy-start.11 = (s32[16]{0:T(128)S(1)}, s32[16]{0:T(128)}, u32[]{:S(2)}) copy-start(s32[16]{0:T(128)} %lengths.3) | copy-start | bytes 196
  0.0 16.6 %copy-start.9 = (bf16[16,1024,2,128]{3,2,1,0:T(2,128)(2,1)S(1)}, bf16[16,1024,2,128]{3,2,1,0:T(2,128)(2,1)}, u32[]{:S(2)}) copy-start(bf16[16,1024,2,128]{3,2,1,0:T(2,128)(2,1)} %param.28) | copy-start | bytes 25165828
  0.0 16.6 %copy-start.10 = (bf16[16,1024,2,128]{3,2,1,0:T(2,128)(2,1)S(1)}, bf16[16,1024,2,128]{3,2,1,0:T(2,128)(2,1)}, u32[]{:S(2)}) copy-start(bf16[16,1024,2,128]{3,2,1,0:T(2,128)(2,1)} %param.29) | copy-start | bytes 25165828
  0.0 16.6 %copy-start.12 = (f32[4]{0:T(128)S(1)}, f32[4]{0:T(128)}, u32[]{:S(2)}) copy-start(f32[4]{0:T(128)} %lambdas.1) | copy-start | bytes 52
  0.0 16.6 %copy-start.13 = (f32[128]{0:T(128)S(1)}, f32[128]{0:T(128)}, u32[]{:S(2)}) copy-start(f32[128]{0:T(128)} %param.27) | copy-start | bytes 1540
  1.2 5.0 %collective-permute-start = (bf16[16,1152]{1,0:T(8,128)(2,1)S(1)}, bf16[16,1152]{1,0:T(8,128)(2,1)S(1)}, u32[]{:S(2)}, u32[]{:S(2)}) collective-permute-start(bf16[16,1152]{1,0:T(8,128)(2,1)S(1)} %get-tuple-element.37), channel_id=1, source_target_pairs={{0,8},{8,0},{16,24},{24,16},{1,9},{9,1},{17,25},{25,17},{2,10},{10... | collective-permute-start | bytes 110600 | tf_op jit(solution)/shard_map/ppermute | solution.py:49
  4.3 4.0 %collective-permute-start.1 = (bf16[16,1152]{1,0:T(8,128)(2,1)S(1)}, bf16[16,1152]{1,0:T(8,128)(2,1)S(1)}, u32[]{:S(2)}, u32[]{:S(2)}) collective-permute-start(bf16[16,1152]{1,0:T(8,128)(2,1)S(1)} %get-tuple-element.38), channel_id=1, source_target_pairs={{0,16},{8,24},{16,0},{24,8},{1,17},{9,25},{17,1},{25,9},{2,18},{10... | collective-permute-start | bytes 110600 | tf_op jit(solution)/shard_map/ppermute | solution.py:49
  5.8 4.9 %collective-permute-start.2 = (bf16[16,1152]{1,0:T(8,128)(2,1)S(1)}, bf16[16,1152]{1,0:T(8,128)(2,1)S(1)}, u32[]{:S(2)}, u32[]{:S(2)}) collective-permute-start(bf16[16,1152]{1,0:T(8,128)(2,1)S(1)} %get-tuple-element.39), channel_id=1, source_target_pairs={{0,24},{8,16},{16,8},{24,0},{1,25},{9,17},{17,9},{25,1},{2,26},{10... | collective-permute-start | bytes 110600 | tf_op jit(solution)/shard_map/ppermute | solution.py:49
  10.7 35.9 %slice-start = ((s8[8388608]{0:T(1024)(128)(4,1)}), s8[4194304]{0:T(1024)(128)(4,1)S(1)}, s32[]{:S(2)}) async-start(s8[8388608]{0:T(1024)(128)(4,1)} %bitcast.7), calls=%async_computation | async-start | bytes 8388608
  11.2 4.2 %collective-permute-start.3 = (bf16[16,1024]{1,0:T(8,128)(2,1)S(1)}, bf16[16,1024]{1,0:T(8,128)(2,1)S(1)}, u32[]{:S(2)}, u32[]{:S(2)}) collective-permute-start(bf16[16,1024]{1,0:T(8,128)(2,1)S(1)} %get-tuple-element.41), channel_id=1, source_target_pairs={{0,8},{8,0},{16,24},{24,16},{1,9},{9,1},{17,25},{25,17},{2,10},{10... | collective-permute-start | bytes 98312 | tf_op jit(solution)/shard_map/ppermute | solution.py:49
  11.8 3.9 %collective-permute-start.4 = (bf16[16,1024]{1,0:T(8,128)(2,1)S(1)}, bf16[16,1024]{1,0:T(8,128)(2,1)S(1)}, u32[]{:S(2)}, u32[]{:S(2)}) collective-permute-start(bf16[16,1024]{1,0:T(8,128)(2,1)S(1)} %get-tuple-element.42), channel_id=1, source_target_pairs={{0,16},{8,24},{16,0},{24,8},{1,17},{9,25},{17,1},{25,9},{2,18},{10... | collective-permute-start | bytes 98312 | tf_op jit(solution)/shard_map/ppermute | solution.py:49
  11.8 4.8 %collective-permute-start.5 = (bf16[16,1024]{1,0:T(8,128)(2,1)S(1)}, bf16[16,1024]{1,0:T(8,128)(2,1)S(1)}, u32[]{:S(2)}, u32[]{:S(2)}) collective-permute-start(bf16[16,1024]{1,0:T(8,128)(2,1)S(1)} %get-tuple-element.43), channel_id=1, source_target_pairs={{0,24},{8,16},{16,8},{24,0},{1,25},{9,17},{17,9},{25,1},{2,26},{10... | collective-permute-start | bytes 98312 | tf_op jit(solution)/shard_map/ppermute | solution.py:49
  16.6 32.0 %slice-start.2 = ((s8[8388608]{0:T(1024)(128)(4,1)}), s8[4194304]{0:T(1024)(128)(4,1)S(1)}, s32[]{:S(2)}) async-start(s8[8388608]{0:T(1024)(128)(4,1)} %bitcast.9), calls=%async_computation.2 | async-start | bytes 8388608
  16.7 11.7 %copy-start.1 = (bf16[512,1024]{1,0:T(8,128)(2,1)S(1)}, bf16[512,1024]{1,0:T(8,128)(2,1)}, u32[]{:S(2)}) copy-start(bf16[512,1024]{1,0:T(8,128)(2,1)} %refs_4_.3) | copy-start | bytes 3145732
  16.7 28.0 %copy-start.14 = (bf16[4096]{0:T(1024)(128)(2,1)S(1)}, bf16[4096]{0:T(1024)(128)(2,1)}, u32[]{:S(2)}) copy-start(bf16[4096]{0:T(1024)(128)(2,1)} %param.41) | copy-start | bytes 24580
  16.7 29.9 %slice-start.1 = ((s8[8388608]{0:T(1024)(128)(4,1)}), s8[4194304]{0:T(1024)(128)(4,1)S(1)}, s32[]{:S(2)}) async-start(s8[8388608]{0:T(1024)(128)(4,1)} %bitcast.7), calls=%async_computation.1 | async-start | bytes 8388608
  16.7 29.9 %copy-start.4 = (bf16[512,512]{1,0:T(8,128)(2,1)S(1)}, bf16[512,512]{1,0:T(8,128)(2,1)}, u32[]{:S(2)}) copy-start(bf16[512,512]{1,0:T(8,128)(2,1)} %refs_8_.3) | copy-start | bytes 1572868
  16.7 29.9 %copy-start.7 = (f32[4096]{0:T(1024)S(1)}, f32[4096]{0:T(1024)}, u32[]{:S(2)}) copy-start(f32[4096]{0:T(1024)} %param.31) | copy-start | bytes 49156
  16.7 31.9 %slice-start.3 = ((s8[8388608]{0:T(1024)(128)(4,1)}), s8[4194304]{0:T(1024)(128)(4,1)S(1)}, s32[]{:S(2)}) async-start(s8[8388608]{0:T(1024)(128)(4,1)} %bitcast.9), calls=%async_computation.3 | async-start | bytes 8388608
  21.1 27.5 %copy-start.5 = (bf16[512,512]{1,0:T(8,128)(2,1)S(1)}, bf16[512,512]{1,0:T(8,128)(2,1)}, u32[]{:S(2)}) copy-start(bf16[512,512]{1,0:T(8,128)(2,1)} %refs_8_.2) | copy-start | bytes 1572868
  21.1 4.7 %collective-permute-start.8 = (bf16[16,512]{1,0:T(8,128)(2,1)S(1)}, bf16[16,512]{1,0:T(8,128)(2,1)S(1)}, u32[]{:S(2)}, u32[]{:S(2)}) collective-permute-start(bf16[16,512]{1,0:T(8,128)(2,1)S(1)} %attend.1.refs_0_), channel_id=1, source_target_pairs={{0,24},{8,16},{16,8},{24,0},{1,25},{9,17},{17,9},{25,1},{2,26},{10... | collective-permute-start | bytes 49160 | tf_op jit(solution)/shard_map/ppermute | solution.py:49
  24.1 3.7 %collective-permute-start.7 = (bf16[16,512]{1,0:T(8,128)(2,1)S(1)}, bf16[16,512]{1,0:T(8,128)(2,1)S(1)}, u32[]{:S(2)}, u32[]{:S(2)}) collective-permute-start(bf16[16,512]{1,0:T(8,128)(2,1)S(1)} %attend.1.refs_0_), channel_id=1, source_target_pairs={{0,16},{8,24},{16,0},{24,8},{1,17},{9,25},{17,1},{25,9},{2,18},{10... | collective-permute-start | bytes 49160 | tf_op jit(solution)/shard_map/ppermute | solution.py:49
  24.6 3.7 %collective-permute-start.6 = (bf16[16,512]{1,0:T(8,128)(2,1)S(1)}, bf16[16,512]{1,0:T(8,128)(2,1)S(1)}, u32[]{:S(2)}, u32[]{:S(2)}) collective-permute-start(bf16[16,512]{1,0:T(8,128)(2,1)S(1)} %attend.1.refs_0_), channel_id=1, source_target_pairs={{0,8},{8,0},{16,24},{24,16},{1,9},{9,1},{17,25},{25,17},{2,10},{10... | collective-permute-start | bytes 49160 | tf_op jit(solution)/shard_map/ppermute | solution.py:49
  28.6 1.3 %collective-permute-start.9 = (bf16[64,512]{1,0:T(8,128)(2,1)S(1)}, bf16[64,512]{1,0:T(8,128)(2,1)S(1)}, u32[]{:S(2)}, u32[]{:S(2)}) collective-permute-start(bf16[64,512]{1,0:T(8,128)(2,1)S(1)} %get-tuple-element.47), channel_id=1, source_target_pairs={{0,1},{1,0},{2,3},{3,2},{4,5},{5,4},{6,7},{7,6},{8,9},{9,8},{10,11... | collective-permute-start | bytes 196616 | tf_op jit(solution)/shard_map/ppermute | solution.py:49
  30.0 8.0 %collective-permute-start.12 = (bf16[64,512]{1,0:T(8,128)(2,1)S(1)}, bf16[64,512]{1,0:T(8,128)(2,1)S(1)}, u32[]{:S(2)}, u32[]{:S(2)}) collective-permute-start(bf16[64,512]{1,0:T(8,128)(2,1)S(1)} %pairsum.1.refs_0_), channel_id=1, source_target_pairs={{6,0},{7,1},{12,10},{13,11},{18,20},{19,21},{24,30},{25,31}} | collective-permute-start | bytes 196616 | tf_op jit(solution)/shard_map/ppermute | solution.py:694
  31.3 8.1 %collective-permute-start.11 = (bf16[64,512]{1,0:T(8,128)(2,1)S(1)}, bf16[64,512]{1,0:T(8,128)(2,1)S(1)}, u32[]{:S(2)}, u32[]{:S(2)}) collective-permute-start(bf16[64,512]{1,0:T(8,128)(2,1)S(1)} %pairsum.1.refs_0_), channel_id=1, source_target_pairs={{4,0},{5,1},{14,10},{15,11},{16,20},{17,21},{26,30},{27,31}} | collective-permute-start | bytes 196616 | tf_op jit(solution)/shard_map/ppermute | solution.py:694
  32.6 8.1 %collective-permute-start.10 = (bf16[64,512]{1,0:T(8,128)(2,1)S(1)}, bf16[64,512]{1,0:T(8,128)(2,1)S(1)}, u32[]{:S(2)}, u32[]{:S(2)}) collective-permute-start(bf16[64,512]{1,0:T(8,128)(2,1)S(1)} %pairsum.1.refs_0_), channel_id=1, source_target_pairs={{2,0},{3,1},{8,10},{9,11},{22,20},{23,21},{28,30},{29,31}} | collective-permute-start | bytes 196616 | tf_op jit(solution)/shard_map/ppermute | solution.py:694
  40.8 4.2 %collective-permute-start.15 = (bf16[64,512]{1,0:T(8,128)(2,1)S(1)}, bf16[64,512]{1,0:T(8,128)(2,1)S(1)}, u32[]{:S(2)}, u32[]{:S(2)}) collective-permute-start(bf16[64,512]{1,0:T(8,128)(2,1)S(1)} %residual.1.refs_0_), channel_id=1, source_target_pairs={{0,24},{1,25},{10,18},{11,19},{20,12},{21,13},{30,6},{31,7}} | collective-permute-start | bytes 196616 | tf_op jit(solution)/shard_map/ppermute | solution.py:706
  42.1 3.2 %collective-permute-start.14 = (bf16[64,512]{1,0:T(8,128)(2,1)S(1)}, bf16[64,512]{1,0:T(8,128)(2,1)S(1)}, u32[]{:S(2)}, u32[]{:S(2)}) collective-permute-start(bf16[64,512]{1,0:T(8,128)(2,1)S(1)} %residual.1.refs_0_), channel_id=1, source_target_pairs={{0,16},{1,17},{10,26},{11,27},{20,4},{21,5},{30,14},{31,15}} | collective-permute-start | bytes 196616 | tf_op jit(solution)/shard_map/ppermute | solution.py:706
  43.4 3.2 %collective-permute-start.13 = (bf16[64,512]{1,0:T(8,128)(2,1)S(1)}, bf16[64,512]{1,0:T(8,128)(2,1)S(1)}, u32[]{:S(2)}, u32[]{:S(2)}) collective-permute-start(bf16[64,512]{1,0:T(8,128)(2,1)S(1)} %residual.1.refs_0_), channel_id=1, source_target_pairs={{0,8},{1,9},{10,2},{11,3},{20,28},{21,29},{30,22},{31,23}} | collective-permute-start | bytes 196616 | tf_op jit(solution)/shard_map/ppermute | solution.py:706
  46.6 26.7 %slice-start.4 = ((s8[8388608]{0:T(1024)(128)(4,1)}), s8[4194304]{0:T(1024)(128)(4,1)S(1)}, s32[]{:S(2)}) async-start(s8[8388608]{0:T(1024)(128)(4,1)} %bitcast.11), calls=%async_computation.4 | async-start | bytes 8388608
  46.6 26.7 %copy-start.6 = (bf16[512,512]{1,0:T(8,128)(2,1)S(1)}, bf16[512,512]{1,0:T(8,128)(2,1)}, u32[]{:S(2)}) copy-start(bf16[512,512]{1,0:T(8,128)(2,1)} %dense_down.1) | copy-start | bytes 1572868
  48.5 24.9 %slice-start.5 = ((s8[8388608]{0:T(1024)(128)(4,1)}), s8[4194304]{0:T(1024)(128)(4,1)S(1)}, s32[]{:S(2)}) async-start(s8[8388608]{0:T(1024)(128)(4,1)} %bitcast.11), calls=%async_computation.5 | async-start | bytes 8388608
  48.5 42.1 %copy-start.8 = (f32[512]{0:T(512)S(1)}, f32[512]{0:T(512)}, u32[]{:S(2)}) copy-start(f32[512]{0:T(512)} %param.32) | copy-start | bytes 6148
  48.5 2.5 %collective-permute-start.17 = (bf16[72,1280]{1,0:T(8,128)(2,1)S(1)}, bf16[72,1280]{1,0:T(8,128)(2,1)S(1)}, u32[]{:S(2)}, u32[]{:S(2)}) collective-permute-start(bf16[72,1280]{1,0:T(8,128)(2,1)S(1)} %get-tuple-element.52), channel_id=1, source_target_pairs={{0,1},{1,0},{2,3},{3,2},{4,5},{5,4},{6,7},{7,6},{8,9},{9,8},{10,11... | collective-permute-start | bytes 552968 | tf_op jit(solution)/shard_map/ppermute | solution.py:49
  50.5 1.6 %collective-permute-start.16 = (bf16[72,1280]{1,0:T(8,128)(2,1)S(1)}, bf16[72,1280]{1,0:T(8,128)(2,1)S(1)}, u32[]{:S(2)}, u32[]{:S(2)}) collective-permute-start(bf16[72,1280]{1,0:T(8,128)(2,1)S(1)} %get-tuple-element.51), channel_id=1, source_target_pairs={{0,1},{1,0},{2,3},{3,2},{4,5},{5,4},{6,7},{7,6},{8,9},{9,8},{10,11... | collective-permute-start | bytes 552968 | tf_op jit(solution)/shard_map/ppermute | solution.py:49
  52.2 5.1 %collective-permute-start.18 = (bf16[72,640]{1,0:T(8,128)(2,1)S(1)}, bf16[72,640]{1,0:T(8,128)(2,1)S(1)}, u32[]{:S(2)}, u32[]{:S(2)}) collective-permute-start(bf16[72,640]{1,0:T(8,128)(2,1)S(1)} %get-tuple-element.54), channel_id=1, source_target_pairs={{0,2},{1,3},{2,0},{3,1},{4,6},{5,7},{6,4},{7,5},{8,10},{9,11},{10,... | collective-permute-start | bytes 276488 | tf_op jit(solution)/shard_map/ppermute | solution.py:49
  54.1 10.1 %collective-permute-start.19 = (bf16[72,640]{1,0:T(8,128)(2,1)S(1)}, bf16[72,640]{1,0:T(8,128)(2,1)S(1)}, u32[]{:S(2)}, u32[]{:S(2)}) collective-permute-start(bf16[72,640]{1,0:T(8,128)(2,1)S(1)} %get-tuple-element.55), channel_id=1, source_target_pairs={{0,4},{1,5},{2,6},{3,7},{4,0},{5,1},{6,2},{7,3},{8,12},{9,13},{10,... | collective-permute-start | bytes 276488 | tf_op jit(solution)/shard_map/ppermute | solution.py:49
  55.8 8.5 %collective-permute-start.20 = (bf16[72,640]{1,0:T(8,128)(2,1)S(1)}, bf16[72,640]{1,0:T(8,128)(2,1)S(1)}, u32[]{:S(2)}, u32[]{:S(2)}) collective-permute-start(bf16[72,640]{1,0:T(8,128)(2,1)S(1)} %get-tuple-element.56), channel_id=1, source_target_pairs={{0,6},{1,7},{2,4},{3,5},{4,2},{5,3},{6,0},{7,1},{8,14},{9,15},{10,... | collective-permute-start | bytes 276488 | tf_op jit(solution)/shard_map/ppermute | solution.py:49
  64.4 6.0 %collective-permute-start.23 = (bf16[1,32,640]{2,1,0:T(8,128)(2,1)S(1)}, bf16[1,32,640]{2,1,0:T(8,128)(2,1)S(1)}, u32[]{:S(2)}, u32[]{:S(2)}) collective-permute-start(bf16[1,32,640]{2,1,0:T(8,128)(2,1)S(1)} %get-tuple-element.57), channel_id=1, source_target_pairs={{0,6},{1,7},{2,4},{3,5},{4,2},{5,3},{6,0},{7,1},{8,14},{9,15},{10,... | collective-permute-start | bytes 122888 | tf_op jit(solution)/shard_map/ppermute | solution.py:49
  65.9 5.4 %collective-permute-start.22 = (bf16[1,32,640]{2,1,0:T(8,128)(2,1)S(1)}, bf16[1,32,640]{2,1,0:T(8,128)(2,1)S(1)}, u32[]{:S(2)}, u32[]{:S(2)}) collective-permute-start(bf16[1,32,640]{2,1,0:T(8,128)(2,1)S(1)} %get-tuple-element.57), channel_id=1, source_target_pairs={{0,4},{1,5},{2,6},{3,7},{4,0},{5,1},{6,2},{7,3},{8,12},{9,13},{10,... | collective-permute-start | bytes 122888 | tf_op jit(solution)/shard_map/ppermute | solution.py:49
  67.8 4.0 %collective-permute-start.21 = (bf16[1,32,640]{2,1,0:T(8,128)(2,1)S(1)}, bf16[1,32,640]{2,1,0:T(8,128)(2,1)S(1)}, u32[]{:S(2)}, u32[]{:S(2)}) collective-permute-start(bf16[1,32,640]{2,1,0:T(8,128)(2,1)S(1)} %get-tuple-element.57), channel_id=1, source_target_pairs={{0,2},{1,3},{2,0},{3,1},{4,6},{5,7},{6,4},{7,5},{8,10},{9,11},{10,... | collective-permute-start | bytes 122888 | tf_op jit(solution)/shard_map/ppermute | solution.py:49
  71.9 1.5 %collective-permute-start.24 = (bf16[4,32,640]{2,1,0:T(8,128)(2,1)S(1)}, bf16[4,32,640]{2,1,0:T(8,128)(2,1)S(1)}, u32[]{:S(2)}, u32[]{:S(2)}) collective-permute-start(bf16[4,32,640]{2,1,0:T(8,128)(2,1)S(1)} %pad_maximum_fusion), channel_id=1, source_target_pairs={{0,1},{1,0},{2,3},{3,2},{4,5},{5,4},{6,7},{7,6},{8,9},{9,8},{10,11... | collective-permute-start | bytes 491528 | tf_op jit(solution)/shard_map/ppermute | solution.py:49
  74.8 4.1 %collective-permute-start.25 = (bf16[16,512]{1,0:T(8,128)(2,1)S(1)}, bf16[16,512]{1,0:T(8,128)(2,1)S(1)}, u32[]{:S(2)}, u32[]{:S(2)}) collective-permute-start(bf16[16,512]{1,0:T(8,128)(2,1)S(1)} %get-tuple-element.62), channel_id=1, source_target_pairs={{0,8},{8,0},{16,24},{24,16},{1,9},{9,1},{17,25},{25,17},{2,10},{10... | collective-permute-start | bytes 49160 | tf_op jit(solution)/shard_map/ppermute | solution.py:49
  76.1 3.7 %collective-permute-start.26 = (bf16[16,512]{1,0:T(8,128)(2,1)S(1)}, bf16[16,512]{1,0:T(8,128)(2,1)S(1)}, u32[]{:S(2)}, u32[]{:S(2)}) collective-permute-start(bf16[16,512]{1,0:T(8,128)(2,1)S(1)} %get-tuple-element.63), channel_id=1, source_target_pairs={{0,16},{8,24},{16,0},{24,8},{1,17},{9,25},{17,1},{25,9},{2,18},{10... | collective-permute-start | bytes 49160 | tf_op jit(solution)/shard_map/ppermute | solution.py:49
  77.6 4.6 %collective-permute-start.27 = (bf16[16,512]{1,0:T(8,128)(2,1)S(1)}, bf16[16,512]{1,0:T(8,128)(2,1)S(1)}, u32[]{:S(2)}, u32[]{:S(2)}) collective-permute-start(bf16[16,512]{1,0:T(8,128)(2,1)S(1)} %get-tuple-element.64), channel_id=1, source_target_pairs={{0,24},{8,16},{16,8},{24,0},{1,25},{9,17},{17,9},{25,1},{2,26},{10... | collective-permute-start | bytes 49160 | tf_op jit(solution)/shard_map/ppermute | solution.py:49
  82.3 1.2 %collective-permute-start.28 = (f32[8,128]{1,0:T(8,128)S(1)}, f32[8,128]{1,0:T(8,128)S(1)}, u32[]{:S(2)}, u32[]{:S(2)}) collective-permute-start(f32[8,128]{1,0:T(8,128)S(1)} %get-tuple-element.66), channel_id=1, source_target_pairs={{0,1},{1,0},{2,3},{3,2},{4,5},{5,4},{6,7},{7,6},{8,9},{9,8},{10,11... | collective-permute-start | bytes 12296 | tf_op jit(solution)/shard_map/ppermute | solution.py:49
  83.5 5.4 %collective-permute-start.31 = (f32[8,128]{1,0:T(8,128)S(1)}, f32[8,128]{1,0:T(8,128)S(1)}, u32[]{:S(2)}, u32[]{:S(2)}) collective-permute-start(f32[8,128]{1,0:T(8,128)S(1)} %add.3.refs_2_), channel_id=1, source_target_pairs={{0,6},{1,7},{2,4},{3,5},{4,2},{5,3},{6,0},{7,1},{8,14},{9,15},{10,... | collective-permute-start | bytes 12296 | tf_op jit(solution)/shard_map/ppermute | solution.py:49
  86.1 4.5 %collective-permute-start.30 = (f32[8,128]{1,0:T(8,128)S(1)}, f32[8,128]{1,0:T(8,128)S(1)}, u32[]{:S(2)}, u32[]{:S(2)}) collective-permute-start(f32[8,128]{1,0:T(8,128)S(1)} %add.3.refs_2_), channel_id=1, source_target_pairs={{0,4},{1,5},{2,6},{3,7},{4,0},{5,1},{6,2},{7,3},{8,12},{9,13},{10,... | collective-permute-start | bytes 12296 | tf_op jit(solution)/shard_map/ppermute | solution.py:49
  86.1 4.5 %collective-permute-start.29 = (f32[8,128]{1,0:T(8,128)S(1)}, f32[8,128]{1,0:T(8,128)S(1)}, u32[]{:S(2)}, u32[]{:S(2)}) collective-permute-start(f32[8,128]{1,0:T(8,128)S(1)} %add.3.refs_2_), channel_id=1, source_target_pairs={{0,2},{1,3},{2,0},{3,1},{4,6},{5,7},{6,4},{7,5},{8,10},{9,11},{10,... | collective-permute-start | bytes 12296 | tf_op jit(solution)/shard_map/ppermute | solution.py:49
